TPU v7x, 256 devices: a whole 4x4x8 slice. The times are simulated.
256 devices in a mesh: sp: 32 (over z, x), tp: 8 (over y, core).
Axes of the slice: x: 4, y: 4, z: 8, core: 2. Of those that a mesh axis runs over, the one named last changes fastest.
Arguments:
- residual: bfloat16 [24576, 2048], P(('sp', 'tp')), may hold values from -6 to 6
- queries: bfloat16 [24576, 1024], P('sp', 'tp'), may hold values from -6 to 6
- key_rows: bfloat16 [24576, 1024], P('sp', 'tp'), may hold values from -6 to 6
- value_rows: bfloat16 [24576, 1024], P('sp', 'tp'), may hold values from -6 to 6
- gate_rows: bfloat16 [24576, 1024], P('sp', 'tp'), may hold values from -6 to 6
- log_decay: float32 [8, 24576], P('tp', 'sp'), may hold values from -1.7 to 0, as said below
- out_gain: float32 [1024], P('tp'), may hold values from 0.1 to 1.9
- out_weight: bfloat16 [1024, 2048], P('tp'), may hold values from -0.1875 to 0.1875
- norm_gain: float32 [2048], replicated, may hold values from 0.1 to 1.9
- expert_gate: bfloat16 [32, 2048, 4096], P('sp', None, 'tp'), may hold values from -0.125 to 0.125
- expert_up: bfloat16 [32, 2048, 4096], P('sp', None, 'tp'), may hold values from -0.125 to 0.125
- expert_down: bfloat16 [32, 4096, 2048], P('sp', 'tp'), may hold values from -0.09375 to 0.09375
- routes: int32 [24576, 2], P(('sp', 'tp')), may hold values from 0 to 31, all different within a row; in each aligned block of 96 rows (0 to 95, 96 to 191, ...) at most 7 rows name the same one
- route_weight: float32 [24576, 2], P(('sp', 'tp')), may hold values from 0.2 to 1
Outputs:
- layer_out: bfloat16 [24576, 2048], P(('sp', 'tp'))
Inputs may be any that keep to these rules, and one draw needn't show every extreme that they name: `log_decay`: every entry is negative. `routes`: among the 96 rows of one device no expert is named by more than 7 rows; the experts of one row differ.
All inputs are finite; a program needn't handle non-finite values.
Results may differ from a plain program's by a relative error of at most 0.015.
Values may be sent and summed in bfloat16 or wider, within the bound.
No kernel may reach another device: no remote copies, remote signals or barrier semaphores. Data moves between devices by JAX's collectives and lax.ppermute only.
A program may use at most 128 MiB of HBM per device.

v0:
```python
import jax
import jax.numpy as jnp
from jax import lax
from jax.experimental import pallas as pl
from jax.experimental.pallas import tpu as pltpu
from jax.sharding import Mesh
from jax.sharding import PartitionSpec as P


SP = ("sp_0", "sp_1")
SP_TP = ("sp_0", "sp_1", "tp")


epsilon = 1e-06
rope_base = 10000.0
BF = jnp.bfloat16
F32 = jnp.float32

OTHER_CORE = [(i, i ^ 1) for i in range(8)]
UP = [(i, (i + 2) % 8) for i in range(8)]
DOWN = [(i, (i - 2) % 8) for i in range(8)]
ACROSS = [(i, (i + 4) % 8) for i in range(8)]

SLOTS = 8
USED = 7
UNIT = 16
BLOCK = 256


def dot(a, b):
    return jnp.dot(a, b, preferred_element_type=F32)


def vmem_call(kernel, out_shape, limit=12 * 1024 * 1024, **kwargs):
    return pl.pallas_call(
        kernel,
        out_shape=out_shape,
        compiler_params=pltpu.CompilerParams(vmem_limit_bytes=limit),
        **kwargs,
    )


def onehot(mask):
    return jnp.where(mask, 1.0, 0.0).astype(BF)


def by_block(size):
    peers = size // SLOTS
    to = lax.broadcasted_iota(jnp.int32, (size, size), 0)
    source = lax.broadcasted_iota(jnp.int32, (size, size), 1)
    return onehot(source == (to & (peers - 1)) * SLOTS + to // peers)


def by_peer(size):
    peers = size // SLOTS
    to = lax.broadcasted_iota(jnp.int32, (size, size), 0)
    source = lax.broadcasted_iota(jnp.int32, (size, size), 1)
    return onehot(source == (to & 7) * peers + to // SLOTS)


def slot_of_row(shape, dim, peers):
    row = lax.broadcasted_iota(jnp.int32, shape, dim)
    return (row & (peers - 1)) * SLOTS + row // peers


def project_and_pack_kernel(*refs):
    mine_ref, others_ref = refs[:2]
    weights = refs[2:10]
    residual_ref, gain_ref, slot_ref, hidden_ref, out_ref, turned = refs[10:]
    tokens, width = residual_ref.shape
    size = out_ref.shape[0]
    peers = size // SLOTS
    heads = jnp.concatenate([ref[k] for ref in (mine_ref, others_ref) for k in range(4)], axis=1)
    squares = jnp.zeros((tokens, 1), F32)
    step = 512
    for start in range(0, width, step):
        columns = slice(start, start + step)
        projected = dot(heads, jnp.concatenate([w[:, columns] for w in weights], axis=0))
        hidden = (residual_ref[:, columns].astype(F32) + projected).astype(BF)
        hidden_ref[:, columns] = hidden
        hidden_f = hidden.astype(F32)
        squares = squares + jnp.sum(hidden_f * hidden_f, axis=1, keepdims=True)
    scale = lax.rsqrt(squares / width + epsilon)
    slot = slot_of_row((USED * peers, tokens), 0, peers)
    chosen = onehot((slot == slot_ref[0:1, :]) | (slot == slot_ref[1:2, :]))
    for i in range(SLOTS):
        columns = slice(i * BLOCK, (i + 1) * BLOCK)
        normed = hidden_ref[:, columns].astype(F32) * scale * gain_ref[:, columns]
        picked = dot(chosen, normed.astype(BF)).astype(BF)
        for c in range(USED):
            turned[i * peers : (i + 1) * peers, c * BLOCK : (c + 1) * BLOCK] = picked[
                c * peers : (c + 1) * peers, :
            ]
    out_ref[...] = dot(by_peer(size), turned[...]).astype(BF)


def units(refs):
    for ref in refs:
        for start in range(0, ref.shape[0], UNIT):
            yield ref, slice(start, start + UNIT)


def unpack(in_ref, *out_refs):
    size = in_ref.shape[0]
    peers = size // SLOTS
    order = by_block(size)
    places = list(units(out_refs))
    each = peers // UNIT
    for c in range(in_ref.shape[1] // BLOCK):
        rows = dot(order, in_ref[:, c * BLOCK : (c + 1) * BLOCK]).astype(BF)
        for k in range(each):
            ref, place = places[c * each + k]
            for i in range(SLOTS):
                start = i * peers + k * UNIT
                ref[place, i * BLOCK : (i + 1) * BLOCK] = rows[start : start + UNIT, :]


def unpack_rows_kernel(in_ref, low_ref, high_ref, both_ref):
    unpack(in_ref, low_ref, high_ref)
    half = low_ref.shape[0]
    both_ref[:half, :] = low_ref[...]
    both_ref[half:, :] = high_ref[...]


def repack_rows_kernel(low_ref, high_ref, core_ref, *refs):
    *chips, out_ref, turned = refs
    size = out_ref.shape[0]
    peers = size // SLOTS
    each = peers // UNIT
    sources = [(low_ref, high_ref), (core_ref,), chips[0::2], chips[1::2]]
    for u, parts in enumerate(zip(*map(units, sources))):
        total = sum(ref[place, :].astype(F32) for ref, place in parts).astype(BF)
        c, start = u // each, u % each * UNIT
        for i in range(SLOTS):
            turned[i * peers + start : i * peers + start + UNIT, c * BLOCK : (c + 1) * BLOCK] = (
                total[:, i * BLOCK : (i + 1) * BLOCK]
            )
    out_ref[...] = dot(by_peer(size), turned[...]).astype(BF)


def add_kernel(own_ref, core_ref, *refs, start):
    *more, out_ref = refs
    total = own_ref[...].astype(F32) + core_ref[start : start + own_ref.shape[0], :].astype(F32)
    for ref in more:
        total = total + ref[...].astype(F32)
    out_ref[...] = total.astype(BF)


def add(own, core, second, *more):
    return vmem_call(
        lambda *refs: add_kernel(*refs, start=own.shape[0] * second),
        jax.ShapeDtypeStruct(own.shape, BF),
    )(own, core, *more)


def route_rows_kernel(slot_ref, weight_ref, high_ref, low_ref):
    slot = slot_of_row(high_ref.shape, 1, high_ref.shape[1] // USED)
    weight = sum(
        jnp.where(slot == slot_ref[:, k : k + 1], weight_ref[:, k : k + 1], 0.0) for k in (0, 1)
    )
    high = weight.astype(BF)
    high_ref[...] = high
    low_ref[...] = (weight - high.astype(F32)).astype(BF)


def combine_kernel(rows_ref, hidden_ref, high_ref, low_ref, out_ref, rows):
    unpack(rows_ref, rows)
    for i in range(SLOTS):
        columns = slice(i * BLOCK, (i + 1) * BLOCK)
        block = rows[:, columns]
        got = dot(high_ref[...], block) + dot(low_ref[...], block)
        out_ref[:, columns] = (hidden_ref[:, columns].astype(F32) + got).astype(BF)


def expert_kernel(*refs, count):
    parts = refs[:count]
    gate_ref, up_ref, down_ref = refs[count : count + 3]
    outs = refs[count + 3 : -2]
    rows, total = refs[-2:]
    step = pl.program_id(0)

    def places(pieces):
        start = 0
        for piece in pieces:
            yield slice(start, start + piece.shape[0])
            start += piece.shape[0]

    @pl.when(step == 0)
    def _():
        for part, place in zip(parts, places(parts)):
            rows[place, :] = part[...]

    tile = rows.shape[0] // 2
    last = step == pl.num_programs(0) - 1

    def one_tile(k, carry):
        place = pl.ds(k * tile, tile)
        x = rows[place, :]
        hidden = (jax.nn.silu(dot(x, gate_ref[0])) * dot(x, up_ref[0])).astype(BF)
        piece = dot(hidden, down_ref[0])

        @pl.when(step == 0)
        def _():
            total[place, :] = piece

        @pl.when(last)
        def _():
            rows[place, :] = (total[place, :] + piece).astype(BF)

        return carry

    lax.fori_loop(0, 2, one_tile, 0)

    @pl.when(last)
    def _():
        for out, place in zip(outs, places(outs)):
            out[...] = rows[place, :]


def expert(parts, gate, up, down):
    count = len(parts)
    height = sum(part.shape[0] for part in parts)
    width = parts[0].shape[1]
    chunk = gate.shape[2] // 2
    outs = [parts[0].shape, parts[1].shape, (height // 2, width)]

    def whole(shape):
        return pl.BlockSpec(shape, lambda j: (0, 0))

    return pl.pallas_call(
        lambda *refs: expert_kernel(*refs, count=count),
        grid=(2,),
        in_specs=[whole(part.shape) for part in parts]
        + [
            pl.BlockSpec((1, width, chunk), lambda j: (0, 0, j)),
            pl.BlockSpec((1, width, chunk), lambda j: (0, 0, j)),
            pl.BlockSpec((1, chunk, width), lambda j: (0, j, 0)),
        ],
        out_specs=[whole(out) for out in outs],
        out_shape=[jax.ShapeDtypeStruct(out, BF) for out in outs],
        scratch_shapes=[pltpu.VMEM((height, width), BF), pltpu.VMEM((height, width), F32)],
        compiler_params=pltpu.CompilerParams(
            dimension_semantics=("arbitrary",), vmem_limit_bytes=20 * 1024 * 1024
        ),
        cost_estimate=pl.CostEstimate(
            flops=6 * height * width * gate.shape[2],
            bytes_accessed=2 * (2 * height * width + 3 * width * gate.shape[2]),
            transcendentals=height * gate.shape[2],
        ),
    )(*parts, gate, up, down)


def shift(a, where):
    return lax.ppermute(a, "tp", where)


def routed_experts(low, high, both, gate, up, down):
    def run(*parts):
        return expert(parts, gate, up, down)

    below_low, above_high = shift(low, UP), shift(high, DOWN)
    other = shift(both, OTHER_CORE)
    below_high, above_low = shift(high, UP), shift(low, DOWN)
    own_low, own_high, own = run(low, high, other)
    far_low, far_high = shift(below_low, UP), shift(above_high, DOWN)

    def both_cores(a, b):
        fetched = [shift(c, OTHER_CORE) for c in (a, b)]
        out_a, out_b, others = run(a, b, *fetched)
        back = shift(others, OTHER_CORE)
        return (out_a, back, 0), (out_b, back, 1)

    first = both_cores(below_low, above_high)
    second = both_cores(below_high, above_low)
    far = both_cores(far_low, far_high)
    from_above_low = shift(add(*first[0]), DOWN)
    from_below_high = shift(add(*first[1]), UP)
    to_above_low = shift(add(*far[0]), UP)
    to_below_high = shift(add(*far[1]), DOWN)
    from_above_high = shift(add(*second[0], to_below_high), DOWN)
    from_below_low = shift(add(*second[1], to_above_low), UP)
    own_back = shift(own, OTHER_CORE)
    return (
        own_low,
        own_high,
        own_back,
        from_below_low,
        from_above_low,
        from_below_high,
        from_above_high,
    )


STATE = 136


def write_state(out_ref, total, state):
    high = total.astype(BF).astype(F32)
    row = lax.broadcasted_iota(jnp.int32, (8, state.shape[1]), 0)
    line = jnp.where(row == 0, high, jnp.where(row == 1, total - high, 0.0))
    message = jnp.concatenate([state, line], axis=0).astype(BF)
    for k in range(out_ref.shape[0]):
        out_ref[k] = message


def read_states(ref):
    size = ref.shape[2]
    states = [ref[k, :size, :].astype(F32) for k in range(ref.shape[0])]
    lines = [ref[k, size:, :].astype(F32) for k in range(ref.shape[0])]
    return [line[0:1, :] + line[1:2, :] for line in lines], states


def weighted(totals, states, end):
    result = jnp.zeros_like(states[0])
    between = jnp.zeros_like(totals[0])
    for k in reversed(range(len(states))):
        result = result + jnp.where(k < end, jnp.exp(between), 0.0) * states[k]
        between = between + jnp.where(k < end, totals[k], 0.0)
    return result, between


def block_state_kernel(
    key_ref, value_ref, decay_ref, cos_ref, sin_ref, rotated_ref, row_ref, column_ref, out_ref
):
    decay = decay_ref[...]
    blocks, width = decay.shape
    high = decay.astype(BF).astype(F32)
    middle = (decay - high).astype(BF).astype(F32)
    words = jnp.concatenate([high, middle, decay - high - middle], axis=0).astype(BF)
    upper = onehot(
        lax.broadcasted_iota(jnp.int32, (width, width), 0)
        <= lax.broadcasted_iota(jnp.int32, (width, width), 1)
    )
    sums = dot(words, upper)
    sums = sums[:blocks] + sums[blocks : 2 * blocks] + sums[2 * blocks :]
    total = jnp.zeros((1, 1), F32)
    rows = []
    for k in range(row_ref.shape[1] // width):
        rows.append(sums[k : k + 1, :] + total)
        total = rows[-1][:, width - 1 :]
    row_ref[...] = jnp.concatenate(rows, axis=1)
    column = jnp.concatenate([jnp.broadcast_to(r, (width, width)).T for r in rows], axis=0)
    column_ref[...] = column
    keys = key_ref[...].astype(F32)
    rotated = (keys * cos_ref[...] + pltpu.roll(keys, width // 2, 1) * sin_ref[...]).astype(BF)
    rotated_ref[...] = rotated
    damped = (rotated.astype(F32) * jnp.exp(total - column)).astype(BF)
    state = lax.dot_general(
        damped, value_ref[...], (((0,), (0,)), ((), ())), preferred_element_type=F32
    )
    write_state(out_ref, total, state)


def chip_row_kernel(in_ref, index_ref, inside_ref, ahead_ref, out_ref):
    totals, states = read_states(in_ref)
    inside, ahead = weighted(totals, states, index_ref[...])
    inside_ref[...] = inside
    ahead_ref[...] = ahead
    state, total = weighted(totals, states, len(states))
    write_state(out_ref, total, state)


def within_kernel(query_ref, rotated_ref, value_ref, row_ref, column_ref, cos_ref, sin_ref, turned_ref, out_ref):
    width = query_ref.shape[1]
    queries = query_ref[...].astype(F32)
    turned = queries * cos_ref[...] + pltpu.roll(queries, width // 2, 1) * sin_ref[...]
    turned_ref[...] = (turned * width**-0.5).astype(BF)
    step = 256

    def some_rows(k, carry):
        place = pl.ds(k * step, step)
        scores = lax.dot_general(
            turned_ref[place, :],
            rotated_ref[...],
            (((1,), (1,)), ((), ())),
            preferred_element_type=F32,
        )
        i = lax.broadcasted_iota(jnp.int32, scores.shape, 0) + k * step
        causal = i >= lax.broadcasted_iota(jnp.int32, scores.shape, 1)
        spread = column_ref[place, 0:1] - row_ref[...]
        decays = jnp.where(causal, jnp.exp(jnp.where(causal, spread, 0.0)), 0.0)
        out_ref[place, :] = dot((scores * decays).astype(BF), value_ref[...])
        return carry

    lax.fori_loop(0, query_ref.shape[0] // step, some_rows, 0)


def mix_kernel(
    in_ref, index_ref, inside_ref, ahead_ref, turned_ref, within_ref, column_ref, gate_ref, gain_ref, out_ref
):
    totals, states = read_states(in_ref)
    before, _ = weighted(totals, states, index_ref[...])
    carried = jnp.exp(ahead_ref[...]) * before + inside_ref[...]
    high = carried.astype(BF)
    low = (carried - high.astype(F32)).astype(BF)
    turned = turned_ref[...]
    readout = dot(turned, high) + dot(turned, low)
    out = within_ref[...] + jnp.exp(column_ref[...]) * readout
    scale = lax.rsqrt(jnp.mean(out * out, axis=1, keepdims=True) + epsilon)
    gate = gate_ref[...].astype(F32)
    out_ref[...] = (out * scale * gain_ref[...] * jax.nn.silu(gate)).astype(BF)


def slot_indices(route_ids, experts):
    flat_ids = route_ids.reshape(-1)
    chosen = (flat_ids[:, None] == jnp.arange(experts, dtype=jnp.int32)[None, :]).astype(jnp.int32)
    before = jnp.cumsum(chosen, axis=0) - chosen
    rank_in = jnp.sum(before * chosen, axis=1)
    return (flat_ids * SLOTS + rank_in).reshape(route_ids.shape)


def layer(
    residual,
    queries,
    key_rows,
    value_rows,
    gate_rows,
    log_decay,
    out_gain,
    out_weight,
    norm_gain,
    expert_gate,
    expert_up,
    expert_down,
    routes,
    route_weight,
):
    length, head_dim = queries.shape
    sp_count = lax.axis_size(SP)
    tp = lax.axis_index("tp")
    tp_count = lax.axis_size("tp")
    positions = (lax.axis_index(SP) * length + jnp.arange(length, dtype=jnp.int32)).astype(F32)
    column = jnp.arange(head_dim)
    half_dim = head_dim // 2
    inverse = rope_base ** (-(2 * (column % half_dim)).astype(F32) / head_dim)
    angles = positions[:, None] * inverse[None, :]
    cosine = jnp.cos(angles)
    sine = jnp.sin(angles) * jnp.where(column < half_dim, -1.0, 1.0)[None, :]
    shape = jax.ShapeDtypeStruct
    decay_rows = jnp.pad(log_decay.reshape(-1, head_dim), ((0, 2), (0, 0)))
    rotated_keys, decay_row, decay_column, message = vmem_call(
        block_state_kernel,
        [
            shape((length, head_dim), BF),
            shape((1, length), F32),
            shape((length, head_dim), F32),
            shape((lax.axis_size("sp_1"), STATE, head_dim), BF),
        ],
    )(key_rows, value_rows, decay_rows, cosine, sine)
    pieces = lax.all_to_all(message, "sp_1", 0, 0, tiled=True)
    rotated_queries, within = vmem_call(
        within_kernel,
        [shape((length, head_dim), BF), shape((length, head_dim), F32)],
        cost_estimate=pl.CostEstimate(
            flops=3 * length * length * head_dim,
            bytes_accessed=12 * length * head_dim,
            transcendentals=length * length,
        ),
    )(queries, rotated_keys, value_rows, decay_row, decay_column, cosine, sine)

    def index_line(axis):
        return jnp.full((1, head_dim), lax.axis_index(axis), jnp.int32)

    inside, ahead, message = vmem_call(
        chip_row_kernel,
        [
            shape((head_dim, head_dim), F32),
            shape((1, head_dim), F32),
            shape((lax.axis_size("sp_0"), STATE, head_dim), BF),
        ],
    )(pieces, index_line("sp_1"))
    pieces = lax.all_to_all(message, "sp_0", 0, 0, tiled=True)
    mixed = vmem_call(mix_kernel, shape((length, head_dim), BF))(
        pieces,
        index_line("sp_0"),
        inside,
        ahead,
        rotated_queries,
        within,
        decay_column,
        gate_rows,
        out_gain[None],
    )

    weights = [
        out_weight, shift(out_weight, DOWN), shift(out_weight, ACROSS), shift(out_weight, UP)
    ]
    weights = weights + [shift(w, OTHER_CORE) for w in weights]

    row_count, model_width = residual.shape
    heads = lax.all_to_all(
        mixed.reshape(tp_count, row_count, head_dim), "tp", 0, 0, tiled=True
    )
    chip, core = tp // 2, tp % 2
    turned = lax.dynamic_slice_in_dim(jnp.concatenate([heads, heads]), 2 * chip, tp_count, 0)
    turned = turned.reshape(tp_count // 2, 2, row_count, head_dim)
    mine = jnp.where(core == 0, turned[:, 0], turned[:, 1])
    others = jnp.where(core == 0, turned[:, 1], turned[:, 0])

    slots = slot_indices(routes, sp_count)
    size = sp_count * SLOTS
    packed = shape((size, USED * BLOCK), BF)
    message = (sp_count, SLOTS, USED * BLOCK)
    turning = [pltpu.VMEM(packed.shape, BF)]
    hidden_res, tokens = vmem_call(
        project_and_pack_kernel,
        [shape((row_count, model_width), BF), packed],
        scratch_shapes=turning,
    )(mine, others, *weights, residual, norm_gain[None], slots.T)
    landed = lax.all_to_all(tokens.reshape(message), SP, 0, 0, tiled=True)
    half = shape((sp_count * USED // 2, model_width), BF)
    rows = vmem_call(
        unpack_rows_kernel, [half, half, shape((sp_count * USED, model_width), BF)]
    )(landed.reshape(packed.shape))
    route = shape((row_count, sp_count * USED), BF)
    high_weight, low_weight = vmem_call(route_rows_kernel, [route, route])(slots, route_weight)
    parts = routed_experts(*rows, expert_gate, expert_up, expert_down)
    repacked = vmem_call(repack_rows_kernel, packed, scratch_shapes=turning)(*parts)
    returned = lax.all_to_all(repacked.reshape(message), SP, 0, 0, tiled=True)
    return vmem_call(
        combine_kernel,
        shape(residual.shape, BF),
        scratch_shapes=[pltpu.VMEM((sp_count * USED, model_width), BF)],
    )(returned.reshape(packed.shape), hidden_res, high_weight, low_weight)


def solution(mesh):
    split = Mesh(mesh.devices.reshape(8, 4, mesh.shape["tp"]), ("sp_0", "sp_1", "tp"))
    in_specs = (
        P(SP_TP, None),
        P(SP, "tp"),
        P(SP, "tp"),
        P(SP, "tp"),
        P(SP, "tp"),
        P("tp", SP),
        P("tp"),
        P("tp", None),
        P(),
        P(SP, None, "tp"),
        P(SP, None, "tp"),
        P(SP, "tp", None),
        P(SP_TP, None),
        P(SP_TP, None),
    )
    out_specs = P(SP_TP, None)
    return jax.shard_map(layer, mesh=split, in_specs=in_specs, out_specs=out_specs, check_vma=False)
```

profile of v0, /device:TPU:2, one launch (start us, length us, event | category | flops | bytes accessed | tf_op | source)
XLA Modules:
  0.0 219.5 jit_solution(6909749600260572941)
XLA Ops:
  0.8 1.4 fusion
  4.1 1.5 shard_map.136
  6.3 5.5 %all-to-all-start = ((bf16[4,136,128]{2,1,0:T(8,128)(2,1)}), bf16[4,136,128]{2,1,0:T(8,128)(2,1)S(1)}, u32[]{:S(2)}, u32[]{:S(2)}) async-start(bf16[4,136,128]{2,1,0:T(8,128)(2,1)} %get-tuple-element.33), calls=%async_computation | async-start | bytes 278528 | tf_op jit(solution)/shard_map/all_to_all | solution.py:450
  11.9 2.3 %collective-permute-start = (bf16[128,2048]{1,0:T(8,128)(2,1)S(1)}, bf16[128,2048]{1,0:T(8,128)(2,1)S(1)}, u32[]{:S(2)}, u32[]{:S(2)}) collective-permute-start(bf16[128,2048]{1,0:T(8,128)(2,1)S(1)} %copy-done.2), channel_id=1, source_target_pairs={{0,6},{1,7},{2,0},{3,1},{4,2},{5,3},{6,4},{7,5},{8,14},{9,15},{10,... | collective-permute-start | bytes 1572872 | tf_op jit(solution)/shard_map/ppermute | solution.py:254
  17.2 8.1 %all-to-all-start.1 = ((bf16[8,136,128]{2,1,0:T(8,128)(2,1)}), bf16[8,136,128]{2,1,0:T(8,128)(2,1)S(1)}, u32[]{:S(2)}, u32[]{:S(2)}) async-start(bf16[8,136,128]{2,1,0:T(8,128)(2,1)} %get-tuple-element.34), calls=%async_computation.1 | async-start | bytes 557056 | tf_op jit(solution)/shard_map/all_to_all | solution.py:472
  28.4 1.6 shard_map.138
  31.5 4.6 %collective-permute-done.refs_3_ = bf16[128,2048]{1,0:T(8,128)(2,1)S(1)} collective-permute-done((bf16[128,2048]{1,0:T(8,128)(2,1)S(1)}, bf16[128,2048]{1,0:T(8,128)(2,1)S(1)}, u32[]{:S(2)}, u32[]{:S(2)}) %collective-permute-start) | collective-permute-done | bytes 524320 | tf_op jit(solution)/shard_map/ppermute | solution.py:254
  36.6 3.3 %collective-permute-done.2.refs_5_ = bf16[128,2048]{1,0:T(8,128)(2,1)} collective-permute-done((bf16[128,2048]{1,0:T(8,128)(2,1)S(1)}, bf16[128,2048]{1,0:T(8,128)(2,1)}, u32[]{:S(2)}, u32[]{:S(2)}) %collective-permute-start.2) | collective-permute-done | bytes 524320 | tf_op jit(solution)/shard_map/ppermute | solution.py:254
  43.8 3.4 %all-to-all-start.2 = ((bf16[8,96,128]{2,1,0:T(8,128)(2,1)}), bf16[8,96,128]{2,1,0:T(8,128)(2,1)S(1)}, u32[]{:S(2)}, u32[]{:S(2)}) async-start(bf16[8,96,128]{2,1,0:T(8,128)(2,1)} %bitcast.1), calls=%async_computation.2 | async-start | bytes 393216 | tf_op jit(solution)/shard_map/all_to_all | solution.py:491
  47.6 6.3 %all-to-all-done.2 = bf16[8,96,128]{2,1,0:T(8,128)(2,1)S(1)} async-done(((bf16[8,96,128]{2,1,0:T(8,128)(2,1)}), bf16[8,96,128]{2,1,0:T(8,128)(2,1)S(1)}, u32[]{:S(2)}, u32[]{:S(2)}) %all-to-all-start.2) | async-done | bytes 196640 | tf_op jit(solution)/shard_map/all_to_all | solution.py:491
  55.1 3.4 %shard_map.140 = (bf16[96,2048]{1,0:T(8,128)(2,1)S(1)}, bf16[256,1792]{1,0:T(8,128)(2,1)S(1)}) custom-call(bf16[4,96,128]{2,1,0:T(8,128)(2,1)S(1)} %get-tuple-element.62.refs_0_, bf16[4,96,128]{2,1,0:T(8,128)(2,1)S(1)} %get-tuple-element.61.refs_1_, bf16[128,2048]{1,0:T(8,128)(2,1)S(1)} %copy-done.2, bf16[128,2048]{1,0:T(8,128)(2,1)S(1)} %collective-permute-done.refs_3_, ...), custom_call_target="tpu_custom_call" | custom-call | tf_op jit(solution)/shard_map/pallas_call | solution.py:505
  58.5 36.5 %all_to_all.25 = bf16[32,8,1792]{2,1,0:T(8,128)(2,1)S(1)} all-to-all(bf16[32,8,1792]{2,1,0:T(8,128)(2,1)S(1)} %bitcast.40), channel_id=1, replica_groups=mesh['sp_0'=8,'sp_1'=4,'tp'=8] {'sp_0','sp_1'}, dimensions={0} | all-to-all | bytes 1835008 | tf_op jit(solution)/shard_map/all_to_all | solution.py:510
  96.1 2.7 %collective-permute-start.16 = (bf16[112,2048]{1,0:T(8,128)(2,1)S(1)}, bf16[112,2048]{1,0:T(8,128)(2,1)S(1)}, u32[]{:S(2)}, u32[]{:S(2)}) collective-permute-start(bf16[112,2048]{1,0:T(8,128)(2,1)S(1)} %get-tuple-element.44.refs_1_), channel_id=1, source_target_pairs={{0,6},{1,7},{2,0},{3,1},{4,2},{5,3},{6,4},{7,5},{8,14},{9,15},{10,... | collective-permute-start | bytes 1376264 | tf_op jit(solution)/shard_map/ppermute | solution.py:254
  98.8 8.3 %collective-permute-done.14.refs_0_ = bf16[112,2048]{1,0:T(8,128)(2,1)S(1)} collective-permute-done((bf16[112,2048]{1,0:T(8,128)(2,1)S(1)}, bf16[112,2048]{1,0:T(8,128)(2,1)S(1)}, u32[]{:S(2)}, u32[]{:S(2)}) %collective-permute-start.14) | collective-permute-done | bytes 458784 | tf_op jit(solution)/shard_map/ppermute | solution.py:254
  107.1 3.2 %collective-permute-start.17 = (bf16[112,2048]{1,0:T(8,128)(2,1)S(1)}, bf16[112,2048]{1,0:T(8,128)(2,1)S(1)}, u32[]{:S(2)}, u32[]{:S(2)}) collective-permute-start(bf16[112,2048]{1,0:T(8,128)(2,1)S(1)} %collective-permute-done.16.refs_1_), channel_id=1, source_target_pairs={{0,6},{1,7},{2,0},{3,1},{4,2},{5,3},{6,4},{7,5},{8,14},{9,15},{10,... | collective-permute-start | bytes 1376264 | tf_op jit(solution)/shard_map/ppermute | solution.py:254
  110.3 3.2 %collective-permute-start.10 = (bf16[112,2048]{1,0:T(8,128)(2,1)S(1)}, bf16[112,2048]{1,0:T(8,128)(2,1)S(1)}, u32[]{:S(2)}, u32[]{:S(2)}) collective-permute-start(bf16[112,2048]{1,0:T(8,128)(2,1)S(1)} %get-tuple-element.43.refs_0_), channel_id=1, source_target_pairs={{0,6},{1,7},{2,0},{3,1},{4,2},{5,3},{6,4},{7,5},{8,14},{9,15},{10,... | collective-permute-start | bytes 1376264 | tf_op jit(solution)/shard_map/ppermute | solution.py:254
  113.5 8.1 %collective-permute-done.15.refs_0_ = bf16[112,2048]{1,0:T(8,128)(2,1)S(1)} collective-permute-done((bf16[112,2048]{1,0:T(8,128)(2,1)S(1)}, bf16[112,2048]{1,0:T(8,128)(2,1)S(1)}, u32[]{:S(2)}, u32[]{:S(2)}) %collective-permute-start.15) | collective-permute-done | bytes 458784 | tf_op jit(solution)/shard_map/ppermute | solution.py:254
  122.2 5.4 %collective-permute-done.9.refs_0_ = bf16[112,2048]{1,0:T(8,128)(2,1)S(1)} collective-permute-done((bf16[112,2048]{1,0:T(8,128)(2,1)S(1)}, bf16[112,2048]{1,0:T(8,128)(2,1)S(1)}, u32[]{:S(2)}, u32[]{:S(2)}) %collective-permute-start.9) | collective-permute-done | bytes 458784 | tf_op jit(solution)/shard_map/ppermute | solution.py:254
  128.6 4.9 %shard_map.144 = (bf16[112,2048]{1,0:T(8,128)(2,1)S(1)}, bf16[112,2048]{1,0:T(8,128)(2,1)S(1)}, bf16[224,2048]{1,0:T(8,128)(2,1)S(1)}) custom-call(bf16[112,2048]{1,0:T(8,128)(2,1)S(1)} %collective-permute-done.15.refs_0_, bf16[112,2048]{1,0:T(8,128)(2,1)S(1)} %collective-permute-done.17.refs_1_, bf16[112,2048]{1,0:T(8,128)(2,1)S(1)} %collective-permute-done.18.refs_2_, ...), custom_call_target="tpu_custom_call" | custom-call | flops 2818572288 | bytes 9961472 | tf_op jit(solution)/shard_map/pallas_call | solution.py:230
  133.7 4.9 %shard_map.147 = (bf16[112,2048]{1,0:T(8,128)(2,1)S(1)}, bf16[112,2048]{1,0:T(8,128)(2,1)S(1)}, bf16[224,2048]{1,0:T(8,128)(2,1)S(1)}) custom-call(bf16[112,2048]{1,0:T(8,128)(2,1)S(1)} %collective-permute-done.14.refs_0_, bf16[112,2048]{1,0:T(8,128)(2,1)S(1)} %collective-permute-done.16.refs_1_, bf16[112,2048]{1,0:T(8,128)(2,1)S(1)} %collective-permute-done.23.refs_2_, ...), custom_call_target="tpu_custom_call" | custom-call | flops 2818572288 | bytes 9961472 | tf_op jit(solution)/shard_map/pallas_call | solution.py:230
  139.2 4.9 %shard_map.143 = (bf16[112,2048]{1,0:T(8,128)(2,1)S(1)}, bf16[112,2048]{1,0:T(8,128)(2,1)S(1)}, bf16[224,2048]{1,0:T(8,128)(2,1)S(1)}) custom-call(bf16[112,2048]{1,0:T(8,128)(2,1)S(1)} %collective-permute-done.9.refs_0_, bf16[112,2048]{1,0:T(8,128)(2,1)S(1)} %collective-permute-done.10.refs_1_, bf16[112,2048]{1,0:T(8,128)(2,1)S(1)} %collective-permute-done.11.refs_2_, ...), custom_call_target="tpu_custom_call" | custom-call | flops 2818572288 | bytes 9961472 | tf_op jit(solution)/shard_map/pallas_call | solution.py:230
  144.5 4.9 %shard_map.142 = (bf16[112,2048]{1,0:T(8,128)(2,1)S(1)}, bf16[112,2048]{1,0:T(8,128)(2,1)S(1)}, bf16[224,2048]{1,0:T(8,128)(2,1)S(1)}) custom-call(bf16[112,2048]{1,0:T(8,128)(2,1)S(1)} %get-tuple-element.43.refs_0_, bf16[112,2048]{1,0:T(8,128)(2,1)S(1)} %get-tuple-element.44.refs_1_, bf16[224,2048]{1,0:T(8,128)(2,1)S(1)} %collective-permute-done.7.refs_2_, ...), custom_call_target="tpu_custom_call" | custom-call | flops 2818572288 | bytes 9961472 | tf_op jit(solution)/shard_map/pallas_call | solution.py:230
  150.2 2.9 %collective-permute-start.28 = (bf16[112,2048]{1,0:T(8,128)(2,1)S(1)}, bf16[112,2048]{1,0:T(8,128)(2,1)S(1)}, u32[]{:S(2)}, u32[]{:S(2)}) collective-permute-start(bf16[112,2048]{1,0:T(8,128)(2,1)S(1)} %shard_map.150), channel_id=1, source_target_pairs={{0,6},{1,7},{2,0},{3,1},{4,2},{5,3},{6,4},{7,5},{8,14},{9,15},{10,... | collective-permute-start | bytes 1376264 | tf_op jit(solution)/shard_map/ppermute | solution.py:254
  153.3 1.6 collective-permute-start.26
  155.6 8.6 %collective-permute-done.21.refs_2_ = bf16[112,2048]{1,0:T(8,128)(2,1)S(1)} collective-permute-done((bf16[112,2048]{1,0:T(8,128)(2,1)S(1)}, bf16[112,2048]{1,0:T(8,128)(2,1)S(1)}, u32[]{:S(2)}, u32[]{:S(2)}) %collective-permute-start.21) | collective-permute-done | bytes 458784 | tf_op jit(solution)/shard_map/ppermute | solution.py:254
  164.7 3.4 %collective-permute-start.29 = (bf16[112,2048]{1,0:T(8,128)(2,1)S(1)}, bf16[112,2048]{1,0:T(8,128)(2,1)S(1)}, u32[]{:S(2)}, u32[]{:S(2)}) collective-permute-start(bf16[112,2048]{1,0:T(8,128)(2,1)S(1)} %shard_map.151), channel_id=1, source_target_pairs={{0,6},{1,7},{2,0},{3,1},{4,2},{5,3},{6,4},{7,5},{8,14},{9,15},{10,... | collective-permute-start | bytes 1376264 | tf_op jit(solution)/shard_map/ppermute | solution.py:254
  168.0 5.9 %collective-permute-done.26.refs_1_ = bf16[112,2048]{1,0:T(8,128)(2,1)S(1)} collective-permute-done((bf16[112,2048]{1,0:T(8,128)(2,1)S(1)}, bf16[112,2048]{1,0:T(8,128)(2,1)S(1)}, u32[]{:S(2)}, u32[]{:S(2)}) %collective-permute-start.26) | collective-permute-done | bytes 458784 | tf_op jit(solution)/shard_map/ppermute | solution.py:254
  174.1 9.3 %collective-permute-done.22.refs_0_ = bf16[112,2048]{1,0:T(8,128)(2,1)S(1)} collective-permute-done((bf16[112,2048]{1,0:T(8,128)(2,1)S(1)}, bf16[112,2048]{1,0:T(8,128)(2,1)S(1)}, u32[]{:S(2)}, u32[]{:S(2)}) %collective-permute-start.22) | collective-permute-done | bytes 458784 | tf_op jit(solution)/shard_map/ppermute | solution.py:254
  183.3 1.7 shard_map.152
  185.1 7.9 %all-to-all-start.4 = ((bf16[32,8,1792]{2,1,0:T(8,128)(2,1)}), bf16[32,8,1792]{2,1,0:T(8,128)(2,1)S(1)}, u32[]{:S(2)}, u32[]{:S(2)}) async-start(bf16[32,8,1792]{2,1,0:T(8,128)(2,1)} %bitcast.10), calls=%async_computation.4 | async-start | bytes 1835008 | tf_op jit(solution)/shard_map/all_to_all | solution.py:519
  193.2 24.7 %all-to-all-done.4 = bf16[32,8,1792]{2,1,0:T(8,128)(2,1)S(1)} async-done(((bf16[32,8,1792]{2,1,0:T(8,128)(2,1)}), bf16[32,8,1792]{2,1,0:T(8,128)(2,1)S(1)}, u32[]{:S(2)}, u32[]{:S(2)}) %all-to-all-start.4) | async-done | bytes 917536 | tf_op jit(solution)/shard_map/all_to_all | solution.py:519
  217.9 1.6 shard_map.154
  (121 shorter events, 23.0 us)
Async XLA Ops:
  6.3 10.1 %all-to-all-start = ((bf16[4,136,128]{2,1,0:T(8,128)(2,1)}), bf16[4,136,128]{2,1,0:T(8,128)(2,1)S(1)}, u32[]{:S(2)}, u32[]{:S(2)}) async-start(bf16[4,136,128]{2,1,0:T(8,128)(2,1)} %get-tuple-element.33), calls=%async_computation | async-start | bytes 278528 | tf_op jit(solution)/shard_map/all_to_all | solution.py:450
  11.9 24.2 %collective-permute-start = (bf16[128,2048]{1,0:T(8,128)(2,1)S(1)}, bf16[128,2048]{1,0:T(8,128)(2,1)S(1)}, u32[]{:S(2)}, u32[]{:S(2)}) collective-permute-start(bf16[128,2048]{1,0:T(8,128)(2,1)S(1)} %copy-done.2), channel_id=1, source_target_pairs={{0,6},{1,7},{2,0},{3,1},{4,2},{5,3},{6,4},{7,5},{8,14},{9,15},{10,... | collective-permute-start | bytes 1572872 | tf_op jit(solution)/shard_map/ppermute | solution.py:254
  14.2 21.9 %collective-permute-start.1 = (bf16[128,2048]{1,0:T(8,128)(2,1)S(1)}, bf16[128,2048]{1,0:T(8,128)(2,1)S(1)}, u32[]{:S(2)}, u32[]{:S(2)}) collective-permute-start(bf16[128,2048]{1,0:T(8,128)(2,1)S(1)} %copy-done.2), channel_id=1, source_target_pairs={{0,4},{1,5},{2,6},{3,7},{4,0},{5,1},{6,2},{7,3},{8,12},{9,13},{10,... | collective-permute-start | bytes 1572872 | tf_op jit(solution)/shard_map/ppermute | solution.py:254
  14.8 25.0 %collective-permute-start.2 = (bf16[128,2048]{1,0:T(8,128)(2,1)S(1)}, bf16[128,2048]{1,0:T(8,128)(2,1)}, u32[]{:S(2)}, u32[]{:S(2)}) collective-permute-start(bf16[128,2048]{1,0:T(8,128)(2,1)S(1)} %copy-done.2), channel_id=1, source_target_pairs={{0,2},{1,3},{2,4},{3,5},{4,6},{5,7},{6,0},{7,1},{8,10},{9,11},{10,... | collective-permute-start | bytes 1572872 | tf_op jit(solution)/shard_map/ppermute | solution.py:254
  15.8 38.3 %collective-permute-start.3 = (bf16[128,2048]{1,0:T(8,128)(2,1)S(1)}, bf16[128,2048]{1,0:T(8,128)(2,1)}, u32[]{:S(2)}, u32[]{:S(2)}) collective-permute-start(bf16[128,2048]{1,0:T(8,128)(2,1)S(1)} %copy-done.2), channel_id=1, source_target_pairs={{0,1},{1,0},{2,3},{3,2},{4,5},{5,4},{6,7},{7,6},{8,9},{9,8},{10,11... | collective-permute-start | bytes 1572872 | tf_op jit(solution)/shard_map/ppermute | solution.py:254
  17.2 22.7 %all-to-all-start.1 = ((bf16[8,136,128]{2,1,0:T(8,128)(2,1)}), bf16[8,136,128]{2,1,0:T(8,128)(2,1)S(1)}, u32[]{:S(2)}, u32[]{:S(2)}) async-start(bf16[8,136,128]{2,1,0:T(8,128)(2,1)} %get-tuple-element.34), calls=%async_computation.1 | async-start | bytes 557056 | tf_op jit(solution)/shard_map/all_to_all | solution.py:472
  36.0 18.0 %collective-permute-start.4 = (bf16[128,2048]{1,0:T(8,128)(2,1)S(1)}, bf16[128,2048]{1,0:T(8,128)(2,1)S(1)}, u32[]{:S(2)}, u32[]{:S(2)}) collective-permute-start(bf16[128,2048]{1,0:T(8,128)(2,1)S(1)} %collective-permute-done.refs_3_), channel_id=1, source_target_pairs={{0,1},{1,0},{2,3},{3,2},{4,5},{5,4},{6,7},{7,6},{8,9},{9,8},{10,11... | collective-permute-start | bytes 1572872 | tf_op jit(solution)/shard_map/ppermute | solution.py:254
  36.0 18.0 %collective-permute-start.5 = (bf16[128,2048]{1,0:T(8,128)(2,1)S(1)}, bf16[128,2048]{1,0:T(8,128)(2,1)}, u32[]{:S(2)}, u32[]{:S(2)}) collective-permute-start(bf16[128,2048]{1,0:T(8,128)(2,1)S(1)} %collective-permute-done.1.refs_4_), channel_id=1, source_target_pairs={{0,1},{1,0},{2,3},{3,2},{4,5},{5,4},{6,7},{7,6},{8,9},{9,8},{10,11... | collective-permute-start | bytes 1572872 | tf_op jit(solution)/shard_map/ppermute | solution.py:254
  39.9 14.3 %collective-permute-start.6 = (bf16[128,2048]{1,0:T(8,128)(2,1)}, bf16[128,2048]{1,0:T(8,128)(2,1)}, u32[]{:S(2)}, u32[]{:S(2)}) collective-permute-start(bf16[128,2048]{1,0:T(8,128)(2,1)} %collective-permute-done.2.refs_5_), channel_id=1, source_target_pairs={{0,1},{1,0},{2,3},{3,2},{4,5},{5,4},{6,7},{7,6},{8,9},{9,8},{10,11... | collective-permute-start | bytes 1572872 | tf_op jit(solution)/shard_map/ppermute | solution.py:254
  43.8 10.1 %all-to-all-start.2 = ((bf16[8,96,128]{2,1,0:T(8,128)(2,1)}), bf16[8,96,128]{2,1,0:T(8,128)(2,1)S(1)}, u32[]{:S(2)}, u32[]{:S(2)}) async-start(bf16[8,96,128]{2,1,0:T(8,128)(2,1)} %bitcast.1), calls=%async_computation.2 | async-start | bytes 393216 | tf_op jit(solution)/shard_map/all_to_all | solution.py:491
  95.4 11.6 %collective-permute-start.14 = (bf16[112,2048]{1,0:T(8,128)(2,1)S(1)}, bf16[112,2048]{1,0:T(8,128)(2,1)S(1)}, u32[]{:S(2)}, u32[]{:S(2)}) collective-permute-start(bf16[112,2048]{1,0:T(8,128)(2,1)S(1)} %get-tuple-element.43.refs_0_), channel_id=1, source_target_pairs={{0,2},{1,3},{2,4},{3,5},{4,6},{5,7},{6,0},{7,1},{8,10},{9,11},{10,... | collective-permute-start | bytes 1376264 | tf_op jit(solution)/shard_map/ppermute | solution.py:254
  96.1 11.0 %collective-permute-start.16 = (bf16[112,2048]{1,0:T(8,128)(2,1)S(1)}, bf16[112,2048]{1,0:T(8,128)(2,1)S(1)}, u32[]{:S(2)}, u32[]{:S(2)}) collective-permute-start(bf16[112,2048]{1,0:T(8,128)(2,1)S(1)} %get-tuple-element.44.refs_1_), channel_id=1, source_target_pairs={{0,6},{1,7},{2,0},{3,1},{4,2},{5,3},{6,4},{7,5},{8,14},{9,15},{10,... | collective-permute-start | bytes 1376264 | tf_op jit(solution)/shard_map/ppermute | solution.py:254
  107.1 14.6 %collective-permute-start.15 = (bf16[112,2048]{1,0:T(8,128)(2,1)S(1)}, bf16[112,2048]{1,0:T(8,128)(2,1)S(1)}, u32[]{:S(2)}, u32[]{:S(2)}) collective-permute-start(bf16[112,2048]{1,0:T(8,128)(2,1)S(1)} %collective-permute-done.14.refs_0_), channel_id=1, source_target_pairs={{0,2},{1,3},{2,4},{3,5},{4,6},{5,7},{6,0},{7,1},{8,10},{9,11},{10,... | collective-permute-start | bytes 1376264 | tf_op jit(solution)/shard_map/ppermute | solution.py:254
  107.1 14.6 %collective-permute-start.17 = (bf16[112,2048]{1,0:T(8,128)(2,1)S(1)}, bf16[112,2048]{1,0:T(8,128)(2,1)S(1)}, u32[]{:S(2)}, u32[]{:S(2)}) collective-permute-start(bf16[112,2048]{1,0:T(8,128)(2,1)S(1)} %collective-permute-done.16.refs_1_), channel_id=1, source_target_pairs={{0,6},{1,7},{2,0},{3,1},{4,2},{5,3},{6,4},{7,5},{8,14},{9,15},{10,... | collective-permute-start | bytes 1376264 | tf_op jit(solution)/shard_map/ppermute | solution.py:254
  110.3 17.3 %collective-permute-start.9 = (bf16[112,2048]{1,0:T(8,128)(2,1)S(1)}, bf16[112,2048]{1,0:T(8,128)(2,1)S(1)}, u32[]{:S(2)}, u32[]{:S(2)}) collective-permute-start(bf16[112,2048]{1,0:T(8,128)(2,1)S(1)} %get-tuple-element.44.refs_1_), channel_id=1, source_target_pairs={{0,2},{1,3},{2,4},{3,5},{4,6},{5,7},{6,0},{7,1},{8,10},{9,11},{10,... | collective-permute-start | bytes 1376264 | tf_op jit(solution)/shard_map/ppermute | solution.py:254
  110.3 17.3 %collective-permute-start.10 = (bf16[112,2048]{1,0:T(8,128)(2,1)S(1)}, bf16[112,2048]{1,0:T(8,128)(2,1)S(1)}, u32[]{:S(2)}, u32[]{:S(2)}) collective-permute-start(bf16[112,2048]{1,0:T(8,128)(2,1)S(1)} %get-tuple-element.43.refs_0_), channel_id=1, source_target_pairs={{0,6},{1,7},{2,0},{3,1},{4,2},{5,3},{6,4},{7,5},{8,14},{9,15},{10,... | collective-permute-start | bytes 1376264 | tf_op jit(solution)/shard_map/ppermute | solution.py:254
  121.7 6.5 %collective-permute-start.19 = (bf16[112,2048]{1,0:T(8,128)(2,1)S(1)}, bf16[112,2048]{1,0:T(8,128)(2,1)S(1)}, u32[]{:S(2)}, u32[]{:S(2)}) collective-permute-start(bf16[112,2048]{1,0:T(8,128)(2,1)S(1)} %collective-permute-done.17.refs_1_), channel_id=1, source_target_pairs={{0,1},{1,0},{2,3},{3,2},{4,5},{5,4},{6,7},{7,6},{8,9},{9,8},{10,11... | collective-permute-start | bytes 1376264 | tf_op jit(solution)/shard_map/ppermute | solution.py:254
  122.2 11.4 %collective-permute-start.23 = (bf16[112,2048]{1,0:T(8,128)(2,1)S(1)}, bf16[112,2048]{1,0:T(8,128)(2,1)S(1)}, u32[]{:S(2)}, u32[]{:S(2)}) collective-permute-start(bf16[112,2048]{1,0:T(8,128)(2,1)S(1)} %collective-permute-done.14.refs_0_), channel_id=1, source_target_pairs={{0,1},{1,0},{2,3},{3,2},{4,5},{5,4},{6,7},{7,6},{8,9},{9,8},{10,11... | collective-permute-start | bytes 1376264 | tf_op jit(solution)/shard_map/ppermute | solution.py:254
  127.6 16.9 %collective-permute-start.7 = (bf16[224,2048]{1,0:T(8,128)(2,1)S(1)}, bf16[224,2048]{1,0:T(8,128)(2,1)S(1)}, u32[]{:S(2)}, u32[]{:S(2)}) collective-permute-start(bf16[224,2048]{1,0:T(8,128)(2,1)S(1)} %get-tuple-element.45), channel_id=1, source_target_pairs={{0,1},{1,0},{2,3},{3,2},{4,5},{5,4},{6,7},{7,6},{8,9},{9,8},{10,11... | collective-permute-start | bytes 2752520 | tf_op jit(solution)/shard_map/ppermute | solution.py:254
  128.1 11.1 %collective-permute-start.11 = (bf16[112,2048]{1,0:T(8,128)(2,1)S(1)}, bf16[112,2048]{1,0:T(8,128)(2,1)S(1)}, u32[]{:S(2)}, u32[]{:S(2)}) collective-permute-start(bf16[112,2048]{1,0:T(8,128)(2,1)S(1)} %collective-permute-done.9.refs_0_), channel_id=1, source_target_pairs={{0,1},{1,0},{2,3},{3,2},{4,5},{5,4},{6,7},{7,6},{8,9},{9,8},{10,11... | collective-permute-start | bytes 1376264 | tf_op jit(solution)/shard_map/ppermute | solution.py:254
  128.2 11.0 %collective-permute-start.12 = (bf16[112,2048]{1,0:T(8,128)(2,1)S(1)}, bf16[112,2048]{1,0:T(8,128)(2,1)S(1)}, u32[]{:S(2)}, u32[]{:S(2)}) collective-permute-start(bf16[112,2048]{1,0:T(8,128)(2,1)S(1)} %collective-permute-done.10.refs_1_), channel_id=1, source_target_pairs={{0,1},{1,0},{2,3},{3,2},{4,5},{5,4},{6,7},{7,6},{8,9},{9,8},{10,11... | collective-permute-start | bytes 1376264 | tf_op jit(solution)/shard_map/ppermute | solution.py:254
  133.5 15.9 %collective-permute-start.20 = (bf16[224,2048]{1,0:T(8,128)(2,1)S(1)}, bf16[224,2048]{1,0:T(8,128)(2,1)S(1)}, u32[]{:S(2)}, u32[]{:S(2)}) collective-permute-start(bf16[224,2048]{1,0:T(8,128)(2,1)S(1)} %get-tuple-element.52), channel_id=1, source_target_pairs={{0,1},{1,0},{2,3},{3,2},{4,5},{5,4},{6,7},{7,6},{8,9},{9,8},{10,11... | collective-permute-start | bytes 2752520 | tf_op jit(solution)/shard_map/ppermute | solution.py:254
  138.7 14.5 %collective-permute-start.25 = (bf16[224,2048]{1,0:T(8,128)(2,1)S(1)}, bf16[224,2048]{1,0:T(8,128)(2,1)S(1)}, u32[]{:S(2)}, u32[]{:S(2)}) collective-permute-start(bf16[224,2048]{1,0:T(8,128)(2,1)S(1)} %get-tuple-element.54), channel_id=1, source_target_pairs={{0,1},{1,0},{2,3},{3,2},{4,5},{5,4},{6,7},{7,6},{8,9},{9,8},{10,11... | collective-permute-start | bytes 2752520 | tf_op jit(solution)/shard_map/ppermute | solution.py:254
  144.1 10.9 %collective-permute-start.13 = (bf16[224,2048]{1,0:T(8,128)(2,1)S(1)}, bf16[224,2048]{1,0:T(8,128)(2,1)S(1)}, u32[]{:S(2)}, u32[]{:S(2)}) collective-permute-start(bf16[224,2048]{1,0:T(8,128)(2,1)S(1)} %get-tuple-element.50), channel_id=1, source_target_pairs={{0,1},{1,0},{2,3},{3,2},{4,5},{5,4},{6,7},{7,6},{8,9},{9,8},{10,11... | collective-permute-start | bytes 2752520 | tf_op jit(solution)/shard_map/ppermute | solution.py:254
  149.6 14.7 %collective-permute-start.21 = (bf16[112,2048]{1,0:T(8,128)(2,1)S(1)}, bf16[112,2048]{1,0:T(8,128)(2,1)S(1)}, u32[]{:S(2)}, u32[]{:S(2)}) collective-permute-start(bf16[112,2048]{1,0:T(8,128)(2,1)S(1)} %shard_map.145), channel_id=1, source_target_pairs={{0,2},{1,3},{2,4},{3,5},{4,6},{5,7},{6,0},{7,1},{8,10},{9,11},{10,... | collective-permute-start | bytes 1376264 | tf_op jit(solution)/shard_map/ppermute | solution.py:254
  149.6 18.4 %collective-permute-start.8 = (bf16[224,2048]{1,0:T(8,128)(2,1)S(1)}, bf16[224,2048]{1,0:T(8,128)(2,1)S(1)}, u32[]{:S(2)}, u32[]{:S(2)}) collective-permute-start(bf16[224,2048]{1,0:T(8,128)(2,1)S(1)} %get-tuple-element.48), channel_id=1, source_target_pairs={{0,1},{1,0},{2,3},{3,2},{4,5},{5,4},{6,7},{7,6},{8,9},{9,8},{10,11... | collective-permute-start | bytes 2752520 | tf_op jit(solution)/shard_map/ppermute | solution.py:254
  150.2 14.2 %collective-permute-start.28 = (bf16[112,2048]{1,0:T(8,128)(2,1)S(1)}, bf16[112,2048]{1,0:T(8,128)(2,1)S(1)}, u32[]{:S(2)}, u32[]{:S(2)}) collective-permute-start(bf16[112,2048]{1,0:T(8,128)(2,1)S(1)} %shard_map.150), channel_id=1, source_target_pairs={{0,6},{1,7},{2,0},{3,1},{4,2},{5,3},{6,4},{7,5},{8,14},{9,15},{10,... | collective-permute-start | bytes 1376264 | tf_op jit(solution)/shard_map/ppermute | solution.py:254
  153.3 20.6 %collective-permute-start.26 = (bf16[112,2048]{1,0:T(8,128)(2,1)S(1)}, bf16[112,2048]{1,0:T(8,128)(2,1)S(1)}, u32[]{:S(2)}, u32[]{:S(2)}) collective-permute-start(bf16[112,2048]{1,0:T(8,128)(2,1)S(1)} %shard_map.148), channel_id=1, source_target_pairs={{0,6},{1,7},{2,0},{3,1},{4,2},{5,3},{6,4},{7,5},{8,14},{9,15},{10,... | collective-permute-start | bytes 1376264 | tf_op jit(solution)/shard_map/ppermute | solution.py:254
  155.0 19.0 %collective-permute-start.27 = (bf16[112,2048]{1,0:T(8,128)(2,1)S(1)}, bf16[112,2048]{1,0:T(8,128)(2,1)S(1)}, u32[]{:S(2)}, u32[]{:S(2)}) collective-permute-start(bf16[112,2048]{1,0:T(8,128)(2,1)S(1)} %shard_map.149), channel_id=1, source_target_pairs={{0,2},{1,3},{2,4},{3,5},{4,6},{5,7},{6,0},{7,1},{8,10},{9,11},{10,... | collective-permute-start | bytes 1376264 | tf_op jit(solution)/shard_map/ppermute | solution.py:254
  164.4 18.9 %collective-permute-start.22 = (bf16[112,2048]{1,0:T(8,128)(2,1)S(1)}, bf16[112,2048]{1,0:T(8,128)(2,1)S(1)}, u32[]{:S(2)}, u32[]{:S(2)}) collective-permute-start(bf16[112,2048]{1,0:T(8,128)(2,1)S(1)} %shard_map.146), channel_id=1, source_target_pairs={{0,2},{1,3},{2,4},{3,5},{4,6},{5,7},{6,0},{7,1},{8,10},{9,11},{10,... | collective-permute-start | bytes 1376264 | tf_op jit(solution)/shard_map/ppermute | solution.py:254
  164.7 18.7 %collective-permute-start.29 = (bf16[112,2048]{1,0:T(8,128)(2,1)S(1)}, bf16[112,2048]{1,0:T(8,128)(2,1)S(1)}, u32[]{:S(2)}, u32[]{:S(2)}) collective-permute-start(bf16[112,2048]{1,0:T(8,128)(2,1)S(1)} %shard_map.151), channel_id=1, source_target_pairs={{0,6},{1,7},{2,0},{3,1},{4,2},{5,3},{6,4},{7,5},{8,14},{9,15},{10,... | collective-permute-start | bytes 1376264 | tf_op jit(solution)/shard_map/ppermute | solution.py:254
  185.1 32.9 %all-to-all-start.4 = ((bf16[32,8,1792]{2,1,0:T(8,128)(2,1)}), bf16[32,8,1792]{2,1,0:T(8,128)(2,1)S(1)}, u32[]{:S(2)}, u32[]{:S(2)}) async-start(bf16[32,8,1792]{2,1,0:T(8,128)(2,1)} %bitcast.10), calls=%async_computation.4 | async-start | bytes 1835008 | tf_op jit(solution)/shard_map/all_to_all | solution.py:519
  (22 other events, 384.9 us)
where the time goes:
time: 221 us; the launch traced here: 220 us
  waiting for transfers between devices  85.2 us (39%)
  starting transfers between devices  50.9 us (23%)
  blocking collectives  36.5 us (17%)
  Pallas kernels  32.6 us (15%)
  local copies, waits for them, and re-layouts  9.58 us (4%)
  other arithmetic  4.38 us (2%)
    ppermute x30, waiting for transfers between devices, shift(): return lax.ppermute(a, 'tp', where)  53.7 us
    all_to_all x1, blocking collectives, layer(): landed = lax.all_to_all(tokens.reshape(message), SP, 0, 0, tiled=True)  36.5 us
    ppermute x30, starting transfers between devices, shift(): return lax.ppermute(a, 'tp', where)  26 us
    all_to_all x1, waiting for transfers between devices, layer(): returned = lax.all_to_all(repacked.reshape(message), SP, 0, 0, tiled=True)  24.7 us
    pallas_call x4, Pallas kernels, expert(): pl.pallas_call(lambda *refs: expert_kernel(*refs, count=count), grid=(2,)...  19.7 us
    unnamed x42, local copies, waits for them, and re-layouts  8.95 us
    all_to_all x1, starting transfers between devices, layer(): pieces = lax.all_to_all(message, 'sp_0', 0, 0, tiled=True)  8.08 us
    all_to_all x1, starting transfers between devices, layer(): returned = lax.all_to_all(repacked.reshape(message), SP, 0, 0, tiled=True)  7.89 us
  transfers between devices with their start and end apart: 34, of which 12 were waited for; matrix products, arithmetic and copies ran while one was open for 1% of the time, Pallas kernels for 11%

commit v1 on v0

--- a/solution.py
+++ b/solution.py
@@ -31,13 +31,53 @@
     return jnp.dot(a, b, preferred_element_type=F32)
 
 
-def vmem_call(kernel, out_shape, limit=12 * 1024 * 1024, **kwargs):
-    return pl.pallas_call(
-        kernel,
-        out_shape=out_shape,
-        compiler_params=pltpu.CompilerParams(vmem_limit_bytes=limit),
-        **kwargs,
-    )
+def whole(shape):
+    return pl.BlockSpec(shape, lambda j: (0,) * len(shape))
+
+
+def vmem_call(kernel, out_shape, late=(), scratch_shapes=(), **kwargs):
+    def call(*args):
+        args = [
+            pltpu.with_memory_space_constraint(a, pltpu.HBM) if k in late else a
+            for k, a in enumerate(args)
+        ]
+        count = len(args)
+        outs = len(jax.tree.leaves(out_shape))
+        buffers = [pltpu.VMEM(args[k].shape, args[k].dtype) for k in late]
+        signals = [pltpu.SemaphoreType.DMA(())] * len(late)
+
+        def body(*refs):
+            ins = list(refs[:count])
+            rest = refs[count : count + outs + len(scratch_shapes)]
+            extra = refs[count + outs + len(scratch_shapes) :]
+            copies = []
+            for n, k in enumerate(late):
+                copies.append(pltpu.make_async_copy(ins[k], extra[n], extra[len(late) + n]))
+                copies[-1].start()
+                ins[k] = extra[n]
+
+            def ready():
+                for copy in copies:
+                    copy.wait()
+
+            if late:
+                kernel(*ins, *rest, ready=ready)
+            else:
+                kernel(*ins, *rest)
+
+        return pl.pallas_call(
+            body,
+            in_specs=[
+                pl.BlockSpec(memory_space=pltpu.HBM if k in late else pltpu.VMEM)
+                for k in range(count)
+            ],
+            out_shape=out_shape,
+            scratch_shapes=[*scratch_shapes, *buffers, *signals],
+            compiler_params=pltpu.CompilerParams(vmem_limit_bytes=12 * 1024 * 1024),
+            **kwargs,
+        )(*args)
+
+    return call
 
 
 def onehot(mask):
@@ -63,7 +103,7 @@
     return (row & (peers - 1)) * SLOTS + row // peers
 
 
-def project_and_pack_kernel(*refs):
+def project_and_pack_kernel(*refs, ready):
     mine_ref, others_ref = refs[:2]
     weights = refs[2:10]
     residual_ref, gain_ref, slot_ref, hidden_ref, out_ref, turned = refs[10:]
@@ -76,6 +116,8 @@
     for start in range(0, width, step):
         columns = slice(start, start + step)
         projected = dot(heads, jnp.concatenate([w[:, columns] for w in weights], axis=0))
+        if start == 0:
+            ready()
         hidden = (residual_ref[:, columns].astype(F32) + projected).astype(BF)
         hidden_ref[:, columns] = hidden
         hidden_f = hidden.astype(F32)
@@ -115,11 +157,26 @@
                 ref[place, i * BLOCK : (i + 1) * BLOCK] = rows[start : start + UNIT, :]
 
 
+def by_unit(rows, body):
+    def step(k, carry):
+        body(pl.multiple_of(k * UNIT, UNIT))
+        return carry
+
+    lax.fori_loop(0, rows // UNIT, step, 0)
+
+
+def copy_rows(out_ref, out_start, in_ref, in_start, rows):
+    def body(start):
+        out_ref[pl.ds(out_start + start, UNIT), :] = in_ref[pl.ds(in_start + start, UNIT), :]
+
+    by_unit(rows, body)
+
+
 def unpack_rows_kernel(in_ref, low_ref, high_ref, both_ref):
     unpack(in_ref, low_ref, high_ref)
     half = low_ref.shape[0]
-    both_ref[:half, :] = low_ref[...]
-    both_ref[half:, :] = high_ref[...]
+    copy_rows(both_ref, 0, low_ref, 0, half)
+    copy_rows(both_ref, half, high_ref, 0, half)
 
 
 def repack_rows_kernel(low_ref, high_ref, core_ref, *refs):
@@ -138,17 +195,22 @@
     out_ref[...] = dot(by_peer(size), turned[...]).astype(BF)
 
 
-def add_kernel(own_ref, core_ref, *refs, start):
+def add_kernel(own_ref, core_ref, *refs, first):
     *more, out_ref = refs
-    total = own_ref[...].astype(F32) + core_ref[start : start + own_ref.shape[0], :].astype(F32)
-    for ref in more:
-        total = total + ref[...].astype(F32)
-    out_ref[...] = total.astype(BF)
+
+    def body(start):
+        place = pl.ds(start, UNIT)
+        total = own_ref[place, :].astype(F32) + core_ref[pl.ds(first + start, UNIT), :].astype(F32)
+        for ref in more:
+            total = total + ref[place, :].astype(F32)
+        out_ref[place, :] = total.astype(BF)
+
+    by_unit(own_ref.shape[0], body)
 
 
 def add(own, core, second, *more):
     return vmem_call(
-        lambda *refs: add_kernel(*refs, start=own.shape[0] * second),
+        lambda *refs: add_kernel(*refs, first=own.shape[0] * second),
         jax.ShapeDtypeStruct(own.shape, BF),
     )(own, core, *more)
 
@@ -179,16 +241,16 @@
     rows, total = refs[-2:]
     step = pl.program_id(0)
 
-    def places(pieces):
+    def starts(pieces):
         start = 0
         for piece in pieces:
-            yield slice(start, start + piece.shape[0])
+            yield start
             start += piece.shape[0]
 
     @pl.when(step == 0)
     def _():
-        for part, place in zip(parts, places(parts)):
-            rows[place, :] = part[...]
+        for part, start in zip(parts, starts(parts)):
+            copy_rows(rows, start, part, 0, part.shape[0])
 
     tile = rows.shape[0] // 2
     last = step == pl.num_programs(0) - 1
@@ -213,8 +275,8 @@
 
     @pl.when(last)
     def _():
-        for out, place in zip(outs, places(outs)):
-            out[...] = rows[place, :]
+        for out, start in zip(outs, starts(outs)):
+            copy_rows(out, 0, rows, start, out.shape[0])
 
 
 def expert(parts, gate, up, down):
@@ -223,9 +285,6 @@
     width = parts[0].shape[1]
     chunk = gate.shape[2] // 2
     outs = [parts[0].shape, parts[1].shape, (height // 2, width)]
-
-    def whole(shape):
-        return pl.BlockSpec(shape, lambda j: (0, 0))
 
     return pl.pallas_call(
         lambda *refs: expert_kernel(*refs, count=count),
@@ -319,11 +378,23 @@
     return result, between
 
 
+def rotate(ref, cos_ref, sin_ref):
+    rows = ref[...].astype(F32)
+    return rows * cos_ref[...] + pltpu.roll(rows, ref.shape[1] // 2, 1) * sin_ref[...]
+
+
 def block_state_kernel(
-    key_ref, value_ref, decay_ref, cos_ref, sin_ref, rotated_ref, row_ref, column_ref, out_ref
+    key_ref, value_ref, decay_ref, cos_ref, sin_ref, row_ref, column_ref, out_ref, ready
 ):
-    decay = decay_ref[...]
-    blocks, width = decay.shape
+    ready()
+    width = key_ref.shape[1]
+    blocks = decay_ref.shape[1] // width
+    decay = jnp.concatenate(
+        [decay_ref[:, k * width : (k + 1) * width] for k in range(blocks)]
+        + [jnp.zeros((-blocks % 8, width), F32)],
+        axis=0,
+    )
+    blocks = decay.shape[0]
     high = decay.astype(BF).astype(F32)
     middle = (decay - high).astype(BF).astype(F32)
     words = jnp.concatenate([high, middle, decay - high - middle], axis=0).astype(BF)
@@ -341,9 +412,7 @@
     row_ref[...] = jnp.concatenate(rows, axis=1)
     column = jnp.concatenate([jnp.broadcast_to(r, (width, width)).T for r in rows], axis=0)
     column_ref[...] = column
-    keys = key_ref[...].astype(F32)
-    rotated = (keys * cos_ref[...] + pltpu.roll(keys, width // 2, 1) * sin_ref[...]).astype(BF)
-    rotated_ref[...] = rotated
+    rotated = rotate(key_ref, cos_ref, sin_ref).astype(BF)
     damped = (rotated.astype(F32) * jnp.exp(total - column)).astype(BF)
     state = lax.dot_general(
         damped, value_ref[...], (((0,), (0,)), ((), ())), preferred_element_type=F32
@@ -360,18 +429,19 @@
     write_state(out_ref, total, state)
 
 
-def within_kernel(query_ref, rotated_ref, value_ref, row_ref, column_ref, cos_ref, sin_ref, turned_ref, out_ref):
+def within_kernel(
+    query_ref, key_ref, value_ref, row_ref, column_ref, cos_ref, sin_ref, turned_ref, out_ref, rotated
+):
     width = query_ref.shape[1]
-    queries = query_ref[...].astype(F32)
-    turned = queries * cos_ref[...] + pltpu.roll(queries, width // 2, 1) * sin_ref[...]
-    turned_ref[...] = (turned * width**-0.5).astype(BF)
+    turned_ref[...] = (rotate(query_ref, cos_ref, sin_ref) * width**-0.5).astype(BF)
+    rotated[...] = rotate(key_ref, cos_ref, sin_ref).astype(BF)
     step = 256
 
     def some_rows(k, carry):
         place = pl.ds(k * step, step)
         scores = lax.dot_general(
             turned_ref[place, :],
-            rotated_ref[...],
+            rotated[...],
             (((1,), (1,)), ((), ())),
             preferred_element_type=F32,
         )
@@ -386,13 +456,14 @@
 
 
 def mix_kernel(
-    in_ref, index_ref, inside_ref, ahead_ref, turned_ref, within_ref, column_ref, gate_ref, gain_ref, out_ref
+    in_ref, index_ref, inside_ref, ahead_ref, turned_ref, within_ref, column_ref, gate_ref, gain_ref, out_ref, ready
 ):
     totals, states = read_states(in_ref)
     before, _ = weighted(totals, states, index_ref[...])
     carried = jnp.exp(ahead_ref[...]) * before + inside_ref[...]
     high = carried.astype(BF)
     low = (carried - high.astype(F32)).astype(BF)
+    ready()
     turned = turned_ref[...]
     readout = dot(turned, high) + dot(turned, low)
     out = within_ref[...] + jnp.exp(column_ref[...]) * readout
@@ -437,26 +508,26 @@
     cosine = jnp.cos(angles)
     sine = jnp.sin(angles) * jnp.where(column < half_dim, -1.0, 1.0)[None, :]
     shape = jax.ShapeDtypeStruct
-    decay_rows = jnp.pad(log_decay.reshape(-1, head_dim), ((0, 2), (0, 0)))
-    rotated_keys, decay_row, decay_column, message = vmem_call(
+    decay_row, decay_column, message = vmem_call(
         block_state_kernel,
         [
-            shape((length, head_dim), BF),
             shape((1, length), F32),
             shape((length, head_dim), F32),
             shape((lax.axis_size("sp_1"), STATE, head_dim), BF),
         ],
-    )(key_rows, value_rows, decay_rows, cosine, sine)
+        late=(0, 1, 2),
+    )(key_rows, value_rows, log_decay, cosine, sine)
     pieces = lax.all_to_all(message, "sp_1", 0, 0, tiled=True)
     rotated_queries, within = vmem_call(
         within_kernel,
         [shape((length, head_dim), BF), shape((length, head_dim), F32)],
+        scratch_shapes=[pltpu.VMEM((length, head_dim), BF)],
         cost_estimate=pl.CostEstimate(
             flops=3 * length * length * head_dim,
             bytes_accessed=12 * length * head_dim,
             transcendentals=length * length,
         ),
-    )(queries, rotated_keys, value_rows, decay_row, decay_column, cosine, sine)
+    )(queries, key_rows, value_rows, decay_row, decay_column, cosine, sine)
 
     def index_line(axis):
         return jnp.full((1, head_dim), lax.axis_index(axis), jnp.int32)
@@ -470,7 +541,7 @@
         ],
     )(pieces, index_line("sp_1"))
     pieces = lax.all_to_all(message, "sp_0", 0, 0, tiled=True)
-    mixed = vmem_call(mix_kernel, shape((length, head_dim), BF))(
+    mixed = vmem_call(mix_kernel, shape((length, head_dim), BF), late=(4, 5, 7))(
         pieces,
         index_line("sp_0"),
         inside,
@@ -505,6 +576,7 @@
     hidden_res, tokens = vmem_call(
         project_and_pack_kernel,
         [shape((row_count, model_width), BF), packed],
+        late=(10,),
         scratch_shapes=turning,
     )(mine, others, *weights, residual, norm_gain[None], slots.T)
     landed = lax.all_to_all(tokens.reshape(message), SP, 0, 0, tiled=True)

time: 221 us -> 218 us (0.986)
  local copies, waits for them, and re-layouts: 9.58 us -> 3.94 us
  Pallas kernels: 32.6 us -> 36.1 us
    unnamed x42 -> x30, local copies, waits for them, and re-layouts: 8.95 us -> 3.31 us
    pallas_call x15, Pallas kernels: 12.9 us -> 15.8 us  [call(): pl.pallas_call(body, in_specs=[pl.BlockSpec(memory_space=pltpu.HBM if k i...]
  transfers between devices with their start and end apart: 34 -> 34, of which waited for: 12 -> 12; matrix products, arithmetic and copies ran while one was open for 1% -> 1% of each run, Pallas kernels for 11% -> 12%
where the time goes in v1:
time: 218 us; the launch traced here: 216 us
  waiting for transfers between devices  84.9 us (39%)
  starting transfers between devices  50.9 us (23%)
  blocking collectives  36.5 us (17%)
  Pallas kernels  36.1 us (17%)
  local copies, waits for them, and re-layouts  3.94 us (2%)
  other arithmetic  3.62 us (2%)
    ppermute x30, waiting for transfers between devices, shift(): return lax.ppermute(a, 'tp', where)  53.4 us
    all_to_all x1, blocking collectives, layer(): landed = lax.all_to_all(tokens.reshape(message), SP, 0, 0, tiled=True)  36.5 us
    ppermute x30, starting transfers between devices, shift(): return lax.ppermute(a, 'tp', where)  26 us
    all_to_all x1, waiting for transfers between devices, layer(): returned = lax.all_to_all(repacked.reshape(message), SP, 0, 0, tiled=True)  24.7 us
    pallas_call x4, Pallas kernels, expert(): pl.pallas_call(lambda *refs: expert_kernel(*refs, count=count), grid=(2,)...  20.4 us
    pallas_call x15, Pallas kernels, call(): pl.pallas_call(body, in_specs=[pl.BlockSpec(memory_space=pltpu.HBM if k i...  15.8 us
    all_to_all x1, starting transfers between devices, layer(): pieces = lax.all_to_all(message, 'sp_0', 0, 0, tiled=True)  8.09 us
    all_to_all x1, starting transfers between devices, layer(): returned = lax.all_to_all(repacked.reshape(message), SP, 0, 0, tiled=True)  7.87 us
  transfers between devices with their start and end apart: 34, of which 12 were waited for; matrix products, arithmetic and copies ran while one was open for 1% of the time, Pallas kernels for 12%

profile of v1, /device:TPU:2, one launch (start us, length us, event | category | flops | bytes accessed | tf_op | source)
XLA Modules:
  0.0 216.4 jit_solution(14306018219671807425)
XLA Ops:
  1.5 2.6 %shard_map.136 = (f32[1,768]{1,0:T(1,128)S(1)}, f32[768,128]{1,0:T(8,128)S(1)}, bf16[4,136,128]{2,1,0:T(8,128)(2,1)}) custom-call(bf16[768,128]{1,0:T(8,128)(2,1)} %refs_1_.4, bf16[768,128]{1,0:T(8,128)(2,1)} %refs_2_.4, f32[1,768]{1,0:T(1,128)} %refs_2_.3, f32[768,128]{1,0:T(8,128)S(1)} %get-tuple-element.62.refs_3_.refs_5_, ...), custom_call_target="tpu_custom_call" | custom-call | tf_op jit(solution)/shard_map/pallas_call | solution.py:68
  4.1 5.5 %all-to-all-start = ((bf16[4,136,128]{2,1,0:T(8,128)(2,1)}), bf16[4,136,128]{2,1,0:T(8,128)(2,1)S(1)}, u32[]{:S(2)}, u32[]{:S(2)}) async-start(bf16[4,136,128]{2,1,0:T(8,128)(2,1)} %get-tuple-element.32), calls=%async_computation | async-start | bytes 278528 | tf_op jit(solution)/shard_map/all_to_all | solution.py:520
  9.6 2.3 %collective-permute-start = (bf16[128,2048]{1,0:T(8,128)(2,1)S(1)}, bf16[128,2048]{1,0:T(8,128)(2,1)S(1)}, u32[]{:S(2)}, u32[]{:S(2)}) collective-permute-start(bf16[128,2048]{1,0:T(8,128)(2,1)S(1)} %copy-done.2), channel_id=1, source_target_pairs={{0,6},{1,7},{2,0},{3,1},{4,2},{5,3},{6,4},{7,5},{8,14},{9,15},{10,... | collective-permute-start | bytes 1572872 | tf_op jit(solution)/shard_map/ppermute | solution.py:313
  15.0 8.1 %all-to-all-start.1 = ((bf16[8,136,128]{2,1,0:T(8,128)(2,1)}), bf16[8,136,128]{2,1,0:T(8,128)(2,1)S(1)}, u32[]{:S(2)}, u32[]{:S(2)}) async-start(bf16[8,136,128]{2,1,0:T(8,128)(2,1)} %copy-done.4), calls=%async_computation.1 | async-start | bytes 557056 | tf_op jit(solution)/shard_map/all_to_all | solution.py:543
  26.2 1.7 shard_map.138
  29.4 4.5 %collective-permute-done.refs_3_ = bf16[128,2048]{1,0:T(8,128)(2,1)S(1)} collective-permute-done((bf16[128,2048]{1,0:T(8,128)(2,1)S(1)}, bf16[128,2048]{1,0:T(8,128)(2,1)S(1)}, u32[]{:S(2)}, u32[]{:S(2)}) %collective-permute-start) | collective-permute-done | bytes 524320 | tf_op jit(solution)/shard_map/ppermute | solution.py:313
  34.3 3.3 %collective-permute-done.2.refs_5_ = bf16[128,2048]{1,0:T(8,128)(2,1)} collective-permute-done((bf16[128,2048]{1,0:T(8,128)(2,1)S(1)}, bf16[128,2048]{1,0:T(8,128)(2,1)}, u32[]{:S(2)}, u32[]{:S(2)}) %collective-permute-start.2) | collective-permute-done | bytes 524320 | tf_op jit(solution)/shard_map/ppermute | solution.py:313
  37.7 2.2 %shard_map.139 = bf16[768,128]{1,0:T(8,128)(2,1)} custom-call(bf16[8,136,128]{2,1,0:T(8,128)(2,1)S(1)} %all-to-all-done.1.refs_0_, s32[1,128]{1,0:T(1,128)S(1)} %broadcast_in_dim.27.refs_1_, f32[128,128]{1,0:T(8,128)S(1)} %get-tuple-element.34.refs_2_, f32[1,128]{1,0:T(1,128)S(1)} %get-tuple-element.35.refs_3_, bf16[768,128]{1,0:T(8,128)(2,1)} %copy-done.6, ...), custom_call_target="tpu_custom_call" | custom-call | tf_op jit(solution)/shard_map/pallas_call | solution.py:68
  39.9 3.4 %all-to-all-start.2 = ((bf16[8,96,128]{2,1,0:T(8,128)(2,1)}), bf16[8,96,128]{2,1,0:T(8,128)(2,1)S(1)}, u32[]{:S(2)}, u32[]{:S(2)}) async-start(bf16[8,96,128]{2,1,0:T(8,128)(2,1)} %bitcast.1), calls=%async_computation.2 | async-start | bytes 393216 | tf_op jit(solution)/shard_map/all_to_all | solution.py:562
  43.7 6.3 %all-to-all-done.2 = bf16[8,96,128]{2,1,0:T(8,128)(2,1)S(1)} async-done(((bf16[8,96,128]{2,1,0:T(8,128)(2,1)}), bf16[8,96,128]{2,1,0:T(8,128)(2,1)S(1)}, u32[]{:S(2)}, u32[]{:S(2)}) %all-to-all-start.2) | async-done | bytes 196640 | tf_op jit(solution)/shard_map/all_to_all | solution.py:562
  50.2 4.4 %shard_map.140 = (bf16[96,2048]{1,0:T(8,128)(2,1)S(1)}, bf16[256,1792]{1,0:T(8,128)(2,1)S(1)}) custom-call(bf16[4,96,128]{2,1,0:T(8,128)(2,1)S(1)} %get-tuple-element.60.refs_0_, bf16[4,96,128]{2,1,0:T(8,128)(2,1)S(1)} %get-tuple-element.59.refs_1_, bf16[128,2048]{1,0:T(8,128)(2,1)S(1)} %copy-done.2, bf16[128,2048]{1,0:T(8,128)(2,1)S(1)} %collective-permute-done.refs_3_, ...), custom_call_target="tpu_custom_call" | custom-call | tf_op jit(solution)/shard_map/pallas_call | solution.py:68
  54.6 36.5 %all_to_all.25 = bf16[32,8,1792]{2,1,0:T(8,128)(2,1)S(1)} all-to-all(bf16[32,8,1792]{2,1,0:T(8,128)(2,1)S(1)} %bitcast.39), channel_id=1, replica_groups=mesh['sp_0'=8,'sp_1'=4,'tp'=8] {'sp_0','sp_1'}, dimensions={0} | all-to-all | bytes 1835008 | tf_op jit(solution)/shard_map/all_to_all | solution.py:582
  92.3 2.7 %collective-permute-start.16 = (bf16[112,2048]{1,0:T(8,128)(2,1)S(1)}, bf16[112,2048]{1,0:T(8,128)(2,1)S(1)}, u32[]{:S(2)}, u32[]{:S(2)}) collective-permute-start(bf16[112,2048]{1,0:T(8,128)(2,1)S(1)} %get-tuple-element.42.refs_1_), channel_id=1, source_target_pairs={{0,6},{1,7},{2,0},{3,1},{4,2},{5,3},{6,4},{7,5},{8,14},{9,15},{10,... | collective-permute-start | bytes 1376264 | tf_op jit(solution)/shard_map/ppermute | solution.py:313
  94.9 8.3 %collective-permute-done.14.refs_0_ = bf16[112,2048]{1,0:T(8,128)(2,1)S(1)} collective-permute-done((bf16[112,2048]{1,0:T(8,128)(2,1)S(1)}, bf16[112,2048]{1,0:T(8,128)(2,1)S(1)}, u32[]{:S(2)}, u32[]{:S(2)}) %collective-permute-start.14) | collective-permute-done | bytes 458784 | tf_op jit(solution)/shard_map/ppermute | solution.py:313
  103.2 3.2 %collective-permute-start.17 = (bf16[112,2048]{1,0:T(8,128)(2,1)S(1)}, bf16[112,2048]{1,0:T(8,128)(2,1)S(1)}, u32[]{:S(2)}, u32[]{:S(2)}) collective-permute-start(bf16[112,2048]{1,0:T(8,128)(2,1)S(1)} %collective-permute-done.16.refs_1_), channel_id=1, source_target_pairs={{0,6},{1,7},{2,0},{3,1},{4,2},{5,3},{6,4},{7,5},{8,14},{9,15},{10,... | collective-permute-start | bytes 1376264 | tf_op jit(solution)/shard_map/ppermute | solution.py:313
  106.5 3.2 %collective-permute-start.10 = (bf16[112,2048]{1,0:T(8,128)(2,1)S(1)}, bf16[112,2048]{1,0:T(8,128)(2,1)S(1)}, u32[]{:S(2)}, u32[]{:S(2)}) collective-permute-start(bf16[112,2048]{1,0:T(8,128)(2,1)S(1)} %get-tuple-element.41.refs_0_), channel_id=1, source_target_pairs={{0,6},{1,7},{2,0},{3,1},{4,2},{5,3},{6,4},{7,5},{8,14},{9,15},{10,... | collective-permute-start | bytes 1376264 | tf_op jit(solution)/shard_map/ppermute | solution.py:313
  109.7 8.1 %collective-permute-done.15.refs_0_ = bf16[112,2048]{1,0:T(8,128)(2,1)S(1)} collective-permute-done((bf16[112,2048]{1,0:T(8,128)(2,1)S(1)}, bf16[112,2048]{1,0:T(8,128)(2,1)S(1)}, u32[]{:S(2)}, u32[]{:S(2)}) %collective-permute-start.15) | collective-permute-done | bytes 458784 | tf_op jit(solution)/shard_map/ppermute | solution.py:313
  118.3 5.4 %collective-permute-done.9.refs_0_ = bf16[112,2048]{1,0:T(8,128)(2,1)S(1)} collective-permute-done((bf16[112,2048]{1,0:T(8,128)(2,1)S(1)}, bf16[112,2048]{1,0:T(8,128)(2,1)S(1)}, u32[]{:S(2)}, u32[]{:S(2)}) %collective-permute-start.9) | collective-permute-done | bytes 458784 | tf_op jit(solution)/shard_map/ppermute | solution.py:313
  124.8 5.1 %shard_map.144 = (bf16[112,2048]{1,0:T(8,128)(2,1)S(1)}, bf16[112,2048]{1,0:T(8,128)(2,1)S(1)}, bf16[224,2048]{1,0:T(8,128)(2,1)S(1)}) custom-call(bf16[112,2048]{1,0:T(8,128)(2,1)S(1)} %collective-permute-done.15.refs_0_, bf16[112,2048]{1,0:T(8,128)(2,1)S(1)} %collective-permute-done.17.refs_1_, bf16[112,2048]{1,0:T(8,128)(2,1)S(1)} %collective-permute-done.18.refs_2_, ...), custom_call_target="tpu_custom_call" | custom-call | flops 2818572288 | bytes 9961472 | tf_op jit(solution)/shard_map/pallas_call | solution.py:289
  130.1 5.1 %shard_map.147 = (bf16[112,2048]{1,0:T(8,128)(2,1)S(1)}, bf16[112,2048]{1,0:T(8,128)(2,1)S(1)}, bf16[224,2048]{1,0:T(8,128)(2,1)S(1)}) custom-call(bf16[112,2048]{1,0:T(8,128)(2,1)S(1)} %collective-permute-done.14.refs_0_, bf16[112,2048]{1,0:T(8,128)(2,1)S(1)} %collective-permute-done.16.refs_1_, bf16[112,2048]{1,0:T(8,128)(2,1)S(1)} %collective-permute-done.23.refs_2_, ...), custom_call_target="tpu_custom_call" | custom-call | flops 2818572288 | bytes 9961472 | tf_op jit(solution)/shard_map/pallas_call | solution.py:289
  135.7 5.1 %shard_map.143 = (bf16[112,2048]{1,0:T(8,128)(2,1)S(1)}, bf16[112,2048]{1,0:T(8,128)(2,1)S(1)}, bf16[224,2048]{1,0:T(8,128)(2,1)S(1)}) custom-call(bf16[112,2048]{1,0:T(8,128)(2,1)S(1)} %collective-permute-done.9.refs_0_, bf16[112,2048]{1,0:T(8,128)(2,1)S(1)} %collective-permute-done.10.refs_1_, bf16[112,2048]{1,0:T(8,128)(2,1)S(1)} %collective-permute-done.11.refs_2_, ...), custom_call_target="tpu_custom_call" | custom-call | flops 2818572288 | bytes 9961472 | tf_op jit(solution)/shard_map/pallas_call | solution.py:289
  141.2 5.1 %shard_map.142 = (bf16[112,2048]{1,0:T(8,128)(2,1)S(1)}, bf16[112,2048]{1,0:T(8,128)(2,1)S(1)}, bf16[224,2048]{1,0:T(8,128)(2,1)S(1)}) custom-call(bf16[112,2048]{1,0:T(8,128)(2,1)S(1)} %get-tuple-element.41.refs_0_, bf16[112,2048]{1,0:T(8,128)(2,1)S(1)} %get-tuple-element.42.refs_1_, bf16[224,2048]{1,0:T(8,128)(2,1)S(1)} %collective-permute-done.7.refs_2_, ...), custom_call_target="tpu_custom_call" | custom-call | flops 2818572288 | bytes 9961472 | tf_op jit(solution)/shard_map/pallas_call | solution.py:289
  147.2 2.9 %collective-permute-start.28 = (bf16[112,2048]{1,0:T(8,128)(2,1)S(1)}, bf16[112,2048]{1,0:T(8,128)(2,1)S(1)}, u32[]{:S(2)}, u32[]{:S(2)}) collective-permute-start(bf16[112,2048]{1,0:T(8,128)(2,1)S(1)} %shard_map.150), channel_id=1, source_target_pairs={{0,6},{1,7},{2,0},{3,1},{4,2},{5,3},{6,4},{7,5},{8,14},{9,15},{10,... | collective-permute-start | bytes 1376264 | tf_op jit(solution)/shard_map/ppermute | solution.py:313
  150.3 1.6 collective-permute-start.26
  152.6 8.5 %collective-permute-done.21.refs_2_ = bf16[112,2048]{1,0:T(8,128)(2,1)S(1)} collective-permute-done((bf16[112,2048]{1,0:T(8,128)(2,1)S(1)}, bf16[112,2048]{1,0:T(8,128)(2,1)S(1)}, u32[]{:S(2)}, u32[]{:S(2)}) %collective-permute-start.21) | collective-permute-done | bytes 458784 | tf_op jit(solution)/shard_map/ppermute | solution.py:313
  161.7 3.4 %collective-permute-start.29 = (bf16[112,2048]{1,0:T(8,128)(2,1)S(1)}, bf16[112,2048]{1,0:T(8,128)(2,1)S(1)}, u32[]{:S(2)}, u32[]{:S(2)}) collective-permute-start(bf16[112,2048]{1,0:T(8,128)(2,1)S(1)} %shard_map.151), channel_id=1, source_target_pairs={{0,6},{1,7},{2,0},{3,1},{4,2},{5,3},{6,4},{7,5},{8,14},{9,15},{10,... | collective-permute-start | bytes 1376264 | tf_op jit(solution)/shard_map/ppermute | solution.py:313
  165.0 5.9 %collective-permute-done.26.refs_4_ = bf16[112,2048]{1,0:T(8,128)(2,1)S(1)} collective-permute-done((bf16[112,2048]{1,0:T(8,128)(2,1)S(1)}, bf16[112,2048]{1,0:T(8,128)(2,1)S(1)}, u32[]{:S(2)}, u32[]{:S(2)}) %collective-permute-start.26) | collective-permute-done | bytes 458784 | tf_op jit(solution)/shard_map/ppermute | solution.py:313
  171.0 9.3 %collective-permute-done.22.refs_3_ = bf16[112,2048]{1,0:T(8,128)(2,1)S(1)} collective-permute-done((bf16[112,2048]{1,0:T(8,128)(2,1)S(1)}, bf16[112,2048]{1,0:T(8,128)(2,1)S(1)}, u32[]{:S(2)}, u32[]{:S(2)}) %collective-permute-start.22) | collective-permute-done | bytes 458784 | tf_op jit(solution)/shard_map/ppermute | solution.py:313
  180.3 1.7 shard_map.152
  182.0 7.9 %all-to-all-start.4 = ((bf16[32,8,1792]{2,1,0:T(8,128)(2,1)}), bf16[32,8,1792]{2,1,0:T(8,128)(2,1)S(1)}, u32[]{:S(2)}, u32[]{:S(2)}) async-start(bf16[32,8,1792]{2,1,0:T(8,128)(2,1)} %bitcast.10), calls=%async_computation.4 | async-start | bytes 1835008 | tf_op jit(solution)/shard_map/all_to_all | solution.py:591
  190.1 24.7 %all-to-all-done.4 = bf16[32,8,1792]{2,1,0:T(8,128)(2,1)S(1)} async-done(((bf16[32,8,1792]{2,1,0:T(8,128)(2,1)}), bf16[32,8,1792]{2,1,0:T(8,128)(2,1)S(1)}, u32[]{:S(2)}, u32[]{:S(2)}) %all-to-all-start.4) | async-done | bytes 917536 | tf_op jit(solution)/shard_map/all_to_all | solution.py:591
  214.8 1.6 shard_map.154
  (107 shorter events, 16.4 us)
Async XLA Ops:
  4.1 10.1 %all-to-all-start = ((bf16[4,136,128]{2,1,0:T(8,128)(2,1)}), bf16[4,136,128]{2,1,0:T(8,128)(2,1)S(1)}, u32[]{:S(2)}, u32[]{:S(2)}) async-start(bf16[4,136,128]{2,1,0:T(8,128)(2,1)} %get-tuple-element.32), calls=%async_computation | async-start | bytes 278528 | tf_op jit(solution)/shard_map/all_to_all | solution.py:520
  9.6 24.2 %collective-permute-start = (bf16[128,2048]{1,0:T(8,128)(2,1)S(1)}, bf16[128,2048]{1,0:T(8,128)(2,1)S(1)}, u32[]{:S(2)}, u32[]{:S(2)}) collective-permute-start(bf16[128,2048]{1,0:T(8,128)(2,1)S(1)} %copy-done.2), channel_id=1, source_target_pairs={{0,6},{1,7},{2,0},{3,1},{4,2},{5,3},{6,4},{7,5},{8,14},{9,15},{10,... | collective-permute-start | bytes 1572872 | tf_op jit(solution)/shard_map/ppermute | solution.py:313
  12.0 21.9 %collective-permute-start.1 = (bf16[128,2048]{1,0:T(8,128)(2,1)S(1)}, bf16[128,2048]{1,0:T(8,128)(2,1)S(1)}, u32[]{:S(2)}, u32[]{:S(2)}) collective-permute-start(bf16[128,2048]{1,0:T(8,128)(2,1)S(1)} %copy-done.2), channel_id=1, source_target_pairs={{0,4},{1,5},{2,6},{3,7},{4,0},{5,1},{6,2},{7,3},{8,12},{9,13},{10,... | collective-permute-start | bytes 1572872 | tf_op jit(solution)/shard_map/ppermute | solution.py:313
  12.6 25.0 %collective-permute-start.2 = (bf16[128,2048]{1,0:T(8,128)(2,1)S(1)}, bf16[128,2048]{1,0:T(8,128)(2,1)}, u32[]{:S(2)}, u32[]{:S(2)}) collective-permute-start(bf16[128,2048]{1,0:T(8,128)(2,1)S(1)} %copy-done.2), channel_id=1, source_target_pairs={{0,2},{1,3},{2,4},{3,5},{4,6},{5,7},{6,0},{7,1},{8,10},{9,11},{10,... | collective-permute-start | bytes 1572872 | tf_op jit(solution)/shard_map/ppermute | solution.py:313
  13.6 36.6 %collective-permute-start.3 = (bf16[128,2048]{1,0:T(8,128)(2,1)S(1)}, bf16[128,2048]{1,0:T(8,128)(2,1)}, u32[]{:S(2)}, u32[]{:S(2)}) collective-permute-start(bf16[128,2048]{1,0:T(8,128)(2,1)S(1)} %copy-done.2), channel_id=1, source_target_pairs={{0,1},{1,0},{2,3},{3,2},{4,5},{5,4},{6,7},{7,6},{8,9},{9,8},{10,11... | collective-permute-start | bytes 1572872 | tf_op jit(solution)/shard_map/ppermute | solution.py:313
  15.0 22.6 %all-to-all-start.1 = ((bf16[8,136,128]{2,1,0:T(8,128)(2,1)}), bf16[8,136,128]{2,1,0:T(8,128)(2,1)S(1)}, u32[]{:S(2)}, u32[]{:S(2)}) async-start(bf16[8,136,128]{2,1,0:T(8,128)(2,1)} %copy-done.4), calls=%async_computation.1 | async-start | bytes 557056 | tf_op jit(solution)/shard_map/all_to_all | solution.py:543
  33.8 16.3 %collective-permute-start.4 = (bf16[128,2048]{1,0:T(8,128)(2,1)S(1)}, bf16[128,2048]{1,0:T(8,128)(2,1)S(1)}, u32[]{:S(2)}, u32[]{:S(2)}) collective-permute-start(bf16[128,2048]{1,0:T(8,128)(2,1)S(1)} %collective-permute-done.refs_3_), channel_id=1, source_target_pairs={{0,1},{1,0},{2,3},{3,2},{4,5},{5,4},{6,7},{7,6},{8,9},{9,8},{10,11... | collective-permute-start | bytes 1572872 | tf_op jit(solution)/shard_map/ppermute | solution.py:313
  33.8 16.3 %collective-permute-start.5 = (bf16[128,2048]{1,0:T(8,128)(2,1)S(1)}, bf16[128,2048]{1,0:T(8,128)(2,1)}, u32[]{:S(2)}, u32[]{:S(2)}) collective-permute-start(bf16[128,2048]{1,0:T(8,128)(2,1)S(1)} %collective-permute-done.1.refs_4_), channel_id=1, source_target_pairs={{0,1},{1,0},{2,3},{3,2},{4,5},{5,4},{6,7},{7,6},{8,9},{9,8},{10,11... | collective-permute-start | bytes 1572872 | tf_op jit(solution)/shard_map/ppermute | solution.py:313
  37.6 12.5 %collective-permute-start.6 = (bf16[128,2048]{1,0:T(8,128)(2,1)}, bf16[128,2048]{1,0:T(8,128)(2,1)}, u32[]{:S(2)}, u32[]{:S(2)}) collective-permute-start(bf16[128,2048]{1,0:T(8,128)(2,1)} %collective-permute-done.2.refs_5_), channel_id=1, source_target_pairs={{0,1},{1,0},{2,3},{3,2},{4,5},{5,4},{6,7},{7,6},{8,9},{9,8},{10,11... | collective-permute-start | bytes 1572872 | tf_op jit(solution)/shard_map/ppermute | solution.py:313
  39.9 10.1 %all-to-all-start.2 = ((bf16[8,96,128]{2,1,0:T(8,128)(2,1)}), bf16[8,96,128]{2,1,0:T(8,128)(2,1)S(1)}, u32[]{:S(2)}, u32[]{:S(2)}) async-start(bf16[8,96,128]{2,1,0:T(8,128)(2,1)} %bitcast.1), calls=%async_computation.2 | async-start | bytes 393216 | tf_op jit(solution)/shard_map/all_to_all | solution.py:562
  91.6 11.6 %collective-permute-start.14 = (bf16[112,2048]{1,0:T(8,128)(2,1)S(1)}, bf16[112,2048]{1,0:T(8,128)(2,1)S(1)}, u32[]{:S(2)}, u32[]{:S(2)}) collective-permute-start(bf16[112,2048]{1,0:T(8,128)(2,1)S(1)} %get-tuple-element.41.refs_0_), channel_id=1, source_target_pairs={{0,2},{1,3},{2,4},{3,5},{4,6},{5,7},{6,0},{7,1},{8,10},{9,11},{10,... | collective-permute-start | bytes 1376264 | tf_op jit(solution)/shard_map/ppermute | solution.py:313
  92.3 11.0 %collective-permute-start.16 = (bf16[112,2048]{1,0:T(8,128)(2,1)S(1)}, bf16[112,2048]{1,0:T(8,128)(2,1)S(1)}, u32[]{:S(2)}, u32[]{:S(2)}) collective-permute-start(bf16[112,2048]{1,0:T(8,128)(2,1)S(1)} %get-tuple-element.42.refs_1_), channel_id=1, source_target_pairs={{0,6},{1,7},{2,0},{3,1},{4,2},{5,3},{6,4},{7,5},{8,14},{9,15},{10,... | collective-permute-start | bytes 1376264 | tf_op jit(solution)/shard_map/ppermute | solution.py:313
  103.2 14.6 %collective-permute-start.15 = (bf16[112,2048]{1,0:T(8,128)(2,1)S(1)}, bf16[112,2048]{1,0:T(8,128)(2,1)S(1)}, u32[]{:S(2)}, u32[]{:S(2)}) collective-permute-start(bf16[112,2048]{1,0:T(8,128)(2,1)S(1)} %collective-permute-done.14.refs_0_), channel_id=1, source_target_pairs={{0,2},{1,3},{2,4},{3,5},{4,6},{5,7},{6,0},{7,1},{8,10},{9,11},{10,... | collective-permute-start | bytes 1376264 | tf_op jit(solution)/shard_map/ppermute | solution.py:313
  103.2 14.6 %collective-permute-start.17 = (bf16[112,2048]{1,0:T(8,128)(2,1)S(1)}, bf16[112,2048]{1,0:T(8,128)(2,1)S(1)}, u32[]{:S(2)}, u32[]{:S(2)}) collective-permute-start(bf16[112,2048]{1,0:T(8,128)(2,1)S(1)} %collective-permute-done.16.refs_1_), channel_id=1, source_target_pairs={{0,6},{1,7},{2,0},{3,1},{4,2},{5,3},{6,4},{7,5},{8,14},{9,15},{10,... | collective-permute-start | bytes 1376264 | tf_op jit(solution)/shard_map/ppermute | solution.py:313
  106.5 17.3 %collective-permute-start.9 = (bf16[112,2048]{1,0:T(8,128)(2,1)S(1)}, bf16[112,2048]{1,0:T(8,128)(2,1)S(1)}, u32[]{:S(2)}, u32[]{:S(2)}) collective-permute-start(bf16[112,2048]{1,0:T(8,128)(2,1)S(1)} %get-tuple-element.42.refs_1_), channel_id=1, source_target_pairs={{0,2},{1,3},{2,4},{3,5},{4,6},{5,7},{6,0},{7,1},{8,10},{9,11},{10,... | collective-permute-start | bytes 1376264 | tf_op jit(solution)/shard_map/ppermute | solution.py:313
  106.5 17.3 %collective-permute-start.10 = (bf16[112,2048]{1,0:T(8,128)(2,1)S(1)}, bf16[112,2048]{1,0:T(8,128)(2,1)S(1)}, u32[]{:S(2)}, u32[]{:S(2)}) collective-permute-start(bf16[112,2048]{1,0:T(8,128)(2,1)S(1)} %get-tuple-element.41.refs_0_), channel_id=1, source_target_pairs={{0,6},{1,7},{2,0},{3,1},{4,2},{5,3},{6,4},{7,5},{8,14},{9,15},{10,... | collective-permute-start | bytes 1376264 | tf_op jit(solution)/shard_map/ppermute | solution.py:313
  117.8 6.5 %collective-permute-start.19 = (bf16[112,2048]{1,0:T(8,128)(2,1)S(1)}, bf16[112,2048]{1,0:T(8,128)(2,1)S(1)}, u32[]{:S(2)}, u32[]{:S(2)}) collective-permute-start(bf16[112,2048]{1,0:T(8,128)(2,1)S(1)} %collective-permute-done.17.refs_1_), channel_id=1, source_target_pairs={{0,1},{1,0},{2,3},{3,2},{4,5},{5,4},{6,7},{7,6},{8,9},{9,8},{10,11... | collective-permute-start | bytes 1376264 | tf_op jit(solution)/shard_map/ppermute | solution.py:313
  118.3 11.5 %collective-permute-start.23 = (bf16[112,2048]{1,0:T(8,128)(2,1)S(1)}, bf16[112,2048]{1,0:T(8,128)(2,1)S(1)}, u32[]{:S(2)}, u32[]{:S(2)}) collective-permute-start(bf16[112,2048]{1,0:T(8,128)(2,1)S(1)} %collective-permute-done.14.refs_0_), channel_id=1, source_target_pairs={{0,1},{1,0},{2,3},{3,2},{4,5},{5,4},{6,7},{7,6},{8,9},{9,8},{10,11... | collective-permute-start | bytes 1376264 | tf_op jit(solution)/shard_map/ppermute | solution.py:313
  123.7 17.4 %collective-permute-start.7 = (bf16[224,2048]{1,0:T(8,128)(2,1)S(1)}, bf16[224,2048]{1,0:T(8,128)(2,1)S(1)}, u32[]{:S(2)}, u32[]{:S(2)}) collective-permute-start(bf16[224,2048]{1,0:T(8,128)(2,1)S(1)} %get-tuple-element.43), channel_id=1, source_target_pairs={{0,1},{1,0},{2,3},{3,2},{4,5},{5,4},{6,7},{7,6},{8,9},{9,8},{10,11... | collective-permute-start | bytes 2752520 | tf_op jit(solution)/shard_map/ppermute | solution.py:313
  124.3 11.4 %collective-permute-start.11 = (bf16[112,2048]{1,0:T(8,128)(2,1)S(1)}, bf16[112,2048]{1,0:T(8,128)(2,1)S(1)}, u32[]{:S(2)}, u32[]{:S(2)}) collective-permute-start(bf16[112,2048]{1,0:T(8,128)(2,1)S(1)} %collective-permute-done.9.refs_0_), channel_id=1, source_target_pairs={{0,1},{1,0},{2,3},{3,2},{4,5},{5,4},{6,7},{7,6},{8,9},{9,8},{10,11... | collective-permute-start | bytes 1376264 | tf_op jit(solution)/shard_map/ppermute | solution.py:313
  124.4 11.3 %collective-permute-start.12 = (bf16[112,2048]{1,0:T(8,128)(2,1)S(1)}, bf16[112,2048]{1,0:T(8,128)(2,1)S(1)}, u32[]{:S(2)}, u32[]{:S(2)}) collective-permute-start(bf16[112,2048]{1,0:T(8,128)(2,1)S(1)} %collective-permute-done.10.refs_1_), channel_id=1, source_target_pairs={{0,1},{1,0},{2,3},{3,2},{4,5},{5,4},{6,7},{7,6},{8,9},{9,8},{10,11... | collective-permute-start | bytes 1376264 | tf_op jit(solution)/shard_map/ppermute | solution.py:313
  129.9 16.4 %collective-permute-start.20 = (bf16[224,2048]{1,0:T(8,128)(2,1)S(1)}, bf16[224,2048]{1,0:T(8,128)(2,1)S(1)}, u32[]{:S(2)}, u32[]{:S(2)}) collective-permute-start(bf16[224,2048]{1,0:T(8,128)(2,1)S(1)} %get-tuple-element.50), channel_id=1, source_target_pairs={{0,1},{1,0},{2,3},{3,2},{4,5},{5,4},{6,7},{7,6},{8,9},{9,8},{10,11... | collective-permute-start | bytes 2752520 | tf_op jit(solution)/shard_map/ppermute | solution.py:313
  135.2 14.9 %collective-permute-start.25 = (bf16[224,2048]{1,0:T(8,128)(2,1)S(1)}, bf16[224,2048]{1,0:T(8,128)(2,1)S(1)}, u32[]{:S(2)}, u32[]{:S(2)}) collective-permute-start(bf16[224,2048]{1,0:T(8,128)(2,1)S(1)} %get-tuple-element.52), channel_id=1, source_target_pairs={{0,1},{1,0},{2,3},{3,2},{4,5},{5,4},{6,7},{7,6},{8,9},{9,8},{10,11... | collective-permute-start | bytes 2752520 | tf_op jit(solution)/shard_map/ppermute | solution.py:313
  140.8 11.2 %collective-permute-start.13 = (bf16[224,2048]{1,0:T(8,128)(2,1)S(1)}, bf16[224,2048]{1,0:T(8,128)(2,1)S(1)}, u32[]{:S(2)}, u32[]{:S(2)}) collective-permute-start(bf16[224,2048]{1,0:T(8,128)(2,1)S(1)} %get-tuple-element.48), channel_id=1, source_target_pairs={{0,1},{1,0},{2,3},{3,2},{4,5},{5,4},{6,7},{7,6},{8,9},{9,8},{10,11... | collective-permute-start | bytes 2752520 | tf_op jit(solution)/shard_map/ppermute | solution.py:313
  146.5 14.7 %collective-permute-start.21 = (bf16[112,2048]{1,0:T(8,128)(2,1)S(1)}, bf16[112,2048]{1,0:T(8,128)(2,1)S(1)}, u32[]{:S(2)}, u32[]{:S(2)}) collective-permute-start(bf16[112,2048]{1,0:T(8,128)(2,1)S(1)} %shard_map.145), channel_id=1, source_target_pairs={{0,2},{1,3},{2,4},{3,5},{4,6},{5,7},{6,0},{7,1},{8,10},{9,11},{10,... | collective-permute-start | bytes 1376264 | tf_op jit(solution)/shard_map/ppermute | solution.py:313
  146.5 18.5 %collective-permute-start.8 = (bf16[224,2048]{1,0:T(8,128)(2,1)S(1)}, bf16[224,2048]{1,0:T(8,128)(2,1)S(1)}, u32[]{:S(2)}, u32[]{:S(2)}) collective-permute-start(bf16[224,2048]{1,0:T(8,128)(2,1)S(1)} %get-tuple-element.46), channel_id=1, source_target_pairs={{0,1},{1,0},{2,3},{3,2},{4,5},{5,4},{6,7},{7,6},{8,9},{9,8},{10,11... | collective-permute-start | bytes 2752520 | tf_op jit(solution)/shard_map/ppermute | solution.py:313
  147.2 14.2 %collective-permute-start.28 = (bf16[112,2048]{1,0:T(8,128)(2,1)S(1)}, bf16[112,2048]{1,0:T(8,128)(2,1)S(1)}, u32[]{:S(2)}, u32[]{:S(2)}) collective-permute-start(bf16[112,2048]{1,0:T(8,128)(2,1)S(1)} %shard_map.150), channel_id=1, source_target_pairs={{0,6},{1,7},{2,0},{3,1},{4,2},{5,3},{6,4},{7,5},{8,14},{9,15},{10,... | collective-permute-start | bytes 1376264 | tf_op jit(solution)/shard_map/ppermute | solution.py:313
  150.3 20.6 %collective-permute-start.26 = (bf16[112,2048]{1,0:T(8,128)(2,1)S(1)}, bf16[112,2048]{1,0:T(8,128)(2,1)S(1)}, u32[]{:S(2)}, u32[]{:S(2)}) collective-permute-start(bf16[112,2048]{1,0:T(8,128)(2,1)S(1)} %shard_map.148), channel_id=1, source_target_pairs={{0,6},{1,7},{2,0},{3,1},{4,2},{5,3},{6,4},{7,5},{8,14},{9,15},{10,... | collective-permute-start | bytes 1376264 | tf_op jit(solution)/shard_map/ppermute | solution.py:313
  152.0 18.9 %collective-permute-start.27 = (bf16[112,2048]{1,0:T(8,128)(2,1)S(1)}, bf16[112,2048]{1,0:T(8,128)(2,1)S(1)}, u32[]{:S(2)}, u32[]{:S(2)}) collective-permute-start(bf16[112,2048]{1,0:T(8,128)(2,1)S(1)} %shard_map.149), channel_id=1, source_target_pairs={{0,2},{1,3},{2,4},{3,5},{4,6},{5,7},{6,0},{7,1},{8,10},{9,11},{10,... | collective-permute-start | bytes 1376264 | tf_op jit(solution)/shard_map/ppermute | solution.py:313
  161.3 18.9 %collective-permute-start.22 = (bf16[112,2048]{1,0:T(8,128)(2,1)S(1)}, bf16[112,2048]{1,0:T(8,128)(2,1)S(1)}, u32[]{:S(2)}, u32[]{:S(2)}) collective-permute-start(bf16[112,2048]{1,0:T(8,128)(2,1)S(1)} %shard_map.146), channel_id=1, source_target_pairs={{0,2},{1,3},{2,4},{3,5},{4,6},{5,7},{6,0},{7,1},{8,10},{9,11},{10,... | collective-permute-start | bytes 1376264 | tf_op jit(solution)/shard_map/ppermute | solution.py:313
  161.7 18.6 %collective-permute-start.29 = (bf16[112,2048]{1,0:T(8,128)(2,1)S(1)}, bf16[112,2048]{1,0:T(8,128)(2,1)S(1)}, u32[]{:S(2)}, u32[]{:S(2)}) collective-permute-start(bf16[112,2048]{1,0:T(8,128)(2,1)S(1)} %shard_map.151), channel_id=1, source_target_pairs={{0,6},{1,7},{2,0},{3,1},{4,2},{5,3},{6,4},{7,5},{8,14},{9,15},{10,... | collective-permute-start | bytes 1376264 | tf_op jit(solution)/shard_map/ppermute | solution.py:313
  182.0 32.9 %all-to-all-start.4 = ((bf16[32,8,1792]{2,1,0:T(8,128)(2,1)}), bf16[32,8,1792]{2,1,0:T(8,128)(2,1)S(1)}, u32[]{:S(2)}, u32[]{:S(2)}) async-start(bf16[32,8,1792]{2,1,0:T(8,128)(2,1)} %bitcast.10), calls=%async_computation.4 | async-start | bytes 1835008 | tf_op jit(solution)/shard_map/all_to_all | solution.py:591
  (16 other events, 375.5 us)

commit v2 on v1

--- a/solution.py
+++ b/solution.py
@@ -25,6 +25,7 @@
 USED = 7
 UNIT = 16
 BLOCK = 256
+EARLY = 64
 
 
 def dot(a, b):
@@ -179,12 +180,15 @@
     copy_rows(both_ref, half, high_ref, 0, half)
 
 
-def repack_rows_kernel(low_ref, high_ref, core_ref, *refs):
-    *chips, out_ref, turned = refs
+def repack_rows_kernel(*refs, counts):
+    out_ref, turned = refs[-2:]
     size = out_ref.shape[0]
     peers = size // SLOTS
     each = peers // UNIT
-    sources = [(low_ref, high_ref), (core_ref,), chips[0::2], chips[1::2]]
+    sources, start = [], 0
+    for count in counts:
+        sources.append(refs[start : start + count])
+        start += count
     for u, parts in enumerate(zip(*map(units, sources))):
         total = sum(ref[place, :].astype(F32) for ref, place in parts).astype(BF)
         c, start = u // each, u % each * UNIT
@@ -195,24 +199,37 @@
     out_ref[...] = dot(by_peer(size), turned[...]).astype(BF)
 
 
-def add_kernel(own_ref, core_ref, *refs, first):
-    *more, out_ref = refs
-
-    def body(start):
-        place = pl.ds(start, UNIT)
-        total = own_ref[place, :].astype(F32) + core_ref[pl.ds(first + start, UNIT), :].astype(F32)
-        for ref in more:
-            total = total + ref[place, :].astype(F32)
-        out_ref[place, :] = total.astype(BF)
-
-    by_unit(own_ref.shape[0], body)
-
-
-def add(own, core, second, *more):
+def add_kernel(*refs, windows):
+    outs = refs[-len(windows) :]
+    for (own, core, more, own_first, core_first), out_ref in zip(windows, outs):
+
+        def body(start):
+            total = refs[own][pl.ds(own_first + start, UNIT), :].astype(F32)
+            total = total + refs[core][pl.ds(core_first + start, UNIT), :].astype(F32)
+            if more is not None:
+                total = total + refs[more][pl.ds(start, UNIT), :].astype(F32)
+            out_ref[pl.ds(start, UNIT), :] = total.astype(BF)
+
+        by_unit(out_ref.shape[0], body)
+
+
+def add(own, core, second, more, first, rows):
+    windows = [(0, 1, 2, first, own.shape[0] * second + first)]
     return vmem_call(
-        lambda *refs: add_kernel(*refs, first=own.shape[0] * second),
-        jax.ShapeDtypeStruct(own.shape, BF),
-    )(own, core, *more)
+        lambda *refs: add_kernel(*refs, windows=windows),
+        [jax.ShapeDtypeStruct((rows, own.shape[1]), BF)],
+    )(own, core, more)[0]
+
+
+def add_both(a, b, core, pieces, skip=0):
+    rows, width = a.shape
+    windows = [
+        (half, 2, None, first, skip + rows * half + first) for half in (0, 1) for first, _ in pieces
+    ]
+    return vmem_call(
+        lambda *refs: add_kernel(*refs, windows=windows),
+        [jax.ShapeDtypeStruct((count, width), BF) for _ in (0, 1) for _, count in pieces],
+    )(a, b, core)
 
 
 def route_rows_kernel(slot_ref, weight_ref, high_ref, low_ref):
@@ -234,7 +251,7 @@
         out_ref[:, columns] = (hidden_ref[:, columns].astype(F32) + got).astype(BF)
 
 
-def expert_kernel(*refs, count):
+def expert_kernel(*refs, count, tiles):
     parts = refs[:count]
     gate_ref, up_ref, down_ref = refs[count : count + 3]
     outs = refs[count + 3 : -2]
@@ -252,7 +269,7 @@
         for part, start in zip(parts, starts(parts)):
             copy_rows(rows, start, part, 0, part.shape[0])
 
-    tile = rows.shape[0] // 2
+    tile = rows.shape[0] // tiles
     last = step == pl.num_programs(0) - 1
 
     def one_tile(k, carry):
@@ -271,7 +288,7 @@
 
         return carry
 
-    lax.fori_loop(0, 2, one_tile, 0)
+    lax.fori_loop(0, tiles, one_tile, 0)
 
     @pl.when(last)
     def _():
@@ -279,15 +296,16 @@
             copy_rows(out, 0, rows, start, out.shape[0])
 
 
-def expert(parts, gate, up, down):
+def expert(own, fetched, gate, up, down, tiles):
+    parts = (*own, *fetched)
     count = len(parts)
     height = sum(part.shape[0] for part in parts)
     width = parts[0].shape[1]
     chunk = gate.shape[2] // 2
-    outs = [parts[0].shape, parts[1].shape, (height // 2, width)]
+    outs = [part.shape for part in own] + [(height // 2, width)]
 
     return pl.pallas_call(
-        lambda *refs: expert_kernel(*refs, count=count),
+        lambda *refs: expert_kernel(*refs, count=count, tiles=tiles),
         grid=(2,),
         in_specs=[whole(part.shape) for part in parts]
         + [
@@ -314,39 +332,40 @@
 
 
 def routed_experts(low, high, both, gate, up, down):
-    def run(*parts):
-        return expert(parts, gate, up, down)
+    def both_cores(own, *fetched, tiles):
+        *outs, others = expert(own, fetched, gate, up, down, tiles)
+        return *outs, shift(others, OTHER_CORE)
+
+    def swap(*parts):
+        return [shift(part, OTHER_CORE) for part in parts]
 
     below_low, above_high = shift(low, UP), shift(high, DOWN)
     other = shift(both, OTHER_CORE)
     below_high, above_low = shift(high, UP), shift(low, DOWN)
-    own_low, own_high, own = run(low, high, other)
     far_low, far_high = shift(below_low, UP), shift(above_high, DOWN)
-
-    def both_cores(a, b):
-        fetched = [shift(c, OTHER_CORE) for c in (a, b)]
-        out_a, out_b, others = run(a, b, *fetched)
-        back = shift(others, OTHER_CORE)
-        return (out_a, back, 0), (out_b, back, 1)
-
-    first = both_cores(below_low, above_high)
-    second = both_cores(below_high, above_low)
-    far = both_cores(far_low, far_high)
-    from_above_low = shift(add(*first[0]), DOWN)
-    from_below_high = shift(add(*first[1]), UP)
-    to_above_low = shift(add(*far[0]), UP)
-    to_below_high = shift(add(*far[1]), DOWN)
-    from_above_high = shift(add(*second[0], to_below_high), DOWN)
-    from_below_low = shift(add(*second[1], to_above_low), UP)
-    own_back = shift(own, OTHER_CORE)
+    near = (below_low, above_high)
+    own_low, own_high, *first = both_cores((low, high, *near), other, *swap(*near), tiles=8)
+    late = (below_high, above_low)
+    second = both_cores(late, *swap(*late), tiles=4)
+    ends = (far_low, far_high)
+    far = both_cores(ends, *swap(*ends), tiles=2)
+    rows = low.shape[0]
+    pieces = ((0, EARLY), (EARLY, rows - EARLY))
+    to_below, to_above = add_both(*first, ((0, rows),), skip=2 * rows)
+    from_above_low, from_below_high = shift(to_below, DOWN), shift(to_above, UP)
+    to_far = add_both(*far, pieces)
+    from_below_low, from_above_high = [], []
+    for k, window in enumerate(pieces):
+        ups, downs = shift(to_far[k], UP), shift(to_far[2 + k], DOWN)
+        ups = add(second[1], second[2], 1, ups, *window)
+        downs = add(second[0], second[2], 0, downs, *window)
+        from_below_low.append(shift(ups, UP))
+        from_above_high.append(shift(downs, DOWN))
     return (
-        own_low,
-        own_high,
-        own_back,
-        from_below_low,
-        from_above_low,
-        from_below_high,
-        from_above_high,
+        (own_low, own_high),
+        (first[2],),
+        (*from_below_low, from_below_high),
+        (from_above_low, *from_above_high),
     )
 
 
@@ -587,7 +606,10 @@
     route = shape((row_count, sp_count * USED), BF)
     high_weight, low_weight = vmem_call(route_rows_kernel, [route, route])(slots, route_weight)
     parts = routed_experts(*rows, expert_gate, expert_up, expert_down)
-    repacked = vmem_call(repack_rows_kernel, packed, scratch_shapes=turning)(*parts)
+    counts = tuple(map(len, parts))
+    repacked = vmem_call(
+        lambda *refs: repack_rows_kernel(*refs, counts=counts), packed, scratch_shapes=turning
+    )(*[ref for part in parts for ref in part])
     returned = lax.all_to_all(repacked.reshape(message), SP, 0, 0, tiled=True)
     return vmem_call(
         combine_kernel,

time: 218 us -> 216 us (level)
  waiting for transfers between devices: 84.9 us -> 79.1 us
  Pallas kernels: 36.1 us -> 41 us
    ppermute x30 -> x33, waiting for transfers between devices: 53.4 us -> 47.9 us  [shift(): return lax.ppermute(a, 'tp', where)]
    pallas_call x4 -> x3, Pallas kernels: 20.4 us -> 25.2 us  [expert(): pl.pallas_call(lambda *refs: expert_kernel(*refs, count=count, tiles=tile...]
    ppermute x30 -> x33, starting transfers between devices: 26 us -> 28.9 us  [shift(): return lax.ppermute(a, 'tp', where)]
    all_to_all x1, starting transfers between devices: 7.87 us -> 5.57 us  [layer(): returned = lax.all_to_all(repacked.reshape(message), SP, 0, 0, tiled=True)]
  transfers between devices with their start and end apart: 34 -> 37, of which waited for: 12 -> 10; matrix products, arithmetic and copies ran while one was open for 1% -> 1% of each run, Pallas kernels for 12% -> 14%
where the time goes in v2:
time: 216 us
  waiting for transfers between devices  79.1 us (37%)
  starting transfers between devices  51.8 us (24%)
  Pallas kernels  41 us (19%)
  blocking collectives  35.8 us (17%)
  local copies, waits for them, and re-layouts  3.94 us (2%)
  other arithmetic  3.62 us (2%)
    ppermute x33, waiting for transfers between devices, shift(): return lax.ppermute(a, 'tp', where)  47.9 us
    all_to_all x1, blocking collectives, layer(): landed = lax.all_to_all(tokens.reshape(message), SP, 0, 0, tiled=True)  35.8 us
    ppermute x33, starting transfers between devices, shift(): return lax.ppermute(a, 'tp', where)  28.9 us
    pallas_call x3, Pallas kernels, expert(): pl.pallas_call(lambda *refs: expert_kernel(*refs, count=count, tiles=tile...  25.2 us
    all_to_all x1, waiting for transfers between devices, layer(): returned = lax.all_to_all(repacked.reshape(message), SP, 0, 0, tiled=True)  23.9 us
    pallas_call x15, Pallas kernels, call(): pl.pallas_call(body, in_specs=[pl.BlockSpec(memory_space=pltpu.HBM if k i...  15.7 us
    all_to_all x1, starting transfers between devices, layer(): pieces = lax.all_to_all(message, 'sp_0', 0, 0, tiled=True)  8.47 us
    all_to_all x1, waiting for transfers between devices, layer(): lax.all_to_all(mixed.reshape(tp_count, row_count, head_dim), 'tp', 0, 0,...  6.34 us
  transfers between devices with their start and end apart: 37, of which 10 were waited for; matrix products, arithmetic and copies ran while one was open for 1% of the time, Pallas kernels for 14%

profile of v2, /device:TPU:2, one launch (start us, length us, event | category | flops | bytes accessed | tf_op | source)
XLA Modules:
  0.0 215.8 jit_solution(2269898020922458148)
XLA Ops:
  0.1 1.4 fusion
  1.5 2.6 %shard_map.136 = (f32[1,768]{1,0:T(1,128)S(1)}, f32[768,128]{1,0:T(8,128)S(1)}, bf16[4,136,128]{2,1,0:T(8,128)(2,1)}) custom-call(bf16[768,128]{1,0:T(8,128)(2,1)} %refs_1_.4, bf16[768,128]{1,0:T(8,128)(2,1)} %refs_2_.4, f32[1,768]{1,0:T(1,128)} %refs_2_.3, f32[768,128]{1,0:T(8,128)S(1)} %get-tuple-element.72.refs_3_.refs_5_, ...), custom_call_target="tpu_custom_call" | custom-call | tf_op jit(solution)/shard_map/pallas_call | solution.py:69
  4.1 5.5 %all-to-all-start = ((bf16[4,136,128]{2,1,0:T(8,128)(2,1)}), bf16[4,136,128]{2,1,0:T(8,128)(2,1)S(1)}, u32[]{:S(2)}, u32[]{:S(2)}) async-start(bf16[4,136,128]{2,1,0:T(8,128)(2,1)} %get-tuple-element.37), calls=%async_computation | async-start | bytes 278528 | tf_op jit(solution)/shard_map/all_to_all | solution.py:539
  10.5 2.9 %collective-permute-start.1 = (bf16[128,2048]{1,0:T(8,128)(2,1)S(1)}, bf16[128,2048]{1,0:T(8,128)(2,1)S(1)}, u32[]{:S(2)}, u32[]{:S(2)}) collective-permute-start(bf16[128,2048]{1,0:T(8,128)(2,1)S(1)} %copy-done.2), channel_id=1, source_target_pairs={{0,4},{1,5},{2,6},{3,7},{4,0},{5,1},{6,2},{7,3},{8,12},{9,13},{10,... | collective-permute-start | bytes 1572872 | tf_op jit(solution)/shard_map/ppermute | solution.py:331
  15.8 8.5 %all-to-all-start.1 = ((bf16[8,136,128]{2,1,0:T(8,128)(2,1)}), bf16[8,136,128]{2,1,0:T(8,128)(2,1)S(1)}, u32[]{:S(2)}, u32[]{:S(2)}) async-start(bf16[8,136,128]{2,1,0:T(8,128)(2,1)} %copy-done.4), calls=%async_computation.1 | async-start | bytes 557056 | tf_op jit(solution)/shard_map/all_to_all | solution.py:562
  27.4 1.7 shard_map.138
  30.9 4.9 %collective-permute-done.1.refs_4_ = bf16[128,2048]{1,0:T(8,128)(2,1)S(1)} collective-permute-done((bf16[128,2048]{1,0:T(8,128)(2,1)S(1)}, bf16[128,2048]{1,0:T(8,128)(2,1)S(1)}, u32[]{:S(2)}, u32[]{:S(2)}) %collective-permute-start.1) | collective-permute-done | bytes 524320 | tf_op jit(solution)/shard_map/ppermute | solution.py:331
  37.2 2.2 %shard_map.139 = bf16[768,128]{1,0:T(8,128)(2,1)} custom-call(bf16[8,136,128]{2,1,0:T(8,128)(2,1)S(1)} %all-to-all-done.1.refs_0_, s32[1,128]{1,0:T(1,128)S(1)} %broadcast_in_dim.27.refs_1_, f32[128,128]{1,0:T(8,128)S(1)} %get-tuple-element.39.refs_2_, f32[1,128]{1,0:T(1,128)S(1)} %get-tuple-element.40.refs_3_, bf16[768,128]{1,0:T(8,128)(2,1)} %copy-done.6, ...), custom_call_target="tpu_custom_call" | custom-call | tf_op jit(solution)/shard_map/pallas_call | solution.py:69
  39.4 3.4 %all-to-all-start.2 = ((bf16[8,96,128]{2,1,0:T(8,128)(2,1)}), bf16[8,96,128]{2,1,0:T(8,128)(2,1)S(1)}, u32[]{:S(2)}, u32[]{:S(2)}) async-start(bf16[8,96,128]{2,1,0:T(8,128)(2,1)} %bitcast.1), calls=%async_computation.2 | async-start | bytes 393216 | tf_op jit(solution)/shard_map/all_to_all | solution.py:581
  43.2 6.3 %all-to-all-done.2 = bf16[8,96,128]{2,1,0:T(8,128)(2,1)S(1)} async-done(((bf16[8,96,128]{2,1,0:T(8,128)(2,1)}), bf16[8,96,128]{2,1,0:T(8,128)(2,1)S(1)}, u32[]{:S(2)}, u32[]{:S(2)}) %all-to-all-start.2) | async-done | bytes 196640 | tf_op jit(solution)/shard_map/all_to_all | solution.py:581
  49.7 4.4 %shard_map.140 = (bf16[96,2048]{1,0:T(8,128)(2,1)S(1)}, bf16[256,1792]{1,0:T(8,128)(2,1)S(1)}) custom-call(bf16[4,96,128]{2,1,0:T(8,128)(2,1)S(1)} %get-tuple-element.70.refs_0_, bf16[4,96,128]{2,1,0:T(8,128)(2,1)S(1)} %get-tuple-element.69.refs_1_, bf16[128,2048]{1,0:T(8,128)(2,1)S(1)} %copy-done.2, bf16[128,2048]{1,0:T(8,128)(2,1)} %collective-permute-done.refs_3_, ...), custom_call_target="tpu_custom_call" | custom-call | tf_op jit(solution)/shard_map/pallas_call | solution.py:69
  54.1 35.8 %all_to_all.25 = bf16[32,8,1792]{2,1,0:T(8,128)(2,1)S(1)} all-to-all(bf16[32,8,1792]{2,1,0:T(8,128)(2,1)S(1)} %bitcast.39), channel_id=1, replica_groups=mesh['sp_0'=8,'sp_1'=4,'tp'=8] {'sp_0','sp_1'}, dimensions={0} | all-to-all | bytes 1835008 | tf_op jit(solution)/shard_map/all_to_all | solution.py:601
  91.4 2.7 %collective-permute-start.8 = (bf16[112,2048]{1,0:T(8,128)(2,1)S(1)}, bf16[112,2048]{1,0:T(8,128)(2,1)S(1)}, u32[]{:S(2)}, u32[]{:S(2)}) collective-permute-start(bf16[112,2048]{1,0:T(8,128)(2,1)S(1)} %get-tuple-element.47.refs_1_), channel_id=1, source_target_pairs={{0,6},{1,7},{2,0},{3,1},{4,2},{5,3},{6,4},{7,5},{8,14},{9,15},{10,... | collective-permute-start | bytes 1376264 | tf_op jit(solution)/shard_map/ppermute | solution.py:331
  94.0 10.6 %collective-permute-done.7.refs_2_ = bf16[112,2048]{1,0:T(8,128)(2,1)S(1)} collective-permute-done((bf16[112,2048]{1,0:T(8,128)(2,1)S(1)}, bf16[112,2048]{1,0:T(8,128)(2,1)S(1)}, u32[]{:S(2)}, u32[]{:S(2)}) %collective-permute-start.7) | collective-permute-done | bytes 458784 | tf_op jit(solution)/shard_map/ppermute | solution.py:331
  104.7 3.2 %collective-permute-start.19 = (bf16[112,2048]{1,0:T(8,128)(2,1)S(1)}, bf16[112,2048]{1,0:T(8,128)(2,1)S(1)}, u32[]{:S(2)}, u32[]{:S(2)}) collective-permute-start(bf16[112,2048]{1,0:T(8,128)(2,1)S(1)} %collective-permute-done.8.refs_3_), channel_id=1, source_target_pairs={{0,6},{1,7},{2,0},{3,1},{4,2},{5,3},{6,4},{7,5},{8,14},{9,15},{10,... | collective-permute-start | bytes 1376264 | tf_op jit(solution)/shard_map/ppermute | solution.py:331
  108.4 9.3 %collective-permute-done.18.refs_0_ = bf16[112,2048]{1,0:T(8,128)(2,1)S(1)} collective-permute-done((bf16[112,2048]{1,0:T(8,128)(2,1)S(1)}, bf16[112,2048]{1,0:T(8,128)(2,1)S(1)}, u32[]{:S(2)}, u32[]{:S(2)}) %collective-permute-start.18) | collective-permute-done | bytes 458784 | tf_op jit(solution)/shard_map/ppermute | solution.py:331
  118.9 13.3 %shard_map.142 = (bf16[112,2048]{1,0:T(8,128)(2,1)S(1)}, bf16[112,2048]{1,0:T(8,128)(2,1)S(1)}, bf16[112,2048]{1,0:T(8,128)(2,1)S(1)}, bf16[112,2048]{1,0:T(8,128)(2,1)S(1)}, bf16[448,2048]{1,0:T(8,128)(2,1)S(1)}) custom-call(bf16[112,2048]{1,0:T(8,128)(2,1)S(1)} %get-tuple-element.46.refs_0_, bf16[112,2048]{1,0:T(8,128)(2,1)S(1)} %get-tuple-element.47.refs_1_, ...), custom_call_target="tpu_custom_call" | custom-call | flops 5637144576 | bytes 13631488 | tf_op jit(solution)/shard_map/pallas_call | solution.py:307
  133.3 5.1 %shard_map.144 = (bf16[112,2048]{1,0:T(8,128)(2,1)S(1)}, bf16[112,2048]{1,0:T(8,128)(2,1)S(1)}, bf16[224,2048]{1,0:T(8,128)(2,1)S(1)}) custom-call(bf16[112,2048]{1,0:T(8,128)(2,1)S(1)} %collective-permute-done.18.refs_0_, bf16[112,2048]{1,0:T(8,128)(2,1)S(1)} %collective-permute-done.19.refs_1_, bf16[112,2048]{1,0:T(8,128)(2,1)S(1)} %collective-permute-done.20.refs_2_, ...), custom_call_target="tpu_custom_call" | custom-call | flops 2818572288 | bytes 9961472 | tf_op jit(solution)/shard_map/pallas_call | solution.py:307
  138.6 6.8 %shard_map.143 = (bf16[112,2048]{1,0:T(8,128)(2,1)S(1)}, bf16[112,2048]{1,0:T(8,128)(2,1)S(1)}, bf16[224,2048]{1,0:T(8,128)(2,1)S(1)}) custom-call(bf16[112,2048]{1,0:T(8,128)(2,1)S(1)} %collective-permute-done.13.refs_0_, bf16[112,2048]{1,0:T(8,128)(2,1)S(1)} %collective-permute-done.14.refs_1_, bf16[112,2048]{1,0:T(8,128)(2,1)S(1)} %collective-permute-done.15.refs_2_, ...), custom_call_target="tpu_custom_call" | custom-call | flops 2818572288 | bytes 9961472 | tf_op jit(solution)/shard_map/pallas_call | solution.py:307
  146.5 1.9 collective-permute-start.25
  148.4 2.0 collective-permute-start.29
  150.4 1.9 collective-permute-start.31
  152.8 8.8 %collective-permute-done.25.refs_2_ = bf16[48,2048]{1,0:T(8,128)(2,1)S(1)} collective-permute-done((bf16[48,2048]{1,0:T(8,128)(2,1)S(1)}, bf16[48,2048]{1,0:T(8,128)(2,1)S(1)}, u32[]{:S(2)}, u32[]{:S(2)}) %collective-permute-start.25) | collective-permute-done | bytes 196640 | tf_op jit(solution)/shard_map/ppermute | solution.py:331
  161.6 2.0 collective-permute-start.28
  164.1 3.3 %collective-permute-start.30 = (bf16[64,2048]{1,0:T(8,128)(2,1)S(1)}, bf16[64,2048]{1,0:T(8,128)(2,1)S(1)}, u32[]{:S(2)}, u32[]{:S(2)}) collective-permute-start(bf16[64,2048]{1,0:T(8,128)(2,1)S(1)} %shard_map.149), channel_id=1, source_target_pairs={{0,6},{1,7},{2,0},{3,1},{4,2},{5,3},{6,4},{7,5},{8,14},{9,15},{10,... | collective-permute-start | bytes 786440 | tf_op jit(solution)/shard_map/ppermute | solution.py:331
  167.5 8.1 %collective-permute-done.26.refs_4_ = bf16[48,2048]{1,0:T(8,128)(2,1)S(1)} collective-permute-done((bf16[48,2048]{1,0:T(8,128)(2,1)S(1)}, bf16[48,2048]{1,0:T(8,128)(2,1)S(1)}, u32[]{:S(2)}, u32[]{:S(2)}) %collective-permute-start.26) | collective-permute-done | bytes 196640 | tf_op jit(solution)/shard_map/ppermute | solution.py:331
  175.6 2.0 collective-permute-start.32
  177.6 5.1 %collective-permute-done.32.refs_8_ = bf16[48,2048]{1,0:T(8,128)(2,1)S(1)} collective-permute-done((bf16[48,2048]{1,0:T(8,128)(2,1)S(1)}, bf16[48,2048]{1,0:T(8,128)(2,1)S(1)}, u32[]{:S(2)}, u32[]{:S(2)}) %collective-permute-start.32) | collective-permute-done | bytes 196640 | tf_op jit(solution)/shard_map/ppermute | solution.py:331
  182.8 1.7 shard_map.151
  184.5 5.6 %all-to-all-start.4 = ((bf16[32,8,1792]{2,1,0:T(8,128)(2,1)}), bf16[32,8,1792]{2,1,0:T(8,128)(2,1)S(1)}, u32[]{:S(2)}, u32[]{:S(2)}) async-start(bf16[32,8,1792]{2,1,0:T(8,128)(2,1)} %bitcast.10), calls=%async_computation.4 | async-start | bytes 1835008 | tf_op jit(solution)/shard_map/all_to_all | solution.py:613
  190.3 23.9 %all-to-all-done.4 = bf16[32,8,1792]{2,1,0:T(8,128)(2,1)S(1)} async-done(((bf16[32,8,1792]{2,1,0:T(8,128)(2,1)}), bf16[32,8,1792]{2,1,0:T(8,128)(2,1)S(1)}, u32[]{:S(2)}, u32[]{:S(2)}) %all-to-all-start.4) | async-done | bytes 917536 | tf_op jit(solution)/shard_map/all_to_all | solution.py:613
  214.2 1.6 shard_map.153
  (112 shorter events, 16.8 us)
Async XLA Ops:
  4.1 10.9 %all-to-all-start = ((bf16[4,136,128]{2,1,0:T(8,128)(2,1)}), bf16[4,136,128]{2,1,0:T(8,128)(2,1)S(1)}, u32[]{:S(2)}, u32[]{:S(2)}) async-start(bf16[4,136,128]{2,1,0:T(8,128)(2,1)} %get-tuple-element.37), calls=%async_computation | async-start | bytes 278528 | tf_op jit(solution)/shard_map/all_to_all | solution.py:539
  9.6 20.9 %collective-permute-start.2 = (bf16[128,2048]{1,0:T(8,128)(2,1)S(1)}, bf16[128,2048]{1,0:T(8,128)(2,1)S(1)}, u32[]{:S(2)}, u32[]{:S(2)}) collective-permute-start(bf16[128,2048]{1,0:T(8,128)(2,1)S(1)} %copy-done.2), channel_id=1, source_target_pairs={{0,2},{1,3},{2,4},{3,5},{4,6},{5,7},{6,0},{7,1},{8,10},{9,11},{10,... | collective-permute-start | bytes 1572872 | tf_op jit(solution)/shard_map/ppermute | solution.py:331
  10.5 25.2 %collective-permute-start.1 = (bf16[128,2048]{1,0:T(8,128)(2,1)S(1)}, bf16[128,2048]{1,0:T(8,128)(2,1)S(1)}, u32[]{:S(2)}, u32[]{:S(2)}) collective-permute-start(bf16[128,2048]{1,0:T(8,128)(2,1)S(1)} %copy-done.2), channel_id=1, source_target_pairs={{0,4},{1,5},{2,6},{3,7},{4,0},{5,1},{6,2},{7,3},{8,12},{9,13},{10,... | collective-permute-start | bytes 1572872 | tf_op jit(solution)/shard_map/ppermute | solution.py:331
  13.4 22.3 %collective-permute-start = (bf16[128,2048]{1,0:T(8,128)(2,1)S(1)}, bf16[128,2048]{1,0:T(8,128)(2,1)}, u32[]{:S(2)}, u32[]{:S(2)}) collective-permute-start(bf16[128,2048]{1,0:T(8,128)(2,1)S(1)} %copy-done.2), channel_id=1, source_target_pairs={{0,6},{1,7},{2,0},{3,1},{4,2},{5,3},{6,4},{7,5},{8,14},{9,15},{10,... | collective-permute-start | bytes 1572872 | tf_op jit(solution)/shard_map/ppermute | solution.py:331
  14.8 34.9 %collective-permute-start.3 = (bf16[128,2048]{1,0:T(8,128)(2,1)S(1)}, bf16[128,2048]{1,0:T(8,128)(2,1)}, u32[]{:S(2)}, u32[]{:S(2)}) collective-permute-start(bf16[128,2048]{1,0:T(8,128)(2,1)S(1)} %copy-done.2), channel_id=1, source_target_pairs={{0,1},{1,0},{2,3},{3,2},{4,5},{5,4},{6,7},{7,6},{8,9},{9,8},{10,11... | collective-permute-start | bytes 1572872 | tf_op jit(solution)/shard_map/ppermute | solution.py:331
  15.8 21.4 %all-to-all-start.1 = ((bf16[8,136,128]{2,1,0:T(8,128)(2,1)}), bf16[8,136,128]{2,1,0:T(8,128)(2,1)S(1)}, u32[]{:S(2)}, u32[]{:S(2)}) async-start(bf16[8,136,128]{2,1,0:T(8,128)(2,1)} %copy-done.4), calls=%async_computation.1 | async-start | bytes 557056 | tf_op jit(solution)/shard_map/all_to_all | solution.py:562
  30.6 19.1 %collective-permute-start.6 = (bf16[128,2048]{1,0:T(8,128)(2,1)S(1)}, bf16[128,2048]{1,0:T(8,128)(2,1)S(1)}, u32[]{:S(2)}, u32[]{:S(2)}) collective-permute-start(bf16[128,2048]{1,0:T(8,128)(2,1)S(1)} %collective-permute-done.2.refs_5_), channel_id=1, source_target_pairs={{0,1},{1,0},{2,3},{3,2},{4,5},{5,4},{6,7},{7,6},{8,9},{9,8},{10,11... | collective-permute-start | bytes 1572872 | tf_op jit(solution)/shard_map/ppermute | solution.py:331
  35.7 13.9 %collective-permute-start.5 = (bf16[128,2048]{1,0:T(8,128)(2,1)S(1)}, bf16[128,2048]{1,0:T(8,128)(2,1)}, u32[]{:S(2)}, u32[]{:S(2)}) collective-permute-start(bf16[128,2048]{1,0:T(8,128)(2,1)S(1)} %collective-permute-done.1.refs_4_), channel_id=1, source_target_pairs={{0,1},{1,0},{2,3},{3,2},{4,5},{5,4},{6,7},{7,6},{8,9},{9,8},{10,11... | collective-permute-start | bytes 1572872 | tf_op jit(solution)/shard_map/ppermute | solution.py:331
  35.7 14.0 %collective-permute-start.4 = (bf16[128,2048]{1,0:T(8,128)(2,1)}, bf16[128,2048]{1,0:T(8,128)(2,1)}, u32[]{:S(2)}, u32[]{:S(2)}) collective-permute-start(bf16[128,2048]{1,0:T(8,128)(2,1)} %collective-permute-done.refs_3_), channel_id=1, source_target_pairs={{0,1},{1,0},{2,3},{3,2},{4,5},{5,4},{6,7},{7,6},{8,9},{9,8},{10,11... | collective-permute-start | bytes 1572872 | tf_op jit(solution)/shard_map/ppermute | solution.py:331
  39.4 10.1 %all-to-all-start.2 = ((bf16[8,96,128]{2,1,0:T(8,128)(2,1)}), bf16[8,96,128]{2,1,0:T(8,128)(2,1)S(1)}, u32[]{:S(2)}, u32[]{:S(2)}) async-start(bf16[8,96,128]{2,1,0:T(8,128)(2,1)} %bitcast.1), calls=%async_computation.2 | async-start | bytes 393216 | tf_op jit(solution)/shard_map/all_to_all | solution.py:581
  90.4 17.7 %collective-permute-start.9 = (bf16[224,2048]{1,0:T(8,128)(2,1)S(1)}, bf16[224,2048]{1,0:T(8,128)(2,1)S(1)}, u32[]{:S(2)}, u32[]{:S(2)}) collective-permute-start(bf16[224,2048]{1,0:T(8,128)(2,1)S(1)} %get-tuple-element.48), channel_id=1, source_target_pairs={{0,1},{1,0},{2,3},{3,2},{4,5},{5,4},{6,7},{7,6},{8,9},{9,8},{10,11... | collective-permute-start | bytes 2752520 | tf_op jit(solution)/shard_map/ppermute | solution.py:331
  90.5 14.1 %collective-permute-start.7 = (bf16[112,2048]{1,0:T(8,128)(2,1)S(1)}, bf16[112,2048]{1,0:T(8,128)(2,1)S(1)}, u32[]{:S(2)}, u32[]{:S(2)}) collective-permute-start(bf16[112,2048]{1,0:T(8,128)(2,1)S(1)} %get-tuple-element.46.refs_0_), channel_id=1, source_target_pairs={{0,2},{1,3},{2,4},{3,5},{4,6},{5,7},{6,0},{7,1},{8,10},{9,11},{10,... | collective-permute-start | bytes 1376264 | tf_op jit(solution)/shard_map/ppermute | solution.py:331
  91.4 13.3 %collective-permute-start.8 = (bf16[112,2048]{1,0:T(8,128)(2,1)S(1)}, bf16[112,2048]{1,0:T(8,128)(2,1)S(1)}, u32[]{:S(2)}, u32[]{:S(2)}) collective-permute-start(bf16[112,2048]{1,0:T(8,128)(2,1)S(1)} %get-tuple-element.47.refs_1_), channel_id=1, source_target_pairs={{0,6},{1,7},{2,0},{3,1},{4,2},{5,3},{6,4},{7,5},{8,14},{9,15},{10,... | collective-permute-start | bytes 1376264 | tf_op jit(solution)/shard_map/ppermute | solution.py:331
  104.7 13.0 %collective-permute-start.18 = (bf16[112,2048]{1,0:T(8,128)(2,1)S(1)}, bf16[112,2048]{1,0:T(8,128)(2,1)S(1)}, u32[]{:S(2)}, u32[]{:S(2)}) collective-permute-start(bf16[112,2048]{1,0:T(8,128)(2,1)S(1)} %collective-permute-done.7.refs_2_), channel_id=1, source_target_pairs={{0,2},{1,3},{2,4},{3,5},{4,6},{5,7},{6,0},{7,1},{8,10},{9,11},{10,... | collective-permute-start | bytes 1376264 | tf_op jit(solution)/shard_map/ppermute | solution.py:331
  104.7 13.0 %collective-permute-start.10 = (bf16[112,2048]{1,0:T(8,128)(2,1)S(1)}, bf16[112,2048]{1,0:T(8,128)(2,1)S(1)}, u32[]{:S(2)}, u32[]{:S(2)}) collective-permute-start(bf16[112,2048]{1,0:T(8,128)(2,1)S(1)} %collective-permute-done.7.refs_2_), channel_id=1, source_target_pairs={{0,1},{1,0},{2,3},{3,2},{4,5},{5,4},{6,7},{7,6},{8,9},{9,8},{10,11... | collective-permute-start | bytes 1376264 | tf_op jit(solution)/shard_map/ppermute | solution.py:331
  104.7 14.1 %collective-permute-start.19 = (bf16[112,2048]{1,0:T(8,128)(2,1)S(1)}, bf16[112,2048]{1,0:T(8,128)(2,1)S(1)}, u32[]{:S(2)}, u32[]{:S(2)}) collective-permute-start(bf16[112,2048]{1,0:T(8,128)(2,1)S(1)} %collective-permute-done.8.refs_3_), channel_id=1, source_target_pairs={{0,6},{1,7},{2,0},{3,1},{4,2},{5,3},{6,4},{7,5},{8,14},{9,15},{10,... | collective-permute-start | bytes 1376264 | tf_op jit(solution)/shard_map/ppermute | solution.py:331
  107.9 10.9 %collective-permute-start.11 = (bf16[112,2048]{1,0:T(8,128)(2,1)S(1)}, bf16[112,2048]{1,0:T(8,128)(2,1)S(1)}, u32[]{:S(2)}, u32[]{:S(2)}) collective-permute-start(bf16[112,2048]{1,0:T(8,128)(2,1)S(1)} %collective-permute-done.8.refs_3_), channel_id=1, source_target_pairs={{0,1},{1,0},{2,3},{3,2},{4,5},{5,4},{6,7},{7,6},{8,9},{9,8},{10,11... | collective-permute-start | bytes 1376264 | tf_op jit(solution)/shard_map/ppermute | solution.py:331
  108.1 24.6 %collective-permute-start.14 = (bf16[112,2048]{1,0:T(8,128)(2,1)S(1)}, bf16[112,2048]{1,0:T(8,128)(2,1)S(1)}, u32[]{:S(2)}, u32[]{:S(2)}) collective-permute-start(bf16[112,2048]{1,0:T(8,128)(2,1)S(1)} %get-tuple-element.46.refs_0_), channel_id=1, source_target_pairs={{0,6},{1,7},{2,0},{3,1},{4,2},{5,3},{6,4},{7,5},{8,14},{9,15},{10,... | collective-permute-start | bytes 1376264 | tf_op jit(solution)/shard_map/ppermute | solution.py:331
  117.7 15.2 %collective-permute-start.13 = (bf16[112,2048]{1,0:T(8,128)(2,1)S(1)}, bf16[112,2048]{1,0:T(8,128)(2,1)S(1)}, u32[]{:S(2)}, u32[]{:S(2)}) collective-permute-start(bf16[112,2048]{1,0:T(8,128)(2,1)S(1)} %get-tuple-element.47.refs_1_), channel_id=1, source_target_pairs={{0,2},{1,3},{2,4},{3,5},{4,6},{5,7},{6,0},{7,1},{8,10},{9,11},{10,... | collective-permute-start | bytes 1376264 | tf_op jit(solution)/shard_map/ppermute | solution.py:331
  117.7 15.6 %collective-permute-start.20 = (bf16[112,2048]{1,0:T(8,128)(2,1)S(1)}, bf16[112,2048]{1,0:T(8,128)(2,1)S(1)}, u32[]{:S(2)}, u32[]{:S(2)}) collective-permute-start(bf16[112,2048]{1,0:T(8,128)(2,1)S(1)} %collective-permute-done.18.refs_0_), channel_id=1, source_target_pairs={{0,1},{1,0},{2,3},{3,2},{4,5},{5,4},{6,7},{7,6},{8,9},{9,8},{10,11... | collective-permute-start | bytes 1376264 | tf_op jit(solution)/shard_map/ppermute | solution.py:331
  118.8 14.5 %collective-permute-start.21 = (bf16[112,2048]{1,0:T(8,128)(2,1)S(1)}, bf16[112,2048]{1,0:T(8,128)(2,1)S(1)}, u32[]{:S(2)}, u32[]{:S(2)}) collective-permute-start(bf16[112,2048]{1,0:T(8,128)(2,1)S(1)} %collective-permute-done.19.refs_1_), channel_id=1, source_target_pairs={{0,1},{1,0},{2,3},{3,2},{4,5},{5,4},{6,7},{7,6},{8,9},{9,8},{10,11... | collective-permute-start | bytes 1376264 | tf_op jit(solution)/shard_map/ppermute | solution.py:331
  132.2 18.2 %collective-permute-start.12 = (bf16[448,2048]{1,0:T(8,128)(2,1)S(1)}, bf16[448,2048]{1,0:T(8,128)(2,1)S(1)}, u32[]{:S(2)}, u32[]{:S(2)}) collective-permute-start(bf16[448,2048]{1,0:T(8,128)(2,1)S(1)} %get-tuple-element.51), channel_id=1, source_target_pairs={{0,1},{1,0},{2,3},{3,2},{4,5},{5,4},{6,7},{7,6},{8,9},{9,8},{10,11... | collective-permute-start | bytes 5505032 | tf_op jit(solution)/shard_map/ppermute | solution.py:331
  146.2 17.5 %collective-permute-start.23 = (bf16[64,2048]{1,0:T(8,128)(2,1)S(1)}, bf16[64,2048]{1,0:T(8,128)(2,1)S(1)}, u32[]{:S(2)}, u32[]{:S(2)}) collective-permute-start(bf16[64,2048]{1,0:T(8,128)(2,1)S(1)} %get-tuple-element.57), channel_id=1, source_target_pairs={{0,2},{1,3},{2,4},{3,5},{4,6},{5,7},{6,0},{7,1},{8,10},{9,11},{10,... | collective-permute-start | bytes 786440 | tf_op jit(solution)/shard_map/ppermute | solution.py:331
  146.5 15.0 %collective-permute-start.25 = (bf16[48,2048]{1,0:T(8,128)(2,1)S(1)}, bf16[48,2048]{1,0:T(8,128)(2,1)S(1)}, u32[]{:S(2)}, u32[]{:S(2)}) collective-permute-start(bf16[48,2048]{1,0:T(8,128)(2,1)S(1)} %get-tuple-element.58), channel_id=1, source_target_pairs={{0,2},{1,3},{2,4},{3,5},{4,6},{5,7},{6,0},{7,1},{8,10},{9,11},{10,... | collective-permute-start | bytes 589832 | tf_op jit(solution)/shard_map/ppermute | solution.py:331
  148.4 15.5 %collective-permute-start.29 = (bf16[64,2048]{1,0:T(8,128)(2,1)S(1)}, bf16[64,2048]{1,0:T(8,128)(2,1)S(1)}, u32[]{:S(2)}, u32[]{:S(2)}) collective-permute-start(bf16[64,2048]{1,0:T(8,128)(2,1)S(1)} %get-tuple-element.64), channel_id=1, source_target_pairs={{0,6},{1,7},{2,0},{3,1},{4,2},{5,3},{6,4},{7,5},{8,14},{9,15},{10,... | collective-permute-start | bytes 786440 | tf_op jit(solution)/shard_map/ppermute | solution.py:331
  150.4 13.8 %collective-permute-start.31 = (bf16[48,2048]{1,0:T(8,128)(2,1)S(1)}, bf16[48,2048]{1,0:T(8,128)(2,1)S(1)}, u32[]{:S(2)}, u32[]{:S(2)}) collective-permute-start(bf16[48,2048]{1,0:T(8,128)(2,1)S(1)} %get-tuple-element.65), channel_id=1, source_target_pairs={{0,6},{1,7},{2,0},{3,1},{4,2},{5,3},{6,4},{7,5},{8,14},{9,15},{10,... | collective-permute-start | bytes 589832 | tf_op jit(solution)/shard_map/ppermute | solution.py:331
  152.6 30.2 %collective-permute-start.27 = (bf16[112,2048]{1,0:T(8,128)(2,1)S(1)}, bf16[112,2048]{1,0:T(8,128)(2,1)S(1)}, u32[]{:S(2)}, u32[]{:S(2)}) collective-permute-start(bf16[112,2048]{1,0:T(8,128)(2,1)S(1)} %get-tuple-element.61), channel_id=1, source_target_pairs={{0,2},{1,3},{2,4},{3,5},{4,6},{5,7},{6,0},{7,1},{8,10},{9,11},{10,... | collective-permute-start | bytes 1376264 | tf_op jit(solution)/shard_map/ppermute | solution.py:331
  161.6 21.2 %collective-permute-start.28 = (bf16[112,2048]{1,0:T(8,128)(2,1)S(1)}, bf16[112,2048]{1,0:T(8,128)(2,1)S(1)}, u32[]{:S(2)}, u32[]{:S(2)}) collective-permute-start(bf16[112,2048]{1,0:T(8,128)(2,1)S(1)} %get-tuple-element.62), channel_id=1, source_target_pairs={{0,6},{1,7},{2,0},{3,1},{4,2},{5,3},{6,4},{7,5},{8,14},{9,15},{10,... | collective-permute-start | bytes 1376264 | tf_op jit(solution)/shard_map/ppermute | solution.py:331
  163.7 11.9 %collective-permute-start.26 = (bf16[48,2048]{1,0:T(8,128)(2,1)S(1)}, bf16[48,2048]{1,0:T(8,128)(2,1)S(1)}, u32[]{:S(2)}, u32[]{:S(2)}) collective-permute-start(bf16[48,2048]{1,0:T(8,128)(2,1)S(1)} %shard_map.147), channel_id=1, source_target_pairs={{0,2},{1,3},{2,4},{3,5},{4,6},{5,7},{6,0},{7,1},{8,10},{9,11},{10,... | collective-permute-start | bytes 589832 | tf_op jit(solution)/shard_map/ppermute | solution.py:331
  163.9 18.8 %collective-permute-start.24 = (bf16[64,2048]{1,0:T(8,128)(2,1)S(1)}, bf16[64,2048]{1,0:T(8,128)(2,1)S(1)}, u32[]{:S(2)}, u32[]{:S(2)}) collective-permute-start(bf16[64,2048]{1,0:T(8,128)(2,1)S(1)} %shard_map.146), channel_id=1, source_target_pairs={{0,2},{1,3},{2,4},{3,5},{4,6},{5,7},{6,0},{7,1},{8,10},{9,11},{10,... | collective-permute-start | bytes 786440 | tf_op jit(solution)/shard_map/ppermute | solution.py:331
  164.1 18.6 %collective-permute-start.30 = (bf16[64,2048]{1,0:T(8,128)(2,1)S(1)}, bf16[64,2048]{1,0:T(8,128)(2,1)S(1)}, u32[]{:S(2)}, u32[]{:S(2)}) collective-permute-start(bf16[64,2048]{1,0:T(8,128)(2,1)S(1)} %shard_map.149), channel_id=1, source_target_pairs={{0,6},{1,7},{2,0},{3,1},{4,2},{5,3},{6,4},{7,5},{8,14},{9,15},{10,... | collective-permute-start | bytes 786440 | tf_op jit(solution)/shard_map/ppermute | solution.py:331
  184.5 29.7 %all-to-all-start.4 = ((bf16[32,8,1792]{2,1,0:T(8,128)(2,1)}), bf16[32,8,1792]{2,1,0:T(8,128)(2,1)S(1)}, u32[]{:S(2)}, u32[]{:S(2)}) async-start(bf16[32,8,1792]{2,1,0:T(8,128)(2,1)} %bitcast.10), calls=%async_computation.4 | async-start | bytes 1835008 | tf_op jit(solution)/shard_map/all_to_all | solution.py:613
  (19 other events, 378.9 us)

commit v3 on v2

--- a/solution.py
+++ b/solution.py
@@ -251,10 +251,11 @@
         out_ref[:, columns] = (hidden_ref[:, columns].astype(F32) + got).astype(BF)
 
 
-def expert_kernel(*refs, count, tiles):
+def expert_kernel(*refs, count, ready, tiles):
     parts = refs[:count]
     gate_ref, up_ref, down_ref = refs[count : count + 3]
-    outs = refs[count + 3 : -2]
+    passed = refs[count + 3 : count + 3 + ready]
+    outs = refs[count + 3 + ready : -2]
     rows, total = refs[-2:]
     step = pl.program_id(0)
 
@@ -292,27 +293,34 @@
 
     @pl.when(last)
     def _():
+        ahead = 0
+        for ref in passed:
+            copy_rows(outs[-1], ahead, ref, 0, ref.shape[0])
+            ahead += ref.shape[0]
         for out, start in zip(outs, starts(outs)):
-            copy_rows(out, 0, rows, start, out.shape[0])
-
-
-def expert(own, fetched, gate, up, down, tiles):
+            first = ahead if out is outs[-1] else 0
+            copy_rows(out, first, rows, start, out.shape[0] - first)
+
+
+def expert(own, fetched, ready, gate, up, down, tiles):
     parts = (*own, *fetched)
     count = len(parts)
+    ahead = sum(part.shape[0] for part in ready)
     height = sum(part.shape[0] for part in parts)
     width = parts[0].shape[1]
     chunk = gate.shape[2] // 2
-    outs = [part.shape for part in own] + [(height // 2, width)]
+    outs = [part.shape for part in own] + [(ahead + height // 2, width)]
 
     return pl.pallas_call(
-        lambda *refs: expert_kernel(*refs, count=count, tiles=tiles),
+        lambda *refs: expert_kernel(*refs, count=count, ready=len(ready), tiles=tiles),
         grid=(2,),
         in_specs=[whole(part.shape) for part in parts]
         + [
             pl.BlockSpec((1, width, chunk), lambda j: (0, 0, j)),
             pl.BlockSpec((1, width, chunk), lambda j: (0, 0, j)),
             pl.BlockSpec((1, chunk, width), lambda j: (0, j, 0)),
-        ],
+        ]
+        + [whole(part.shape) for part in ready],
         out_specs=[whole(out) for out in outs],
         out_shape=[jax.ShapeDtypeStruct(out, BF) for out in outs],
         scratch_shapes=[pltpu.VMEM((height, width), BF), pltpu.VMEM((height, width), F32)],
@@ -324,7 +332,7 @@
             bytes_accessed=2 * (2 * height * width + 3 * width * gate.shape[2]),
             transcendentals=height * gate.shape[2],
         ),
-    )(*parts, gate, up, down)
+    )(*parts, gate, up, down, *ready)
 
 
 def shift(a, where):
@@ -332,9 +340,8 @@
 
 
 def routed_experts(low, high, both, gate, up, down):
-    def both_cores(own, *fetched, tiles):
-        *outs, others = expert(own, fetched, gate, up, down, tiles)
-        return *outs, shift(others, OTHER_CORE)
+    def run(own, *fetched, ready=(), tiles=4):
+        return expert(own, fetched, ready, gate, up, down, tiles)
 
     def swap(*parts):
         return [shift(part, OTHER_CORE) for part in parts]
@@ -342,13 +349,17 @@
     below_low, above_high = shift(low, UP), shift(high, DOWN)
     other = shift(both, OTHER_CORE)
     below_high, above_low = shift(high, UP), shift(low, DOWN)
+    own_low, own_high, own = run((low, high), other)
     far_low, far_high = shift(below_low, UP), shift(above_high, DOWN)
     near = (below_low, above_high)
-    own_low, own_high, *first = both_cores((low, high, *near), other, *swap(*near), tiles=8)
+    *first, others = run(near, *swap(*near), ready=(own,))
+    first += swap(others)
     late = (below_high, above_low)
-    second = both_cores(late, *swap(*late), tiles=4)
+    *second, others = run(late, *swap(*late))
+    second += swap(others)
     ends = (far_low, far_high)
-    far = both_cores(ends, *swap(*ends), tiles=2)
+    *far, others = run(ends, *swap(*ends), tiles=2)
+    far += swap(others)
     rows = low.shape[0]
     pieces = ((0, EARLY), (EARLY, rows - EARLY))
     to_below, to_above = add_both(*first, ((0, rows),), skip=2 * rows)
@@ -493,9 +504,10 @@
 
 def slot_indices(route_ids, experts):
     flat_ids = route_ids.reshape(-1)
-    chosen = (flat_ids[:, None] == jnp.arange(experts, dtype=jnp.int32)[None, :]).astype(jnp.int32)
-    before = jnp.cumsum(chosen, axis=0) - chosen
-    rank_in = jnp.sum(before * chosen, axis=1)
+    chosen = (flat_ids[:, None] == jnp.arange(experts, dtype=jnp.int32)[None, :]).astype(BF)
+    place = jnp.arange(flat_ids.shape[0])
+    before = dot((place[:, None] > place[None, :]).astype(BF), chosen)
+    rank_in = jnp.sum(before * chosen.astype(F32), axis=1).astype(jnp.int32)
     return (flat_ids * SLOTS + rank_in).reshape(route_ids.shape)
 
 

time: 216 us -> 215 us (level)
  starting transfers between devices: 51.8 us -> 46.6 us
    ppermute x33, starting transfers between devices: 28.9 us -> 24.3 us  [shift(): return lax.ppermute(a, 'tp', where)]
    ppermute x33, waiting for transfers between devices: 47.9 us -> 52.3 us  [shift(): return lax.ppermute(a, 'tp', where)]
    all_to_all x1, waiting for transfers between devices: 23.9 us -> 21.7 us  [layer(): returned = lax.all_to_all(repacked.reshape(message), SP, 0, 0, tiled=True)]
    pallas_call x3 -> x4, Pallas kernels: 25.2 us -> 25.7 us  [expert(): pl.pallas_call(lambda *refs: expert_kernel(*refs, count=count, ready=len(...]
  transfers between devices with their start and end apart: 37 -> 37, of which waited for: 10 -> 12; matrix products, arithmetic and copies ran while one was open for 1% -> 1% of each run, Pallas kernels for 14% -> 14%
where the time goes in v3:
time: 215 us; the launch traced here: 214 us
  waiting for transfers between devices  81.2 us (38%)
  starting transfers between devices  46.6 us (22%)
  Pallas kernels  41.4 us (19%)
  blocking collectives  36.5 us (17%)
  local copies, waits for them, and re-layouts  5.79 us (3%)
    ppermute x33, waiting for transfers between devices, shift(): return lax.ppermute(a, 'tp', where)  52.3 us
    all_to_all x1, blocking collectives, layer(): landed = lax.all_to_all(tokens.reshape(message), SP, 0, 0, tiled=True)  36.5 us
    pallas_call x4, Pallas kernels, expert(): pl.pallas_call(lambda *refs: expert_kernel(*refs, count=count, ready=len(...  25.7 us
    ppermute x33, starting transfers between devices, shift(): return lax.ppermute(a, 'tp', where)  24.3 us
    all_to_all x1, waiting for transfers between devices, layer(): returned = lax.all_to_all(repacked.reshape(message), SP, 0, 0, tiled=True)  21.7 us
    pallas_call x15, Pallas kernels, call(): pl.pallas_call(body, in_specs=[pl.BlockSpec(memory_space=pltpu.HBM if k i...  15.8 us
    all_to_all x1, starting transfers between devices, layer(): pieces = lax.all_to_all(message, 'sp_0', 0, 0, tiled=True)  7.83 us
    all_to_all x1, waiting for transfers between devices, layer(): lax.all_to_all(mixed.reshape(tp_count, row_count, head_dim), 'tp', 0, 0,...  6.53 us
  transfers between devices with their start and end apart: 37, of which 12 were waited for; matrix products, arithmetic and copies ran while one was open for 1% of the time, Pallas kernels for 14%

profile of v3, /device:TPU:2, one launch (start us, length us, event | category | flops | bytes accessed | tf_op | source)
XLA Modules:
  0.0 213.8 jit_solution(9993410182815553303)
XLA Ops:
  0.1 1.4 fusion.1
  1.5 2.6 %shard_map.136 = (f32[1,768]{1,0:T(1,128)S(1)}, f32[768,128]{1,0:T(8,128)S(1)}, bf16[4,136,128]{2,1,0:T(8,128)(2,1)}) custom-call(bf16[768,128]{1,0:T(8,128)(2,1)} %refs_1_.4, bf16[768,128]{1,0:T(8,128)(2,1)} %refs_2_.4, f32[1,768]{1,0:T(1,128)} %refs_2_.3, f32[768,128]{1,0:T(8,128)S(1)} %get-tuple-element.74.refs_3_.refs_5_, ...), custom_call_target="tpu_custom_call" | custom-call | tf_op jit(solution)/shard_map/pallas_call | solution.py:69
  4.1 5.5 %all-to-all-start = ((bf16[4,136,128]{2,1,0:T(8,128)(2,1)}), bf16[4,136,128]{2,1,0:T(8,128)(2,1)S(1)}, u32[]{:S(2)}, u32[]{:S(2)}) async-start(bf16[4,136,128]{2,1,0:T(8,128)(2,1)} %get-tuple-element.38), calls=%async_computation | async-start | bytes 278528 | tf_op jit(solution)/shard_map/all_to_all | solution.py:551
  9.6 2.3 %collective-permute-start = (bf16[128,2048]{1,0:T(8,128)(2,1)S(1)}, bf16[128,2048]{1,0:T(8,128)(2,1)S(1)}, u32[]{:S(2)}, u32[]{:S(2)}) collective-permute-start(bf16[128,2048]{1,0:T(8,128)(2,1)S(1)} %copy-done.2), channel_id=1, source_target_pairs={{0,6},{1,7},{2,0},{3,1},{4,2},{5,3},{6,4},{7,5},{8,14},{9,15},{10,... | collective-permute-start | bytes 1572872 | tf_op jit(solution)/shard_map/ppermute | solution.py:339
  15.0 7.8 %all-to-all-start.1 = ((bf16[8,136,128]{2,1,0:T(8,128)(2,1)}), bf16[8,136,128]{2,1,0:T(8,128)(2,1)S(1)}, u32[]{:S(2)}, u32[]{:S(2)}) async-start(bf16[8,136,128]{2,1,0:T(8,128)(2,1)} %copy-done.4), calls=%async_computation.1 | async-start | bytes 557056 | tf_op jit(solution)/shard_map/all_to_all | solution.py:574
  26.4 1.7 shard_map.138
  29.5 4.3 %collective-permute-done.refs_3_ = bf16[128,2048]{1,0:T(8,128)(2,1)S(1)} collective-permute-done((bf16[128,2048]{1,0:T(8,128)(2,1)S(1)}, bf16[128,2048]{1,0:T(8,128)(2,1)S(1)}, u32[]{:S(2)}, u32[]{:S(2)}) %collective-permute-start) | collective-permute-done | bytes 524320 | tf_op jit(solution)/shard_map/ppermute | solution.py:339
  34.3 3.3 %collective-permute-done.2.refs_5_ = bf16[128,2048]{1,0:T(8,128)(2,1)} collective-permute-done((bf16[128,2048]{1,0:T(8,128)(2,1)S(1)}, bf16[128,2048]{1,0:T(8,128)(2,1)}, u32[]{:S(2)}, u32[]{:S(2)}) %collective-permute-start.2) | collective-permute-done | bytes 524320 | tf_op jit(solution)/shard_map/ppermute | solution.py:339
  37.7 2.2 %shard_map.139 = bf16[768,128]{1,0:T(8,128)(2,1)} custom-call(bf16[8,136,128]{2,1,0:T(8,128)(2,1)S(1)} %all-to-all-done.1.refs_0_, s32[1,128]{1,0:T(1,128)S(1)} %broadcast_in_dim.29.refs_1_, f32[128,128]{1,0:T(8,128)S(1)} %get-tuple-element.40.refs_2_, f32[1,128]{1,0:T(1,128)S(1)} %get-tuple-element.41.refs_3_, bf16[768,128]{1,0:T(8,128)(2,1)} %copy-done.6, ...), custom_call_target="tpu_custom_call" | custom-call | tf_op jit(solution)/shard_map/pallas_call | solution.py:69
  39.9 3.4 %all-to-all-start.2 = ((bf16[8,96,128]{2,1,0:T(8,128)(2,1)}), bf16[8,96,128]{2,1,0:T(8,128)(2,1)S(1)}, u32[]{:S(2)}, u32[]{:S(2)}) async-start(bf16[8,96,128]{2,1,0:T(8,128)(2,1)} %bitcast.1), calls=%async_computation.2 | async-start | bytes 393216 | tf_op jit(solution)/shard_map/all_to_all | solution.py:593
  43.5 6.5 %all-to-all-done.2 = bf16[8,96,128]{2,1,0:T(8,128)(2,1)S(1)} async-done(((bf16[8,96,128]{2,1,0:T(8,128)(2,1)}), bf16[8,96,128]{2,1,0:T(8,128)(2,1)S(1)}, u32[]{:S(2)}, u32[]{:S(2)}) %all-to-all-start.2) | async-done | bytes 196640 | tf_op jit(solution)/shard_map/all_to_all | solution.py:593
  50.2 4.4 %shard_map.140 = (bf16[96,2048]{1,0:T(8,128)(2,1)S(1)}, bf16[256,1792]{1,0:T(8,128)(2,1)S(1)}) custom-call(bf16[4,96,128]{2,1,0:T(8,128)(2,1)S(1)} %get-tuple-element.72.refs_0_, bf16[4,96,128]{2,1,0:T(8,128)(2,1)S(1)} %get-tuple-element.71.refs_1_, bf16[128,2048]{1,0:T(8,128)(2,1)S(1)} %copy-done.2, bf16[128,2048]{1,0:T(8,128)(2,1)S(1)} %collective-permute-done.refs_3_, ...), custom_call_target="tpu_custom_call" | custom-call | tf_op jit(solution)/shard_map/pallas_call | solution.py:69
  54.6 36.5 %all_to_all.25 = bf16[32,8,1792]{2,1,0:T(8,128)(2,1)S(1)} all-to-all(bf16[32,8,1792]{2,1,0:T(8,128)(2,1)S(1)} %bitcast.27), channel_id=1, replica_groups=mesh['sp_0'=8,'sp_1'=4,'tp'=8] {'sp_0','sp_1'}, dimensions={0} | all-to-all | bytes 1835008 | tf_op jit(solution)/shard_map/all_to_all | solution.py:613
  92.3 2.7 %collective-permute-start.9 = (bf16[112,2048]{1,0:T(8,128)(2,1)S(1)}, bf16[112,2048]{1,0:T(8,128)(2,1)S(1)}, u32[]{:S(2)}, u32[]{:S(2)}) collective-permute-start(bf16[112,2048]{1,0:T(8,128)(2,1)S(1)} %get-tuple-element.48.refs_1_), channel_id=1, source_target_pairs={{0,6},{1,7},{2,0},{3,1},{4,2},{5,3},{6,4},{7,5},{8,14},{9,15},{10,... | collective-permute-start | bytes 1376264 | tf_op jit(solution)/shard_map/ppermute | solution.py:339
  95.0 10.8 %collective-permute-done.8.refs_0_ = bf16[112,2048]{1,0:T(8,128)(2,1)S(1)} collective-permute-done((bf16[112,2048]{1,0:T(8,128)(2,1)S(1)}, bf16[112,2048]{1,0:T(8,128)(2,1)S(1)}, u32[]{:S(2)}, u32[]{:S(2)}) %collective-permute-start.8) | collective-permute-done | bytes 458784 | tf_op jit(solution)/shard_map/ppermute | solution.py:339
  105.8 3.2 %collective-permute-start.19 = (bf16[112,2048]{1,0:T(8,128)(2,1)S(1)}, bf16[112,2048]{1,0:T(8,128)(2,1)S(1)}, u32[]{:S(2)}, u32[]{:S(2)}) collective-permute-start(bf16[112,2048]{1,0:T(8,128)(2,1)S(1)} %collective-permute-done.9.refs_1_), channel_id=1, source_target_pairs={{0,6},{1,7},{2,0},{3,1},{4,2},{5,3},{6,4},{7,5},{8,14},{9,15},{10,... | collective-permute-start | bytes 1376264 | tf_op jit(solution)/shard_map/ppermute | solution.py:339
  109.6 6.8 %shard_map.142 = (bf16[112,2048]{1,0:T(8,128)(2,1)S(1)}, bf16[112,2048]{1,0:T(8,128)(2,1)S(1)}, bf16[224,2048]{1,0:T(8,128)(2,1)S(1)}) custom-call(bf16[112,2048]{1,0:T(8,128)(2,1)S(1)} %get-tuple-element.47.refs_0_, bf16[112,2048]{1,0:T(8,128)(2,1)S(1)} %get-tuple-element.48.refs_1_, bf16[224,2048]{1,0:T(8,128)(2,1)S(1)} %collective-permute-done.7.refs_2_, ...), custom_call_target="tpu_custom_call" | custom-call | flops 2818572288 | bytes 9961472 | tf_op jit(solution)/shard_map/pallas_call | solution.py:314
  116.4 4.0 %collective-permute-done.18.refs_0_ = bf16[112,2048]{1,0:T(8,128)(2,1)S(1)} collective-permute-done((bf16[112,2048]{1,0:T(8,128)(2,1)S(1)}, bf16[112,2048]{1,0:T(8,128)(2,1)S(1)}, u32[]{:S(2)}, u32[]{:S(2)}) %collective-permute-start.18) | collective-permute-done | bytes 458784 | tf_op jit(solution)/shard_map/ppermute | solution.py:339
  120.9 6.9 %shard_map.143 = (bf16[112,2048]{1,0:T(8,128)(2,1)S(1)}, bf16[112,2048]{1,0:T(8,128)(2,1)S(1)}, bf16[448,2048]{1,0:T(8,128)(2,1)S(1)}) custom-call(bf16[112,2048]{1,0:T(8,128)(2,1)S(1)} %collective-permute-done.8.refs_0_, bf16[112,2048]{1,0:T(8,128)(2,1)S(1)} %collective-permute-done.9.refs_1_, bf16[112,2048]{1,0:T(8,128)(2,1)S(1)} %collective-permute-done.10.refs_2_, ...), custom_call_target="tpu_custom_call" | custom-call | flops 2818572288 | bytes 9961472 | tf_op jit(solution)/shard_map/pallas_call | solution.py:314
  130.2 5.1 %shard_map.145 = (bf16[112,2048]{1,0:T(8,128)(2,1)S(1)}, bf16[112,2048]{1,0:T(8,128)(2,1)S(1)}, bf16[224,2048]{1,0:T(8,128)(2,1)S(1)}) custom-call(bf16[112,2048]{1,0:T(8,128)(2,1)S(1)} %collective-permute-done.18.refs_0_, bf16[112,2048]{1,0:T(8,128)(2,1)S(1)} %collective-permute-done.19.refs_1_, bf16[112,2048]{1,0:T(8,128)(2,1)S(1)} %collective-permute-done.20.refs_2_, ...), custom_call_target="tpu_custom_call" | custom-call | flops 2818572288 | bytes 9961472 | tf_op jit(solution)/shard_map/pallas_call | solution.py:314
  135.9 6.8 %shard_map.144 = (bf16[112,2048]{1,0:T(8,128)(2,1)S(1)}, bf16[112,2048]{1,0:T(8,128)(2,1)S(1)}, bf16[224,2048]{1,0:T(8,128)(2,1)S(1)}) custom-call(bf16[112,2048]{1,0:T(8,128)(2,1)S(1)} %collective-permute-done.13.refs_0_, bf16[112,2048]{1,0:T(8,128)(2,1)S(1)} %collective-permute-done.14.refs_1_, bf16[112,2048]{1,0:T(8,128)(2,1)S(1)} %collective-permute-done.15.refs_2_, ...), custom_call_target="tpu_custom_call" | custom-call | flops 2818572288 | bytes 9961472 | tf_op jit(solution)/shard_map/pallas_call | solution.py:314
  143.3 3.0 %collective-permute-start.29 = (bf16[64,2048]{1,0:T(8,128)(2,1)S(1)}, bf16[64,2048]{1,0:T(8,128)(2,1)S(1)}, u32[]{:S(2)}, u32[]{:S(2)}) collective-permute-start(bf16[64,2048]{1,0:T(8,128)(2,1)S(1)} %get-tuple-element.66), channel_id=1, source_target_pairs={{0,6},{1,7},{2,0},{3,1},{4,2},{5,3},{6,4},{7,5},{8,14},{9,15},{10,... | collective-permute-start | bytes 786440 | tf_op jit(solution)/shard_map/ppermute | solution.py:339
  146.4 1.9 collective-permute-start.23
  148.8 8.0 %collective-permute-done.31.refs_2_ = bf16[48,2048]{1,0:T(8,128)(2,1)S(1)} collective-permute-done((bf16[48,2048]{1,0:T(8,128)(2,1)S(1)}, bf16[48,2048]{1,0:T(8,128)(2,1)S(1)}, u32[]{:S(2)}, u32[]{:S(2)}) %collective-permute-start.31) | collective-permute-done | bytes 196640 | tf_op jit(solution)/shard_map/ppermute | solution.py:339
  156.8 3.7 %collective-permute-start.28 = (bf16[112,2048]{1,0:T(8,128)(2,1)S(1)}, bf16[112,2048]{1,0:T(8,128)(2,1)S(1)}, u32[]{:S(2)}, u32[]{:S(2)}) collective-permute-start(bf16[112,2048]{1,0:T(8,128)(2,1)S(1)} %get-tuple-element.64), channel_id=1, source_target_pairs={{0,6},{1,7},{2,0},{3,1},{4,2},{5,3},{6,4},{7,5},{8,14},{9,15},{10,... | collective-permute-start | bytes 1376264 | tf_op jit(solution)/shard_map/ppermute | solution.py:339
  161.0 2.1 collective-permute-start.24
  163.2 12.4 %collective-permute-done.32.refs_8_ = bf16[48,2048]{1,0:T(8,128)(2,1)S(1)} collective-permute-done((bf16[48,2048]{1,0:T(8,128)(2,1)S(1)}, bf16[48,2048]{1,0:T(8,128)(2,1)S(1)}, u32[]{:S(2)}, u32[]{:S(2)}) %collective-permute-start.32) | collective-permute-done | bytes 196640 | tf_op jit(solution)/shard_map/ppermute | solution.py:339
  175.6 7.3 %collective-permute-done.26.refs_4_ = bf16[48,2048]{1,0:T(8,128)(2,1)S(1)} collective-permute-done((bf16[48,2048]{1,0:T(8,128)(2,1)S(1)}, bf16[48,2048]{1,0:T(8,128)(2,1)S(1)}, u32[]{:S(2)}, u32[]{:S(2)}) %collective-permute-start.26) | collective-permute-done | bytes 196640 | tf_op jit(solution)/shard_map/ppermute | solution.py:339
  182.9 1.7 shard_map.152
  184.7 5.6 %all-to-all-start.4 = ((bf16[32,8,1792]{2,1,0:T(8,128)(2,1)}), bf16[32,8,1792]{2,1,0:T(8,128)(2,1)S(1)}, u32[]{:S(2)}, u32[]{:S(2)}) async-start(bf16[32,8,1792]{2,1,0:T(8,128)(2,1)} %bitcast.9), calls=%async_computation.4 | async-start | bytes 1835008 | tf_op jit(solution)/shard_map/all_to_all | solution.py:625
  190.5 21.7 %all-to-all-done.4 = bf16[32,8,1792]{2,1,0:T(8,128)(2,1)S(1)} async-done(((bf16[32,8,1792]{2,1,0:T(8,128)(2,1)}), bf16[32,8,1792]{2,1,0:T(8,128)(2,1)S(1)}, u32[]{:S(2)}, u32[]{:S(2)}) %all-to-all-start.4) | async-done | bytes 917536 | tf_op jit(solution)/shard_map/all_to_all | solution.py:625
  212.2 1.6 shard_map.154
  (109 shorter events, 16.0 us)
Async XLA Ops:
  4.1 10.1 %all-to-all-start = ((bf16[4,136,128]{2,1,0:T(8,128)(2,1)}), bf16[4,136,128]{2,1,0:T(8,128)(2,1)S(1)}, u32[]{:S(2)}, u32[]{:S(2)}) async-start(bf16[4,136,128]{2,1,0:T(8,128)(2,1)} %get-tuple-element.38), calls=%async_computation | async-start | bytes 278528 | tf_op jit(solution)/shard_map/all_to_all | solution.py:551
  9.6 24.2 %collective-permute-start = (bf16[128,2048]{1,0:T(8,128)(2,1)S(1)}, bf16[128,2048]{1,0:T(8,128)(2,1)S(1)}, u32[]{:S(2)}, u32[]{:S(2)}) collective-permute-start(bf16[128,2048]{1,0:T(8,128)(2,1)S(1)} %copy-done.2), channel_id=1, source_target_pairs={{0,6},{1,7},{2,0},{3,1},{4,2},{5,3},{6,4},{7,5},{8,14},{9,15},{10,... | collective-permute-start | bytes 1572872 | tf_op jit(solution)/shard_map/ppermute | solution.py:339
  12.0 21.9 %collective-permute-start.1 = (bf16[128,2048]{1,0:T(8,128)(2,1)S(1)}, bf16[128,2048]{1,0:T(8,128)(2,1)S(1)}, u32[]{:S(2)}, u32[]{:S(2)}) collective-permute-start(bf16[128,2048]{1,0:T(8,128)(2,1)S(1)} %copy-done.2), channel_id=1, source_target_pairs={{0,4},{1,5},{2,6},{3,7},{4,0},{5,1},{6,2},{7,3},{8,12},{9,13},{10,... | collective-permute-start | bytes 1572872 | tf_op jit(solution)/shard_map/ppermute | solution.py:339
  12.6 25.0 %collective-permute-start.2 = (bf16[128,2048]{1,0:T(8,128)(2,1)S(1)}, bf16[128,2048]{1,0:T(8,128)(2,1)}, u32[]{:S(2)}, u32[]{:S(2)}) collective-permute-start(bf16[128,2048]{1,0:T(8,128)(2,1)S(1)} %copy-done.2), channel_id=1, source_target_pairs={{0,2},{1,3},{2,4},{3,5},{4,6},{5,7},{6,0},{7,1},{8,10},{9,11},{10,... | collective-permute-start | bytes 1572872 | tf_op jit(solution)/shard_map/ppermute | solution.py:339
  15.0 22.7 %all-to-all-start.1 = ((bf16[8,136,128]{2,1,0:T(8,128)(2,1)}), bf16[8,136,128]{2,1,0:T(8,128)(2,1)S(1)}, u32[]{:S(2)}, u32[]{:S(2)}) async-start(bf16[8,136,128]{2,1,0:T(8,128)(2,1)} %copy-done.4), calls=%async_computation.1 | async-start | bytes 557056 | tf_op jit(solution)/shard_map/all_to_all | solution.py:574
  22.8 27.3 %collective-permute-start.3 = (bf16[128,2048]{1,0:T(8,128)(2,1)S(1)}, bf16[128,2048]{1,0:T(8,128)(2,1)}, u32[]{:S(2)}, u32[]{:S(2)}) collective-permute-start(bf16[128,2048]{1,0:T(8,128)(2,1)S(1)} %copy-done.2), channel_id=1, source_target_pairs={{0,1},{1,0},{2,3},{3,2},{4,5},{5,4},{6,7},{7,6},{8,9},{9,8},{10,11... | collective-permute-start | bytes 1572872 | tf_op jit(solution)/shard_map/ppermute | solution.py:339
  33.8 16.3 %collective-permute-start.4 = (bf16[128,2048]{1,0:T(8,128)(2,1)S(1)}, bf16[128,2048]{1,0:T(8,128)(2,1)S(1)}, u32[]{:S(2)}, u32[]{:S(2)}) collective-permute-start(bf16[128,2048]{1,0:T(8,128)(2,1)S(1)} %collective-permute-done.refs_3_), channel_id=1, source_target_pairs={{0,1},{1,0},{2,3},{3,2},{4,5},{5,4},{6,7},{7,6},{8,9},{9,8},{10,11... | collective-permute-start | bytes 1572872 | tf_op jit(solution)/shard_map/ppermute | solution.py:339
  33.8 16.3 %collective-permute-start.5 = (bf16[128,2048]{1,0:T(8,128)(2,1)S(1)}, bf16[128,2048]{1,0:T(8,128)(2,1)}, u32[]{:S(2)}, u32[]{:S(2)}) collective-permute-start(bf16[128,2048]{1,0:T(8,128)(2,1)S(1)} %collective-permute-done.1.refs_4_), channel_id=1, source_target_pairs={{0,1},{1,0},{2,3},{3,2},{4,5},{5,4},{6,7},{7,6},{8,9},{9,8},{10,11... | collective-permute-start | bytes 1572872 | tf_op jit(solution)/shard_map/ppermute | solution.py:339
  37.6 12.5 %collective-permute-start.6 = (bf16[128,2048]{1,0:T(8,128)(2,1)}, bf16[128,2048]{1,0:T(8,128)(2,1)}, u32[]{:S(2)}, u32[]{:S(2)}) collective-permute-start(bf16[128,2048]{1,0:T(8,128)(2,1)} %collective-permute-done.2.refs_5_), channel_id=1, source_target_pairs={{0,1},{1,0},{2,3},{3,2},{4,5},{5,4},{6,7},{7,6},{8,9},{9,8},{10,11... | collective-permute-start | bytes 1572872 | tf_op jit(solution)/shard_map/ppermute | solution.py:339
  39.9 10.1 %all-to-all-start.2 = ((bf16[8,96,128]{2,1,0:T(8,128)(2,1)}), bf16[8,96,128]{2,1,0:T(8,128)(2,1)S(1)}, u32[]{:S(2)}, u32[]{:S(2)}) async-start(bf16[8,96,128]{2,1,0:T(8,128)(2,1)} %bitcast.1), calls=%async_computation.2 | async-start | bytes 393216 | tf_op jit(solution)/shard_map/all_to_all | solution.py:593
  91.6 18.0 %collective-permute-start.7 = (bf16[224,2048]{1,0:T(8,128)(2,1)S(1)}, bf16[224,2048]{1,0:T(8,128)(2,1)S(1)}, u32[]{:S(2)}, u32[]{:S(2)}) collective-permute-start(bf16[224,2048]{1,0:T(8,128)(2,1)S(1)} %get-tuple-element.49), channel_id=1, source_target_pairs={{0,1},{1,0},{2,3},{3,2},{4,5},{5,4},{6,7},{7,6},{8,9},{9,8},{10,11... | collective-permute-start | bytes 2752520 | tf_op jit(solution)/shard_map/ppermute | solution.py:339
  91.7 14.1 %collective-permute-start.8 = (bf16[112,2048]{1,0:T(8,128)(2,1)S(1)}, bf16[112,2048]{1,0:T(8,128)(2,1)S(1)}, u32[]{:S(2)}, u32[]{:S(2)}) collective-permute-start(bf16[112,2048]{1,0:T(8,128)(2,1)S(1)} %get-tuple-element.47.refs_0_), channel_id=1, source_target_pairs={{0,2},{1,3},{2,4},{3,5},{4,6},{5,7},{6,0},{7,1},{8,10},{9,11},{10,... | collective-permute-start | bytes 1376264 | tf_op jit(solution)/shard_map/ppermute | solution.py:339
  92.3 13.5 %collective-permute-start.9 = (bf16[112,2048]{1,0:T(8,128)(2,1)S(1)}, bf16[112,2048]{1,0:T(8,128)(2,1)S(1)}, u32[]{:S(2)}, u32[]{:S(2)}) collective-permute-start(bf16[112,2048]{1,0:T(8,128)(2,1)S(1)} %get-tuple-element.48.refs_1_), channel_id=1, source_target_pairs={{0,6},{1,7},{2,0},{3,1},{4,2},{5,3},{6,4},{7,5},{8,14},{9,15},{10,... | collective-permute-start | bytes 1376264 | tf_op jit(solution)/shard_map/ppermute | solution.py:339
  105.8 14.6 %collective-permute-start.18 = (bf16[112,2048]{1,0:T(8,128)(2,1)S(1)}, bf16[112,2048]{1,0:T(8,128)(2,1)S(1)}, u32[]{:S(2)}, u32[]{:S(2)}) collective-permute-start(bf16[112,2048]{1,0:T(8,128)(2,1)S(1)} %collective-permute-done.8.refs_0_), channel_id=1, source_target_pairs={{0,2},{1,3},{2,4},{3,5},{4,6},{5,7},{6,0},{7,1},{8,10},{9,11},{10,... | collective-permute-start | bytes 1376264 | tf_op jit(solution)/shard_map/ppermute | solution.py:339
  105.8 14.6 %collective-permute-start.19 = (bf16[112,2048]{1,0:T(8,128)(2,1)S(1)}, bf16[112,2048]{1,0:T(8,128)(2,1)S(1)}, u32[]{:S(2)}, u32[]{:S(2)}) collective-permute-start(bf16[112,2048]{1,0:T(8,128)(2,1)S(1)} %collective-permute-done.9.refs_1_), channel_id=1, source_target_pairs={{0,6},{1,7},{2,0},{3,1},{4,2},{5,3},{6,4},{7,5},{8,14},{9,15},{10,... | collective-permute-start | bytes 1376264 | tf_op jit(solution)/shard_map/ppermute | solution.py:339
  109.1 11.4 %collective-permute-start.10 = (bf16[112,2048]{1,0:T(8,128)(2,1)S(1)}, bf16[112,2048]{1,0:T(8,128)(2,1)S(1)}, u32[]{:S(2)}, u32[]{:S(2)}) collective-permute-start(bf16[112,2048]{1,0:T(8,128)(2,1)S(1)} %collective-permute-done.8.refs_0_), channel_id=1, source_target_pairs={{0,1},{1,0},{2,3},{3,2},{4,5},{5,4},{6,7},{7,6},{8,9},{9,8},{10,11... | collective-permute-start | bytes 1376264 | tf_op jit(solution)/shard_map/ppermute | solution.py:339
  109.1 11.9 %collective-permute-start.11 = (bf16[112,2048]{1,0:T(8,128)(2,1)S(1)}, bf16[112,2048]{1,0:T(8,128)(2,1)S(1)}, u32[]{:S(2)}, u32[]{:S(2)}) collective-permute-start(bf16[112,2048]{1,0:T(8,128)(2,1)S(1)} %collective-permute-done.9.refs_1_), channel_id=1, source_target_pairs={{0,1},{1,0},{2,3},{3,2},{4,5},{5,4},{6,7},{7,6},{8,9},{9,8},{10,11... | collective-permute-start | bytes 1376264 | tf_op jit(solution)/shard_map/ppermute | solution.py:339
  109.6 19.3 %collective-permute-start.13 = (bf16[112,2048]{1,0:T(8,128)(2,1)S(1)}, bf16[112,2048]{1,0:T(8,128)(2,1)S(1)}, u32[]{:S(2)}, u32[]{:S(2)}) collective-permute-start(bf16[112,2048]{1,0:T(8,128)(2,1)S(1)} %get-tuple-element.48.refs_1_), channel_id=1, source_target_pairs={{0,2},{1,3},{2,4},{3,5},{4,6},{5,7},{6,0},{7,1},{8,10},{9,11},{10,... | collective-permute-start | bytes 1376264 | tf_op jit(solution)/shard_map/ppermute | solution.py:339
  120.4 9.7 %collective-permute-start.14 = (bf16[112,2048]{1,0:T(8,128)(2,1)S(1)}, bf16[112,2048]{1,0:T(8,128)(2,1)S(1)}, u32[]{:S(2)}, u32[]{:S(2)}) collective-permute-start(bf16[112,2048]{1,0:T(8,128)(2,1)S(1)} %get-tuple-element.47.refs_0_), channel_id=1, source_target_pairs={{0,6},{1,7},{2,0},{3,1},{4,2},{5,3},{6,4},{7,5},{8,14},{9,15},{10,... | collective-permute-start | bytes 1376264 | tf_op jit(solution)/shard_map/ppermute | solution.py:339
  120.4 9.7 %collective-permute-start.20 = (bf16[112,2048]{1,0:T(8,128)(2,1)S(1)}, bf16[112,2048]{1,0:T(8,128)(2,1)S(1)}, u32[]{:S(2)}, u32[]{:S(2)}) collective-permute-start(bf16[112,2048]{1,0:T(8,128)(2,1)S(1)} %collective-permute-done.18.refs_0_), channel_id=1, source_target_pairs={{0,1},{1,0},{2,3},{3,2},{4,5},{5,4},{6,7},{7,6},{8,9},{9,8},{10,11... | collective-permute-start | bytes 1376264 | tf_op jit(solution)/shard_map/ppermute | solution.py:339
  120.4 9.7 %collective-permute-start.21 = (bf16[112,2048]{1,0:T(8,128)(2,1)S(1)}, bf16[112,2048]{1,0:T(8,128)(2,1)S(1)}, u32[]{:S(2)}, u32[]{:S(2)}) collective-permute-start(bf16[112,2048]{1,0:T(8,128)(2,1)S(1)} %collective-permute-done.19.refs_1_), channel_id=1, source_target_pairs={{0,1},{1,0},{2,3},{3,2},{4,5},{5,4},{6,7},{7,6},{8,9},{9,8},{10,11... | collective-permute-start | bytes 1376264 | tf_op jit(solution)/shard_map/ppermute | solution.py:339
  127.9 20.5 %collective-permute-start.12 = (bf16[448,2048]{1,0:T(8,128)(2,1)S(1)}, bf16[448,2048]{1,0:T(8,128)(2,1)S(1)}, u32[]{:S(2)}, u32[]{:S(2)}) collective-permute-start(bf16[448,2048]{1,0:T(8,128)(2,1)S(1)} %get-tuple-element.53), channel_id=1, source_target_pairs={{0,1},{1,0},{2,3},{3,2},{4,5},{5,4},{6,7},{7,6},{8,9},{9,8},{10,11... | collective-permute-start | bytes 5505032 | tf_op jit(solution)/shard_map/ppermute | solution.py:339
  143.3 17.2 %collective-permute-start.29 = (bf16[64,2048]{1,0:T(8,128)(2,1)S(1)}, bf16[64,2048]{1,0:T(8,128)(2,1)S(1)}, u32[]{:S(2)}, u32[]{:S(2)}) collective-permute-start(bf16[64,2048]{1,0:T(8,128)(2,1)S(1)} %get-tuple-element.66), channel_id=1, source_target_pairs={{0,6},{1,7},{2,0},{3,1},{4,2},{5,3},{6,4},{7,5},{8,14},{9,15},{10,... | collective-permute-start | bytes 786440 | tf_op jit(solution)/shard_map/ppermute | solution.py:339
  146.3 10.4 %collective-permute-start.31 = (bf16[48,2048]{1,0:T(8,128)(2,1)S(1)}, bf16[48,2048]{1,0:T(8,128)(2,1)S(1)}, u32[]{:S(2)}, u32[]{:S(2)}) collective-permute-start(bf16[48,2048]{1,0:T(8,128)(2,1)S(1)} %get-tuple-element.67), channel_id=1, source_target_pairs={{0,6},{1,7},{2,0},{3,1},{4,2},{5,3},{6,4},{7,5},{8,14},{9,15},{10,... | collective-permute-start | bytes 589832 | tf_op jit(solution)/shard_map/ppermute | solution.py:339
  146.4 14.3 %collective-permute-start.23 = (bf16[64,2048]{1,0:T(8,128)(2,1)S(1)}, bf16[64,2048]{1,0:T(8,128)(2,1)S(1)}, u32[]{:S(2)}, u32[]{:S(2)}) collective-permute-start(bf16[64,2048]{1,0:T(8,128)(2,1)S(1)} %get-tuple-element.59), channel_id=1, source_target_pairs={{0,2},{1,3},{2,4},{3,5},{4,6},{5,7},{6,0},{7,1},{8,10},{9,11},{10,... | collective-permute-start | bytes 786440 | tf_op jit(solution)/shard_map/ppermute | solution.py:339
  148.4 12.7 %collective-permute-start.25 = (bf16[48,2048]{1,0:T(8,128)(2,1)S(1)}, bf16[48,2048]{1,0:T(8,128)(2,1)S(1)}, u32[]{:S(2)}, u32[]{:S(2)}) collective-permute-start(bf16[48,2048]{1,0:T(8,128)(2,1)S(1)} %get-tuple-element.60), channel_id=1, source_target_pairs={{0,2},{1,3},{2,4},{3,5},{4,6},{5,7},{6,0},{7,1},{8,10},{9,11},{10,... | collective-permute-start | bytes 589832 | tf_op jit(solution)/shard_map/ppermute | solution.py:339
  148.7 34.2 %collective-permute-start.27 = (bf16[112,2048]{1,0:T(8,128)(2,1)S(1)}, bf16[112,2048]{1,0:T(8,128)(2,1)S(1)}, u32[]{:S(2)}, u32[]{:S(2)}) collective-permute-start(bf16[112,2048]{1,0:T(8,128)(2,1)S(1)} %get-tuple-element.63), channel_id=1, source_target_pairs={{0,2},{1,3},{2,4},{3,5},{4,6},{5,7},{6,0},{7,1},{8,10},{9,11},{10,... | collective-permute-start | bytes 1376264 | tf_op jit(solution)/shard_map/ppermute | solution.py:339
  156.8 26.2 %collective-permute-start.28 = (bf16[112,2048]{1,0:T(8,128)(2,1)S(1)}, bf16[112,2048]{1,0:T(8,128)(2,1)S(1)}, u32[]{:S(2)}, u32[]{:S(2)}) collective-permute-start(bf16[112,2048]{1,0:T(8,128)(2,1)S(1)} %get-tuple-element.64), channel_id=1, source_target_pairs={{0,6},{1,7},{2,0},{3,1},{4,2},{5,3},{6,4},{7,5},{8,14},{9,15},{10,... | collective-permute-start | bytes 1376264 | tf_op jit(solution)/shard_map/ppermute | solution.py:339
  160.5 15.0 %collective-permute-start.32 = (bf16[48,2048]{1,0:T(8,128)(2,1)S(1)}, bf16[48,2048]{1,0:T(8,128)(2,1)S(1)}, u32[]{:S(2)}, u32[]{:S(2)}) collective-permute-start(bf16[48,2048]{1,0:T(8,128)(2,1)S(1)} %shard_map.151), channel_id=1, source_target_pairs={{0,6},{1,7},{2,0},{3,1},{4,2},{5,3},{6,4},{7,5},{8,14},{9,15},{10,... | collective-permute-start | bytes 589832 | tf_op jit(solution)/shard_map/ppermute | solution.py:339
  160.8 22.1 %collective-permute-start.30 = (bf16[64,2048]{1,0:T(8,128)(2,1)S(1)}, bf16[64,2048]{1,0:T(8,128)(2,1)S(1)}, u32[]{:S(2)}, u32[]{:S(2)}) collective-permute-start(bf16[64,2048]{1,0:T(8,128)(2,1)S(1)} %shard_map.150), channel_id=1, source_target_pairs={{0,6},{1,7},{2,0},{3,1},{4,2},{5,3},{6,4},{7,5},{8,14},{9,15},{10,... | collective-permute-start | bytes 786440 | tf_op jit(solution)/shard_map/ppermute | solution.py:339
  161.0 21.9 %collective-permute-start.24 = (bf16[64,2048]{1,0:T(8,128)(2,1)S(1)}, bf16[64,2048]{1,0:T(8,128)(2,1)S(1)}, u32[]{:S(2)}, u32[]{:S(2)}) collective-permute-start(bf16[64,2048]{1,0:T(8,128)(2,1)S(1)} %shard_map.147), channel_id=1, source_target_pairs={{0,2},{1,3},{2,4},{3,5},{4,6},{5,7},{6,0},{7,1},{8,10},{9,11},{10,... | collective-permute-start | bytes 786440 | tf_op jit(solution)/shard_map/ppermute | solution.py:339
  184.7 27.5 %all-to-all-start.4 = ((bf16[32,8,1792]{2,1,0:T(8,128)(2,1)}), bf16[32,8,1792]{2,1,0:T(8,128)(2,1)S(1)}, u32[]{:S(2)}, u32[]{:S(2)}) async-start(bf16[32,8,1792]{2,1,0:T(8,128)(2,1)} %bitcast.9), calls=%async_computation.4 | async-start | bytes 1835008 | tf_op jit(solution)/shard_map/all_to_all | solution.py:625
  (20 other events, 375.3 us)

commit v4 on v3

--- a/solution.py
+++ b/solution.py
@@ -111,12 +111,12 @@
     tokens, width = residual_ref.shape
     size = out_ref.shape[0]
     peers = size // SLOTS
-    heads = jnp.concatenate([ref[k] for ref in (mine_ref, others_ref) for k in range(4)], axis=1)
+    heads = [ref[k] for ref in (mine_ref, others_ref) for k in range(4)]
     squares = jnp.zeros((tokens, 1), F32)
     step = 512
     for start in range(0, width, step):
         columns = slice(start, start + step)
-        projected = dot(heads, jnp.concatenate([w[:, columns] for w in weights], axis=0))
+        projected = sum(dot(head, w[:, columns]) for head, w in zip(heads, weights))
         if start == 0:
             ready()
         hidden = (residual_ref[:, columns].astype(F32) + projected).astype(BF)
@@ -355,10 +355,10 @@
     *first, others = run(near, *swap(*near), ready=(own,))
     first += swap(others)
     late = (below_high, above_low)
-    *second, others = run(late, *swap(*late))
+    *second, others = run(late, *swap(*late), tiles=2)
     second += swap(others)
     ends = (far_low, far_high)
-    *far, others = run(ends, *swap(*ends), tiles=2)
+    *far, others = run(ends, *swap(*ends), tiles=1)
     far += swap(others)
     rows = low.shape[0]
     pieces = ((0, EARLY), (EARLY, rows - EARLY))
@@ -380,6 +380,7 @@
     )
 
 
+STEP = 32
 STATE = 136
 
 
@@ -408,14 +409,31 @@
     return result, between
 
 
-def rotate(ref, cos_ref, sin_ref):
+def rotary(cos_ref, sin_ref):
+    steps = cos_ref.shape[0] - STEP
+    near_cos, near_sin = cos_ref[steps:, :], sin_ref[steps:, :]
+    cosine, sine = [], []
+    for k in range(steps):
+        far_cos, far_sin = cos_ref[k : k + 1, :], sin_ref[k : k + 1, :]
+        cosine.append(far_cos * near_cos - far_sin * near_sin)
+        sine.append(far_sin * near_cos + far_cos * near_sin)
+    return jnp.concatenate(cosine, axis=0), jnp.concatenate(sine, axis=0)
+
+
+def rotate(ref, cosine, sine):
     rows = ref[...].astype(F32)
-    return rows * cos_ref[...] + pltpu.roll(rows, ref.shape[1] // 2, 1) * sin_ref[...]
+    return rows * cosine + pltpu.roll(rows, ref.shape[1] // 2, 1) * sine
+
+
+def column_of(row_ref, width):
+    rows = [row_ref[:, k : k + width] for k in range(0, row_ref.shape[1], width)]
+    return jnp.concatenate([jnp.broadcast_to(r, (width, width)).T for r in rows], axis=0)
 
 
 def block_state_kernel(
-    key_ref, value_ref, decay_ref, cos_ref, sin_ref, row_ref, column_ref, out_ref, ready
+    key_ref, value_ref, decay_ref, cos_ref, sin_ref, row_ref, out_ref, ready
 ):
+    cosine, sine = rotary(cos_ref, sin_ref)
     ready()
     width = key_ref.shape[1]
     blocks = decay_ref.shape[1] // width
@@ -440,9 +458,8 @@
         rows.append(sums[k : k + 1, :] + total)
         total = rows[-1][:, width - 1 :]
     row_ref[...] = jnp.concatenate(rows, axis=1)
-    column = jnp.concatenate([jnp.broadcast_to(r, (width, width)).T for r in rows], axis=0)
-    column_ref[...] = column
-    rotated = rotate(key_ref, cos_ref, sin_ref).astype(BF)
+    column = column_of(row_ref, width)
+    rotated = rotate(key_ref, cosine, sine).astype(BF)
     damped = (rotated.astype(F32) * jnp.exp(total - column)).astype(BF)
     state = lax.dot_general(
         damped, value_ref[...], (((0,), (0,)), ((), ())), preferred_element_type=F32
@@ -460,11 +477,13 @@
 
 
 def within_kernel(
-    query_ref, key_ref, value_ref, row_ref, column_ref, cos_ref, sin_ref, turned_ref, out_ref, rotated
+    query_ref, key_ref, value_ref, row_ref, cos_ref, sin_ref, turned_ref, out_ref, rotated, column
 ):
     width = query_ref.shape[1]
-    turned_ref[...] = (rotate(query_ref, cos_ref, sin_ref) * width**-0.5).astype(BF)
-    rotated[...] = rotate(key_ref, cos_ref, sin_ref).astype(BF)
+    cosine, sine = rotary(cos_ref, sin_ref)
+    turned_ref[...] = (rotate(query_ref, cosine, sine) * width**-0.5).astype(BF)
+    rotated[...] = rotate(key_ref, cosine, sine).astype(BF)
+    column[...] = column_of(row_ref, width)
     step = 256
 
     def some_rows(k, carry):
@@ -477,7 +496,7 @@
         )
         i = lax.broadcasted_iota(jnp.int32, scores.shape, 0) + k * step
         causal = i >= lax.broadcasted_iota(jnp.int32, scores.shape, 1)
-        spread = column_ref[place, 0:1] - row_ref[...]
+        spread = column[place, 0:1] - row_ref[...]
         decays = jnp.where(causal, jnp.exp(jnp.where(causal, spread, 0.0)), 0.0)
         out_ref[place, :] = dot((scores * decays).astype(BF), value_ref[...])
         return carry
@@ -486,17 +505,18 @@
 
 
 def mix_kernel(
-    in_ref, index_ref, inside_ref, ahead_ref, turned_ref, within_ref, column_ref, gate_ref, gain_ref, out_ref, ready
+    in_ref, index_ref, inside_ref, ahead_ref, turned_ref, within_ref, row_ref, gate_ref, gain_ref, out_ref, ready
 ):
     totals, states = read_states(in_ref)
     before, _ = weighted(totals, states, index_ref[...])
     carried = jnp.exp(ahead_ref[...]) * before + inside_ref[...]
     high = carried.astype(BF)
     low = (carried - high.astype(F32)).astype(BF)
+    decay = jnp.exp(column_of(row_ref, turned_ref.shape[1]))
     ready()
     turned = turned_ref[...]
     readout = dot(turned, high) + dot(turned, low)
-    out = within_ref[...] + jnp.exp(column_ref[...]) * readout
+    out = within_ref[...] + decay * readout
     scale = lax.rsqrt(jnp.mean(out * out, axis=1, keepdims=True) + epsilon)
     gate = gate_ref[...].astype(F32)
     out_ref[...] = (out * scale * gain_ref[...] * jax.nn.silu(gate)).astype(BF)
@@ -531,7 +551,10 @@
     sp_count = lax.axis_size(SP)
     tp = lax.axis_index("tp")
     tp_count = lax.axis_size("tp")
-    positions = (lax.axis_index(SP) * length + jnp.arange(length, dtype=jnp.int32)).astype(F32)
+    start = lax.axis_index(SP) * length
+    positions = jnp.concatenate(
+        [start + jnp.arange(0, length, STEP, dtype=jnp.int32), jnp.arange(STEP, dtype=jnp.int32)]
+    ).astype(F32)
     column = jnp.arange(head_dim)
     half_dim = head_dim // 2
     inverse = rope_base ** (-(2 * (column % half_dim)).astype(F32) / head_dim)
@@ -539,11 +562,10 @@
     cosine = jnp.cos(angles)
     sine = jnp.sin(angles) * jnp.where(column < half_dim, -1.0, 1.0)[None, :]
     shape = jax.ShapeDtypeStruct
-    decay_row, decay_column, message = vmem_call(
+    decay_row, message = vmem_call(
         block_state_kernel,
         [
             shape((1, length), F32),
-            shape((length, head_dim), F32),
             shape((lax.axis_size("sp_1"), STATE, head_dim), BF),
         ],
         late=(0, 1, 2),
@@ -552,13 +574,13 @@
     rotated_queries, within = vmem_call(
         within_kernel,
         [shape((length, head_dim), BF), shape((length, head_dim), F32)],
-        scratch_shapes=[pltpu.VMEM((length, head_dim), BF)],
+        scratch_shapes=[pltpu.VMEM((length, head_dim), BF), pltpu.VMEM((length, head_dim), F32)],
         cost_estimate=pl.CostEstimate(
             flops=3 * length * length * head_dim,
             bytes_accessed=12 * length * head_dim,
             transcendentals=length * length,
         ),
-    )(queries, key_rows, value_rows, decay_row, decay_column, cosine, sine)
+    )(queries, key_rows, value_rows, decay_row, cosine, sine)
 
     def index_line(axis):
         return jnp.full((1, head_dim), lax.axis_index(axis), jnp.int32)
@@ -579,7 +601,7 @@
         ahead,
         rotated_queries,
         within,
-        decay_column,
+        decay_row,
         gate_rows,
         out_gain[None],
     )

time: 215 us -> 212 us (0.986)
  waiting for transfers between devices: 81.2 us -> 79 us
    pallas_call x4, Pallas kernels: 25.7 us -> 23.3 us  [expert(): pl.pallas_call(lambda *refs: expert_kernel(*refs, count=count, ready=len(...]
where the time goes in v4:
time: 212 us; the launch traced here: 210 us
  waiting for transfers between devices  79 us (37%)
  starting transfers between devices  47 us (22%)
  Pallas kernels  39.8 us (19%)
  blocking collectives  36.5 us (17%)
  local copies, waits for them, and re-layouts  6.24 us (3%)
    ppermute x33, waiting for transfers between devices, shift(): return lax.ppermute(a, 'tp', where)  50.9 us
    all_to_all x1, blocking collectives, layer(): landed = lax.all_to_all(tokens.reshape(message), SP, 0, 0, tiled=True)  36.5 us
    ppermute x33, starting transfers between devices, shift(): return lax.ppermute(a, 'tp', where)  24.4 us
    pallas_call x4, Pallas kernels, expert(): pl.pallas_call(lambda *refs: expert_kernel(*refs, count=count, ready=len(...  23.3 us
    all_to_all x1, waiting for transfers between devices, layer(): returned = lax.all_to_all(repacked.reshape(message), SP, 0, 0, tiled=True)  21.7 us
    pallas_call x15, Pallas kernels, call(): pl.pallas_call(body, in_specs=[pl.BlockSpec(memory_space=pltpu.HBM if k i...  16.5 us
    all_to_all x1, starting transfers between devices, layer(): pieces = lax.all_to_all(message, 'sp_0', 0, 0, tiled=True)  7.94 us
    all_to_all x1, waiting for transfers between devices, layer(): lax.all_to_all(mixed.reshape(tp_count, row_count, head_dim), 'tp', 0, 0,...  5.73 us
  transfers between devices with their start and end apart: 37, of which 12 were waited for; matrix products, arithmetic and copies ran while one was open for 1% of the time, Pallas kernels for 14%

profile of v4, /device:TPU:2, one launch (start us, length us, event | category | flops | bytes accessed | tf_op | source)
XLA Modules:
  0.0 210.5 jit_solution(4954334859704245764)
XLA Ops:
  0.3 2.6 %shard_map.136 = (f32[1,768]{1,0:T(1,128)S(1)}, bf16[4,136,128]{2,1,0:T(8,128)(2,1)}) custom-call(bf16[768,128]{1,0:T(8,128)(2,1)} %refs_1_.4, bf16[768,128]{1,0:T(8,128)(2,1)} %refs_2_.4, f32[1,768]{1,0:T(1,128)} %refs_2_.3, f32[56,128]{1,0:T(8,128)S(1)} %get-tuple-element.72.refs_3_.refs_4_, f32[56,128]{1,0:T(8,128)S(1)} %get-tuple-element.71.refs_4_.refs_5_), custom_call_target="tpu_custom_call" | custom-call | tf_op jit(solution)/shard_map/pallas_call | solution.py:69
  2.9 5.6 %all-to-all-start = ((bf16[4,136,128]{2,1,0:T(8,128)(2,1)}), bf16[4,136,128]{2,1,0:T(8,128)(2,1)S(1)}, u32[]{:S(2)}, u32[]{:S(2)}) async-start(bf16[4,136,128]{2,1,0:T(8,128)(2,1)} %get-tuple-element.37), calls=%async_computation | async-start | bytes 278528 | tf_op jit(solution)/shard_map/all_to_all | solution.py:573
  8.5 2.3 %collective-permute-start = (bf16[128,2048]{1,0:T(8,128)(2,1)}, bf16[128,2048]{1,0:T(8,128)(2,1)S(1)}, u32[]{:S(2)}, u32[]{:S(2)}) collective-permute-start(bf16[128,2048]{1,0:T(8,128)(2,1)} %refs_2_.5), channel_id=1, source_target_pairs={{0,6},{1,7},{2,0},{3,1},{4,2},{5,3},{6,4},{7,5},{8,14},{9,15},{10,... | collective-permute-start | bytes 1572872 | tf_op jit(solution)/shard_map/ppermute | solution.py:339
  13.8 7.9 %all-to-all-start.1 = ((bf16[8,136,128]{2,1,0:T(8,128)(2,1)}), bf16[8,136,128]{2,1,0:T(8,128)(2,1)S(1)}, u32[]{:S(2)}, u32[]{:S(2)}) async-start(bf16[8,136,128]{2,1,0:T(8,128)(2,1)} %get-tuple-element.38), calls=%async_computation.1 | async-start | bytes 557056 | tf_op jit(solution)/shard_map/all_to_all | solution.py:596
  26.6 1.8 shard_map.138
  29.8 3.1 %collective-permute-done.refs_3_ = bf16[128,2048]{1,0:T(8,128)(2,1)S(1)} collective-permute-done((bf16[128,2048]{1,0:T(8,128)(2,1)}, bf16[128,2048]{1,0:T(8,128)(2,1)S(1)}, u32[]{:S(2)}, u32[]{:S(2)}) %collective-permute-start) | collective-permute-done | bytes 524320 | tf_op jit(solution)/shard_map/ppermute | solution.py:339
  33.5 3.1 %collective-permute-done.2.refs_5_ = bf16[128,2048]{1,0:T(8,128)(2,1)S(1)} collective-permute-done((bf16[128,2048]{1,0:T(8,128)(2,1)}, bf16[128,2048]{1,0:T(8,128)(2,1)S(1)}, u32[]{:S(2)}, u32[]{:S(2)}) %collective-permute-start.2) | collective-permute-done | bytes 524320 | tf_op jit(solution)/shard_map/ppermute | solution.py:339
  36.6 2.2 %shard_map.139 = bf16[768,128]{1,0:T(8,128)(2,1)} custom-call(bf16[8,136,128]{2,1,0:T(8,128)(2,1)S(1)} %all-to-all-done.1.refs_0_, s32[1,128]{1,0:T(1,128)S(1)} %broadcast_in_dim.29.refs_1_, f32[128,128]{1,0:T(8,128)S(1)} %get-tuple-element.39.refs_2_, f32[1,128]{1,0:T(1,128)S(1)} %get-tuple-element.40.refs_3_, bf16[768,128]{1,0:T(8,128)(2,1)} %copy-done.6, ...), custom_call_target="tpu_custom_call" | custom-call | tf_op jit(solution)/shard_map/pallas_call | solution.py:69
  38.8 3.4 %all-to-all-start.2 = ((bf16[8,96,128]{2,1,0:T(8,128)(2,1)}), bf16[8,96,128]{2,1,0:T(8,128)(2,1)S(1)}, u32[]{:S(2)}, u32[]{:S(2)}) async-start(bf16[8,96,128]{2,1,0:T(8,128)(2,1)} %bitcast.1), calls=%async_computation.2 | async-start | bytes 393216 | tf_op jit(solution)/shard_map/all_to_all | solution.py:615
  43.2 5.7 %all-to-all-done.2 = bf16[8,96,128]{2,1,0:T(8,128)(2,1)S(1)} async-done(((bf16[8,96,128]{2,1,0:T(8,128)(2,1)}), bf16[8,96,128]{2,1,0:T(8,128)(2,1)S(1)}, u32[]{:S(2)}, u32[]{:S(2)}) %all-to-all-start.2) | async-done | bytes 196640 | tf_op jit(solution)/shard_map/all_to_all | solution.py:615
  49.1 4.2 %shard_map.140 = (bf16[96,2048]{1,0:T(8,128)(2,1)S(1)}, bf16[256,1792]{1,0:T(8,128)(2,1)S(1)}) custom-call(bf16[4,96,128]{2,1,0:T(8,128)(2,1)S(1)} %get-tuple-element.70.refs_0_, bf16[4,96,128]{2,1,0:T(8,128)(2,1)S(1)} %get-tuple-element.69.refs_1_, bf16[128,2048]{1,0:T(8,128)(2,1)S(1)} %copy-done, bf16[128,2048]{1,0:T(8,128)(2,1)S(1)} %collective-permute-done.refs_3_, ...), custom_call_target="tpu_custom_call" | custom-call | tf_op jit(solution)/shard_map/pallas_call | solution.py:69
  53.4 36.5 %all_to_all.25 = bf16[32,8,1792]{2,1,0:T(8,128)(2,1)S(1)} all-to-all(bf16[32,8,1792]{2,1,0:T(8,128)(2,1)S(1)} %bitcast.27), channel_id=1, replica_groups=mesh['sp_0'=8,'sp_1'=4,'tp'=8] {'sp_0','sp_1'}, dimensions={0} | all-to-all | bytes 1835008 | tf_op jit(solution)/shard_map/all_to_all | solution.py:635
  91.2 2.7 %collective-permute-start.9 = (bf16[112,2048]{1,0:T(8,128)(2,1)S(1)}, bf16[112,2048]{1,0:T(8,128)(2,1)S(1)}, u32[]{:S(2)}, u32[]{:S(2)}) collective-permute-start(bf16[112,2048]{1,0:T(8,128)(2,1)S(1)} %get-tuple-element.46.refs_1_), channel_id=1, source_target_pairs={{0,6},{1,7},{2,0},{3,1},{4,2},{5,3},{6,4},{7,5},{8,14},{9,15},{10,... | collective-permute-start | bytes 1376264 | tf_op jit(solution)/shard_map/ppermute | solution.py:339
  93.8 10.8 %collective-permute-done.8.refs_0_ = bf16[112,2048]{1,0:T(8,128)(2,1)S(1)} collective-permute-done((bf16[112,2048]{1,0:T(8,128)(2,1)S(1)}, bf16[112,2048]{1,0:T(8,128)(2,1)S(1)}, u32[]{:S(2)}, u32[]{:S(2)}) %collective-permute-start.8) | collective-permute-done | bytes 458784 | tf_op jit(solution)/shard_map/ppermute | solution.py:339
  104.6 3.2 %collective-permute-start.19 = (bf16[112,2048]{1,0:T(8,128)(2,1)S(1)}, bf16[112,2048]{1,0:T(8,128)(2,1)S(1)}, u32[]{:S(2)}, u32[]{:S(2)}) collective-permute-start(bf16[112,2048]{1,0:T(8,128)(2,1)S(1)} %collective-permute-done.9.refs_1_), channel_id=1, source_target_pairs={{0,6},{1,7},{2,0},{3,1},{4,2},{5,3},{6,4},{7,5},{8,14},{9,15},{10,... | collective-permute-start | bytes 1376264 | tf_op jit(solution)/shard_map/ppermute | solution.py:339
  108.4 6.8 %shard_map.142 = (bf16[112,2048]{1,0:T(8,128)(2,1)S(1)}, bf16[112,2048]{1,0:T(8,128)(2,1)S(1)}, bf16[224,2048]{1,0:T(8,128)(2,1)S(1)}) custom-call(bf16[112,2048]{1,0:T(8,128)(2,1)S(1)} %get-tuple-element.45.refs_0_, bf16[112,2048]{1,0:T(8,128)(2,1)S(1)} %get-tuple-element.46.refs_1_, bf16[224,2048]{1,0:T(8,128)(2,1)S(1)} %collective-permute-done.7.refs_2_, ...), custom_call_target="tpu_custom_call" | custom-call | flops 2818572288 | bytes 9961472 | tf_op jit(solution)/shard_map/pallas_call | solution.py:314
  115.3 4.0 %collective-permute-done.18.refs_0_ = bf16[112,2048]{1,0:T(8,128)(2,1)S(1)} collective-permute-done((bf16[112,2048]{1,0:T(8,128)(2,1)S(1)}, bf16[112,2048]{1,0:T(8,128)(2,1)S(1)}, u32[]{:S(2)}, u32[]{:S(2)}) %collective-permute-start.18) | collective-permute-done | bytes 458784 | tf_op jit(solution)/shard_map/ppermute | solution.py:339
  119.8 6.9 %shard_map.143 = (bf16[112,2048]{1,0:T(8,128)(2,1)S(1)}, bf16[112,2048]{1,0:T(8,128)(2,1)S(1)}, bf16[448,2048]{1,0:T(8,128)(2,1)S(1)}) custom-call(bf16[112,2048]{1,0:T(8,128)(2,1)S(1)} %collective-permute-done.8.refs_0_, bf16[112,2048]{1,0:T(8,128)(2,1)S(1)} %collective-permute-done.9.refs_1_, bf16[112,2048]{1,0:T(8,128)(2,1)S(1)} %collective-permute-done.10.refs_2_, ...), custom_call_target="tpu_custom_call" | custom-call | flops 2818572288 | bytes 9961472 | tf_op jit(solution)/shard_map/pallas_call | solution.py:314
  127.7 1.3 collective-permute-done.14.refs_1_
  129.0 4.5 %shard_map.145 = (bf16[112,2048]{1,0:T(8,128)(2,1)S(1)}, bf16[112,2048]{1,0:T(8,128)(2,1)S(1)}, bf16[224,2048]{1,0:T(8,128)(2,1)S(1)}) custom-call(bf16[112,2048]{1,0:T(8,128)(2,1)S(1)} %collective-permute-done.18.refs_0_, bf16[112,2048]{1,0:T(8,128)(2,1)S(1)} %collective-permute-done.19.refs_1_, bf16[112,2048]{1,0:T(8,128)(2,1)S(1)} %collective-permute-done.20.refs_2_, ...), custom_call_target="tpu_custom_call" | custom-call | flops 2818572288 | bytes 9961472 | tf_op jit(solution)/shard_map/pallas_call | solution.py:314
  134.1 5.1 %shard_map.144 = (bf16[112,2048]{1,0:T(8,128)(2,1)S(1)}, bf16[112,2048]{1,0:T(8,128)(2,1)S(1)}, bf16[224,2048]{1,0:T(8,128)(2,1)S(1)}) custom-call(bf16[112,2048]{1,0:T(8,128)(2,1)S(1)} %collective-permute-done.13.refs_0_, bf16[112,2048]{1,0:T(8,128)(2,1)S(1)} %collective-permute-done.14.refs_1_, bf16[112,2048]{1,0:T(8,128)(2,1)S(1)} %collective-permute-done.15.refs_2_, ...), custom_call_target="tpu_custom_call" | custom-call | flops 2818572288 | bytes 9961472 | tf_op jit(solution)/shard_map/pallas_call | solution.py:314
  139.8 3.1 %collective-permute-start.29 = (bf16[64,2048]{1,0:T(8,128)(2,1)S(1)}, bf16[64,2048]{1,0:T(8,128)(2,1)S(1)}, u32[]{:S(2)}, u32[]{:S(2)}) collective-permute-start(bf16[64,2048]{1,0:T(8,128)(2,1)S(1)} %get-tuple-element.64), channel_id=1, source_target_pairs={{0,6},{1,7},{2,0},{3,1},{4,2},{5,3},{6,4},{7,5},{8,14},{9,15},{10,... | collective-permute-start | bytes 786440 | tf_op jit(solution)/shard_map/ppermute | solution.py:339
  143.0 1.9 collective-permute-start.23
  145.4 8.0 %collective-permute-done.31.refs_2_ = bf16[48,2048]{1,0:T(8,128)(2,1)S(1)} collective-permute-done((bf16[48,2048]{1,0:T(8,128)(2,1)S(1)}, bf16[48,2048]{1,0:T(8,128)(2,1)S(1)}, u32[]{:S(2)}, u32[]{:S(2)}) %collective-permute-start.31) | collective-permute-done | bytes 196640 | tf_op jit(solution)/shard_map/ppermute | solution.py:339
  153.3 3.7 %collective-permute-start.28 = (bf16[112,2048]{1,0:T(8,128)(2,1)S(1)}, bf16[112,2048]{1,0:T(8,128)(2,1)S(1)}, u32[]{:S(2)}, u32[]{:S(2)}) collective-permute-start(bf16[112,2048]{1,0:T(8,128)(2,1)S(1)} %get-tuple-element.62), channel_id=1, source_target_pairs={{0,6},{1,7},{2,0},{3,1},{4,2},{5,3},{6,4},{7,5},{8,14},{9,15},{10,... | collective-permute-start | bytes 1376264 | tf_op jit(solution)/shard_map/ppermute | solution.py:339
  157.6 2.1 collective-permute-start.24
  159.7 12.4 %collective-permute-done.32.refs_8_ = bf16[48,2048]{1,0:T(8,128)(2,1)S(1)} collective-permute-done((bf16[48,2048]{1,0:T(8,128)(2,1)S(1)}, bf16[48,2048]{1,0:T(8,128)(2,1)S(1)}, u32[]{:S(2)}, u32[]{:S(2)}) %collective-permute-start.32) | collective-permute-done | bytes 196640 | tf_op jit(solution)/shard_map/ppermute | solution.py:339
  172.1 7.3 %collective-permute-done.26.refs_4_ = bf16[48,2048]{1,0:T(8,128)(2,1)S(1)} collective-permute-done((bf16[48,2048]{1,0:T(8,128)(2,1)S(1)}, bf16[48,2048]{1,0:T(8,128)(2,1)S(1)}, u32[]{:S(2)}, u32[]{:S(2)}) %collective-permute-start.26) | collective-permute-done | bytes 196640 | tf_op jit(solution)/shard_map/ppermute | solution.py:339
  179.5 1.7 shard_map.152
  181.2 5.7 %all-to-all-start.4 = ((bf16[32,8,1792]{2,1,0:T(8,128)(2,1)}), bf16[32,8,1792]{2,1,0:T(8,128)(2,1)S(1)}, u32[]{:S(2)}, u32[]{:S(2)}) async-start(bf16[32,8,1792]{2,1,0:T(8,128)(2,1)} %bitcast.9), calls=%async_computation.4 | async-start | bytes 1835008 | tf_op jit(solution)/shard_map/all_to_all | solution.py:647
  187.2 21.7 %all-to-all-done.4 = bf16[32,8,1792]{2,1,0:T(8,128)(2,1)S(1)} async-done(((bf16[32,8,1792]{2,1,0:T(8,128)(2,1)}), bf16[32,8,1792]{2,1,0:T(8,128)(2,1)S(1)}, u32[]{:S(2)}, u32[]{:S(2)}) %all-to-all-start.4) | async-done | bytes 917536 | tf_op jit(solution)/shard_map/all_to_all | solution.py:647
  208.9 1.6 shard_map.154
  (111 shorter events, 17.0 us)
Async XLA Ops:
  2.9 10.1 %all-to-all-start = ((bf16[4,136,128]{2,1,0:T(8,128)(2,1)}), bf16[4,136,128]{2,1,0:T(8,128)(2,1)S(1)}, u32[]{:S(2)}, u32[]{:S(2)}) async-start(bf16[4,136,128]{2,1,0:T(8,128)(2,1)} %get-tuple-element.37), calls=%async_computation | async-start | bytes 278528 | tf_op jit(solution)/shard_map/all_to_all | solution.py:573
  8.5 24.5 %collective-permute-start = (bf16[128,2048]{1,0:T(8,128)(2,1)}, bf16[128,2048]{1,0:T(8,128)(2,1)S(1)}, u32[]{:S(2)}, u32[]{:S(2)}) collective-permute-start(bf16[128,2048]{1,0:T(8,128)(2,1)} %refs_2_.5), channel_id=1, source_target_pairs={{0,6},{1,7},{2,0},{3,1},{4,2},{5,3},{6,4},{7,5},{8,14},{9,15},{10,... | collective-permute-start | bytes 1572872 | tf_op jit(solution)/shard_map/ppermute | solution.py:339
  10.8 22.2 %collective-permute-start.1 = (bf16[128,2048]{1,0:T(8,128)(2,1)}, bf16[128,2048]{1,0:T(8,128)(2,1)S(1)}, u32[]{:S(2)}, u32[]{:S(2)}) collective-permute-start(bf16[128,2048]{1,0:T(8,128)(2,1)} %refs_2_.5), channel_id=1, source_target_pairs={{0,4},{1,5},{2,6},{3,7},{4,0},{5,1},{6,2},{7,3},{8,12},{9,13},{10,... | collective-permute-start | bytes 1572872 | tf_op jit(solution)/shard_map/ppermute | solution.py:339
  11.4 25.1 %collective-permute-start.2 = (bf16[128,2048]{1,0:T(8,128)(2,1)}, bf16[128,2048]{1,0:T(8,128)(2,1)S(1)}, u32[]{:S(2)}, u32[]{:S(2)}) collective-permute-start(bf16[128,2048]{1,0:T(8,128)(2,1)} %refs_2_.5), channel_id=1, source_target_pairs={{0,2},{1,3},{2,4},{3,5},{4,6},{5,7},{6,0},{7,1},{8,10},{9,11},{10,... | collective-permute-start | bytes 1572872 | tf_op jit(solution)/shard_map/ppermute | solution.py:339
  13.8 22.8 %all-to-all-start.1 = ((bf16[8,136,128]{2,1,0:T(8,128)(2,1)}), bf16[8,136,128]{2,1,0:T(8,128)(2,1)S(1)}, u32[]{:S(2)}, u32[]{:S(2)}) async-start(bf16[8,136,128]{2,1,0:T(8,128)(2,1)} %get-tuple-element.38), calls=%async_computation.1 | async-start | bytes 557056 | tf_op jit(solution)/shard_map/all_to_all | solution.py:596
  21.7 27.3 %collective-permute-start.3 = (bf16[128,2048]{1,0:T(8,128)(2,1)}, bf16[128,2048]{1,0:T(8,128)(2,1)S(1)}, u32[]{:S(2)}, u32[]{:S(2)}) collective-permute-start(bf16[128,2048]{1,0:T(8,128)(2,1)} %refs_2_.5), channel_id=1, source_target_pairs={{0,1},{1,0},{2,3},{3,2},{4,5},{5,4},{6,7},{7,6},{8,9},{9,8},{10,11... | collective-permute-start | bytes 1572872 | tf_op jit(solution)/shard_map/ppermute | solution.py:339
  33.0 16.1 %collective-permute-start.4 = (bf16[128,2048]{1,0:T(8,128)(2,1)S(1)}, bf16[128,2048]{1,0:T(8,128)(2,1)S(1)}, u32[]{:S(2)}, u32[]{:S(2)}) collective-permute-start(bf16[128,2048]{1,0:T(8,128)(2,1)S(1)} %collective-permute-done.refs_3_), channel_id=1, source_target_pairs={{0,1},{1,0},{2,3},{3,2},{4,5},{5,4},{6,7},{7,6},{8,9},{9,8},{10,11... | collective-permute-start | bytes 1572872 | tf_op jit(solution)/shard_map/ppermute | solution.py:339
  33.0 16.1 %collective-permute-start.5 = (bf16[128,2048]{1,0:T(8,128)(2,1)S(1)}, bf16[128,2048]{1,0:T(8,128)(2,1)}, u32[]{:S(2)}, u32[]{:S(2)}) collective-permute-start(bf16[128,2048]{1,0:T(8,128)(2,1)S(1)} %collective-permute-done.1.refs_4_), channel_id=1, source_target_pairs={{0,1},{1,0},{2,3},{3,2},{4,5},{5,4},{6,7},{7,6},{8,9},{9,8},{10,11... | collective-permute-start | bytes 1572872 | tf_op jit(solution)/shard_map/ppermute | solution.py:339
  36.6 12.5 %collective-permute-start.6 = (bf16[128,2048]{1,0:T(8,128)(2,1)S(1)}, bf16[128,2048]{1,0:T(8,128)(2,1)}, u32[]{:S(2)}, u32[]{:S(2)}) collective-permute-start(bf16[128,2048]{1,0:T(8,128)(2,1)S(1)} %collective-permute-done.2.refs_5_), channel_id=1, source_target_pairs={{0,1},{1,0},{2,3},{3,2},{4,5},{5,4},{6,7},{7,6},{8,9},{9,8},{10,11... | collective-permute-start | bytes 1572872 | tf_op jit(solution)/shard_map/ppermute | solution.py:339
  38.8 10.1 %all-to-all-start.2 = ((bf16[8,96,128]{2,1,0:T(8,128)(2,1)}), bf16[8,96,128]{2,1,0:T(8,128)(2,1)S(1)}, u32[]{:S(2)}, u32[]{:S(2)}) async-start(bf16[8,96,128]{2,1,0:T(8,128)(2,1)} %bitcast.1), calls=%async_computation.2 | async-start | bytes 393216 | tf_op jit(solution)/shard_map/all_to_all | solution.py:615
  90.4 18.0 %collective-permute-start.7 = (bf16[224,2048]{1,0:T(8,128)(2,1)S(1)}, bf16[224,2048]{1,0:T(8,128)(2,1)S(1)}, u32[]{:S(2)}, u32[]{:S(2)}) collective-permute-start(bf16[224,2048]{1,0:T(8,128)(2,1)S(1)} %get-tuple-element.47), channel_id=1, source_target_pairs={{0,1},{1,0},{2,3},{3,2},{4,5},{5,4},{6,7},{7,6},{8,9},{9,8},{10,11... | collective-permute-start | bytes 2752520 | tf_op jit(solution)/shard_map/ppermute | solution.py:339
  90.5 14.1 %collective-permute-start.8 = (bf16[112,2048]{1,0:T(8,128)(2,1)S(1)}, bf16[112,2048]{1,0:T(8,128)(2,1)S(1)}, u32[]{:S(2)}, u32[]{:S(2)}) collective-permute-start(bf16[112,2048]{1,0:T(8,128)(2,1)S(1)} %get-tuple-element.45.refs_0_), channel_id=1, source_target_pairs={{0,2},{1,3},{2,4},{3,5},{4,6},{5,7},{6,0},{7,1},{8,10},{9,11},{10,... | collective-permute-start | bytes 1376264 | tf_op jit(solution)/shard_map/ppermute | solution.py:339
  91.2 13.5 %collective-permute-start.9 = (bf16[112,2048]{1,0:T(8,128)(2,1)S(1)}, bf16[112,2048]{1,0:T(8,128)(2,1)S(1)}, u32[]{:S(2)}, u32[]{:S(2)}) collective-permute-start(bf16[112,2048]{1,0:T(8,128)(2,1)S(1)} %get-tuple-element.46.refs_1_), channel_id=1, source_target_pairs={{0,6},{1,7},{2,0},{3,1},{4,2},{5,3},{6,4},{7,5},{8,14},{9,15},{10,... | collective-permute-start | bytes 1376264 | tf_op jit(solution)/shard_map/ppermute | solution.py:339
  104.6 14.6 %collective-permute-start.18 = (bf16[112,2048]{1,0:T(8,128)(2,1)S(1)}, bf16[112,2048]{1,0:T(8,128)(2,1)S(1)}, u32[]{:S(2)}, u32[]{:S(2)}) collective-permute-start(bf16[112,2048]{1,0:T(8,128)(2,1)S(1)} %collective-permute-done.8.refs_0_), channel_id=1, source_target_pairs={{0,2},{1,3},{2,4},{3,5},{4,6},{5,7},{6,0},{7,1},{8,10},{9,11},{10,... | collective-permute-start | bytes 1376264 | tf_op jit(solution)/shard_map/ppermute | solution.py:339
  104.6 14.6 %collective-permute-start.19 = (bf16[112,2048]{1,0:T(8,128)(2,1)S(1)}, bf16[112,2048]{1,0:T(8,128)(2,1)S(1)}, u32[]{:S(2)}, u32[]{:S(2)}) collective-permute-start(bf16[112,2048]{1,0:T(8,128)(2,1)S(1)} %collective-permute-done.9.refs_1_), channel_id=1, source_target_pairs={{0,6},{1,7},{2,0},{3,1},{4,2},{5,3},{6,4},{7,5},{8,14},{9,15},{10,... | collective-permute-start | bytes 1376264 | tf_op jit(solution)/shard_map/ppermute | solution.py:339
  107.9 11.4 %collective-permute-start.10 = (bf16[112,2048]{1,0:T(8,128)(2,1)S(1)}, bf16[112,2048]{1,0:T(8,128)(2,1)S(1)}, u32[]{:S(2)}, u32[]{:S(2)}) collective-permute-start(bf16[112,2048]{1,0:T(8,128)(2,1)S(1)} %collective-permute-done.8.refs_0_), channel_id=1, source_target_pairs={{0,1},{1,0},{2,3},{3,2},{4,5},{5,4},{6,7},{7,6},{8,9},{9,8},{10,11... | collective-permute-start | bytes 1376264 | tf_op jit(solution)/shard_map/ppermute | solution.py:339
  107.9 11.9 %collective-permute-start.11 = (bf16[112,2048]{1,0:T(8,128)(2,1)S(1)}, bf16[112,2048]{1,0:T(8,128)(2,1)S(1)}, u32[]{:S(2)}, u32[]{:S(2)}) collective-permute-start(bf16[112,2048]{1,0:T(8,128)(2,1)S(1)} %collective-permute-done.9.refs_1_), channel_id=1, source_target_pairs={{0,1},{1,0},{2,3},{3,2},{4,5},{5,4},{6,7},{7,6},{8,9},{9,8},{10,11... | collective-permute-start | bytes 1376264 | tf_op jit(solution)/shard_map/ppermute | solution.py:339
  108.4 19.3 %collective-permute-start.13 = (bf16[112,2048]{1,0:T(8,128)(2,1)S(1)}, bf16[112,2048]{1,0:T(8,128)(2,1)S(1)}, u32[]{:S(2)}, u32[]{:S(2)}) collective-permute-start(bf16[112,2048]{1,0:T(8,128)(2,1)S(1)} %get-tuple-element.46.refs_1_), channel_id=1, source_target_pairs={{0,2},{1,3},{2,4},{3,5},{4,6},{5,7},{6,0},{7,1},{8,10},{9,11},{10,... | collective-permute-start | bytes 1376264 | tf_op jit(solution)/shard_map/ppermute | solution.py:339
  119.2 9.7 %collective-permute-start.14 = (bf16[112,2048]{1,0:T(8,128)(2,1)S(1)}, bf16[112,2048]{1,0:T(8,128)(2,1)S(1)}, u32[]{:S(2)}, u32[]{:S(2)}) collective-permute-start(bf16[112,2048]{1,0:T(8,128)(2,1)S(1)} %get-tuple-element.45.refs_0_), channel_id=1, source_target_pairs={{0,6},{1,7},{2,0},{3,1},{4,2},{5,3},{6,4},{7,5},{8,14},{9,15},{10,... | collective-permute-start | bytes 1376264 | tf_op jit(solution)/shard_map/ppermute | solution.py:339
  119.2 9.7 %collective-permute-start.20 = (bf16[112,2048]{1,0:T(8,128)(2,1)S(1)}, bf16[112,2048]{1,0:T(8,128)(2,1)S(1)}, u32[]{:S(2)}, u32[]{:S(2)}) collective-permute-start(bf16[112,2048]{1,0:T(8,128)(2,1)S(1)} %collective-permute-done.18.refs_0_), channel_id=1, source_target_pairs={{0,1},{1,0},{2,3},{3,2},{4,5},{5,4},{6,7},{7,6},{8,9},{9,8},{10,11... | collective-permute-start | bytes 1376264 | tf_op jit(solution)/shard_map/ppermute | solution.py:339
  119.3 9.7 %collective-permute-start.21 = (bf16[112,2048]{1,0:T(8,128)(2,1)S(1)}, bf16[112,2048]{1,0:T(8,128)(2,1)S(1)}, u32[]{:S(2)}, u32[]{:S(2)}) collective-permute-start(bf16[112,2048]{1,0:T(8,128)(2,1)S(1)} %collective-permute-done.19.refs_1_), channel_id=1, source_target_pairs={{0,1},{1,0},{2,3},{3,2},{4,5},{5,4},{6,7},{7,6},{8,9},{9,8},{10,11... | collective-permute-start | bytes 1376264 | tf_op jit(solution)/shard_map/ppermute | solution.py:339
  126.7 18.3 %collective-permute-start.12 = (bf16[448,2048]{1,0:T(8,128)(2,1)S(1)}, bf16[448,2048]{1,0:T(8,128)(2,1)S(1)}, u32[]{:S(2)}, u32[]{:S(2)}) collective-permute-start(bf16[448,2048]{1,0:T(8,128)(2,1)S(1)} %get-tuple-element.51), channel_id=1, source_target_pairs={{0,1},{1,0},{2,3},{3,2},{4,5},{5,4},{6,7},{7,6},{8,9},{9,8},{10,11... | collective-permute-start | bytes 5505032 | tf_op jit(solution)/shard_map/ppermute | solution.py:339
  139.8 17.3 %collective-permute-start.29 = (bf16[64,2048]{1,0:T(8,128)(2,1)S(1)}, bf16[64,2048]{1,0:T(8,128)(2,1)S(1)}, u32[]{:S(2)}, u32[]{:S(2)}) collective-permute-start(bf16[64,2048]{1,0:T(8,128)(2,1)S(1)} %get-tuple-element.64), channel_id=1, source_target_pairs={{0,6},{1,7},{2,0},{3,1},{4,2},{5,3},{6,4},{7,5},{8,14},{9,15},{10,... | collective-permute-start | bytes 786440 | tf_op jit(solution)/shard_map/ppermute | solution.py:339
  142.9 10.4 %collective-permute-start.31 = (bf16[48,2048]{1,0:T(8,128)(2,1)S(1)}, bf16[48,2048]{1,0:T(8,128)(2,1)S(1)}, u32[]{:S(2)}, u32[]{:S(2)}) collective-permute-start(bf16[48,2048]{1,0:T(8,128)(2,1)S(1)} %get-tuple-element.65), channel_id=1, source_target_pairs={{0,6},{1,7},{2,0},{3,1},{4,2},{5,3},{6,4},{7,5},{8,14},{9,15},{10,... | collective-permute-start | bytes 589832 | tf_op jit(solution)/shard_map/ppermute | solution.py:339
  143.0 14.3 %collective-permute-start.23 = (bf16[64,2048]{1,0:T(8,128)(2,1)S(1)}, bf16[64,2048]{1,0:T(8,128)(2,1)S(1)}, u32[]{:S(2)}, u32[]{:S(2)}) collective-permute-start(bf16[64,2048]{1,0:T(8,128)(2,1)S(1)} %get-tuple-element.57), channel_id=1, source_target_pairs={{0,2},{1,3},{2,4},{3,5},{4,6},{5,7},{6,0},{7,1},{8,10},{9,11},{10,... | collective-permute-start | bytes 786440 | tf_op jit(solution)/shard_map/ppermute | solution.py:339
  144.9 12.7 %collective-permute-start.25 = (bf16[48,2048]{1,0:T(8,128)(2,1)S(1)}, bf16[48,2048]{1,0:T(8,128)(2,1)S(1)}, u32[]{:S(2)}, u32[]{:S(2)}) collective-permute-start(bf16[48,2048]{1,0:T(8,128)(2,1)S(1)} %get-tuple-element.58), channel_id=1, source_target_pairs={{0,2},{1,3},{2,4},{3,5},{4,6},{5,7},{6,0},{7,1},{8,10},{9,11},{10,... | collective-permute-start | bytes 589832 | tf_op jit(solution)/shard_map/ppermute | solution.py:339
  145.3 34.2 %collective-permute-start.27 = (bf16[112,2048]{1,0:T(8,128)(2,1)S(1)}, bf16[112,2048]{1,0:T(8,128)(2,1)S(1)}, u32[]{:S(2)}, u32[]{:S(2)}) collective-permute-start(bf16[112,2048]{1,0:T(8,128)(2,1)S(1)} %get-tuple-element.61), channel_id=1, source_target_pairs={{0,2},{1,3},{2,4},{3,5},{4,6},{5,7},{6,0},{7,1},{8,10},{9,11},{10,... | collective-permute-start | bytes 1376264 | tf_op jit(solution)/shard_map/ppermute | solution.py:339
  153.3 26.2 %collective-permute-start.28 = (bf16[112,2048]{1,0:T(8,128)(2,1)S(1)}, bf16[112,2048]{1,0:T(8,128)(2,1)S(1)}, u32[]{:S(2)}, u32[]{:S(2)}) collective-permute-start(bf16[112,2048]{1,0:T(8,128)(2,1)S(1)} %get-tuple-element.62), channel_id=1, source_target_pairs={{0,6},{1,7},{2,0},{3,1},{4,2},{5,3},{6,4},{7,5},{8,14},{9,15},{10,... | collective-permute-start | bytes 1376264 | tf_op jit(solution)/shard_map/ppermute | solution.py:339
  157.1 15.0 %collective-permute-start.32 = (bf16[48,2048]{1,0:T(8,128)(2,1)S(1)}, bf16[48,2048]{1,0:T(8,128)(2,1)S(1)}, u32[]{:S(2)}, u32[]{:S(2)}) collective-permute-start(bf16[48,2048]{1,0:T(8,128)(2,1)S(1)} %shard_map.151), channel_id=1, source_target_pairs={{0,6},{1,7},{2,0},{3,1},{4,2},{5,3},{6,4},{7,5},{8,14},{9,15},{10,... | collective-permute-start | bytes 589832 | tf_op jit(solution)/shard_map/ppermute | solution.py:339
  157.3 22.1 %collective-permute-start.30 = (bf16[64,2048]{1,0:T(8,128)(2,1)S(1)}, bf16[64,2048]{1,0:T(8,128)(2,1)S(1)}, u32[]{:S(2)}, u32[]{:S(2)}) collective-permute-start(bf16[64,2048]{1,0:T(8,128)(2,1)S(1)} %shard_map.150), channel_id=1, source_target_pairs={{0,6},{1,7},{2,0},{3,1},{4,2},{5,3},{6,4},{7,5},{8,14},{9,15},{10,... | collective-permute-start | bytes 786440 | tf_op jit(solution)/shard_map/ppermute | solution.py:339
  157.6 21.9 %collective-permute-start.24 = (bf16[64,2048]{1,0:T(8,128)(2,1)S(1)}, bf16[64,2048]{1,0:T(8,128)(2,1)S(1)}, u32[]{:S(2)}, u32[]{:S(2)}) collective-permute-start(bf16[64,2048]{1,0:T(8,128)(2,1)S(1)} %shard_map.147), channel_id=1, source_target_pairs={{0,2},{1,3},{2,4},{3,5},{4,6},{5,7},{6,0},{7,1},{8,10},{9,11},{10,... | collective-permute-start | bytes 786440 | tf_op jit(solution)/shard_map/ppermute | solution.py:339
  181.2 27.7 %all-to-all-start.4 = ((bf16[32,8,1792]{2,1,0:T(8,128)(2,1)}), bf16[32,8,1792]{2,1,0:T(8,128)(2,1)S(1)}, u32[]{:S(2)}, u32[]{:S(2)}) async-start(bf16[32,8,1792]{2,1,0:T(8,128)(2,1)} %bitcast.9), calls=%async_computation.4 | async-start | bytes 1835008 | tf_op jit(solution)/shard_map/all_to_all | solution.py:647
  (20 other events, 437.5 us)
